TPU v7x, 32 devices: a whole 2x2x4 slice. The times are simulated.
32 devices in a mesh: grp: 2 (over y), kv: 4 (over z), tp: 4 (over x, core).
Axes of the slice: x: 2, y: 2, z: 4, core: 2. Of those that a mesh axis runs over, the one named last changes fastest.
Arguments:
- tokens: bfloat16 [8, 3, 4096], P(('grp', 'kv')), parts along dimension 0, may hold values from -6 to 6
- input_norm_scale: float32 [4096], replicated, may hold values from 0.1 to 1.9
- head_input_matrix: bfloat16 [4096, 8192], P('kv', 'tp'), may hold values from -0.09375 to 0.09375
- output_gate_matrix: bfloat16 [4096, 8192], P('kv', 'tp'), may hold values from -0.09375 to 0.09375
- group_input_matrix: bfloat16 [4096, 512], P('kv', 'tp'), may hold values from -0.09375 to 0.09375
- group_readout_matrix: bfloat16 [4096, 512], P('kv', 'tp'), may hold values from -0.09375 to 0.09375
- step_size_matrix: bfloat16 [4096, 128], P(None, 'tp'), may hold values from -0.09375 to 0.09375
- step_size_bias: float32 [128], P('tp'), may hold values from -4 to -1
- log_decay_rate: float32 [128], P('tp'), may hold values from -4.6 to 2
- direct_path_weight: float32 [128], P('tp'), may hold values from 0.1 to 1.9
- convolution_tap_weight: bfloat16 [4, 8, 1152], P(None, 'tp'), may hold values from -3 to 3
- convolution_history_rows: bfloat16 [8, 6, 8, 1152], P(('grp', 'kv'), None, 'tp'), parts along dimension 0, may hold values from -6 to 6
- per_proposal_states: float32 [8, 3, 128, 64, 64], P(('grp', 'kv'), None, 'tp'), parts along dimension 0, may hold values from -4 to 4
- accepted: int32 [8], P(('grp', 'kv')), parts along dimension 0, may hold values from 1 to 3
- proposal_extra_decay: float32 [8, 3, 128], P(('grp', 'kv'), None, 'tp'), parts along dimension 0, may hold values from -0.69 to 0
- group_norm_scale: float32 [8192], P('tp'), may hold values from 0.1 to 1.9
- output_projection_matrix: bfloat16 [8192, 4096], P('tp', 'kv'), may hold values from -0.0625 to 0.0625
Outputs:
- mixed: bfloat16 [8, 3, 4096], P(('grp', 'tp'), None, 'kv'), parts along dimension 0
- new_states: float32 [8, 3, 128, 64, 64], P(('grp', 'kv'), None, 'tp'), parts along dimension 0
- new_tail: bfloat16 [8, 6, 8, 1152], P(('grp', 'kv'), None, 'tp'), parts along dimension 0
There are 2 independent parts, one for each index of `grp`. A program takes and returns all parts, laid end to end along the dimension named above; an argument that names none is the same for every part. Nothing has to cross between parts.
All inputs are finite; a program needn't handle non-finite values.
Results may differ from a plain program's by a relative error of at most 0.015.
Values may be sent and summed in bfloat16 or wider, within the bound.
No kernel may reach another device: no remote copies, remote signals or barrier semaphores. Data moves between devices by JAX's collectives and lax.ppermute only.
A program may use at most 64 MiB of HBM per device.

v0:
```python
import jax
import jax.numpy as jnp
from jax import lax
from jax.sharding import PartitionSpec as P

epsilon = 1e-06


def rms_scale(values):
    return lax.rsqrt(jnp.mean(values * values, axis=-1, keepdims=True) + epsilon)


def causal_states(log_decay_factor, head_step_size, ssm_inputs, inject, start_state):
    cumulative = jnp.cumsum(log_decay_factor, axis=1)
    length = log_decay_factor.shape[1]
    lower = (jnp.arange(length)[:, None] >= jnp.arange(length)[None, :])[None, :, :, None]
    spread = cumulative[:, :, None, :] - cumulative[:, None, :, :]
    factors = jnp.where(lower, jnp.exp(jnp.where(lower, spread, 0.0)), 0.0)
    mixing = factors * head_step_size[:, None, :, :]
    carried = jnp.exp(cumulative)[..., None, None] * start_state[:, None]
    return carried + jnp.einsum("sjih,sihp,sihn->sjhpn", mixing, ssm_inputs, inject)


def combine_head_outputs(
    incoming_token_rows,
    gate_portion,
    unactivated_step,
    step_size_bias,
    log_decay_rate,
    direct_path_weight,
    convolution_tap_weight,
    convolution_history_rows,
    per_proposal_states,
    accepted,
    proposal_extra_decay,
    group_norm_scale,
):
    sequences, proposals, group_count, group_width = incoming_token_rows.shape
    head_count = step_size_bias.shape[0]
    head_dim = per_proposal_states.shape[3]
    state_size = per_proposal_states.shape[4]
    per_group = head_count // group_count
    group_inner = per_group * head_dim
    tap_count = convolution_tap_weight.shape[0]
    offsets = accepted[:, None] + jnp.arange(tap_count - 1, dtype=jnp.int32)[None, :]
    context = jnp.take_along_axis(convolution_history_rows, offsets[:, :, None, None], axis=1)
    convolution_span = jnp.concatenate([context, incoming_token_rows], axis=1)
    widened = convolution_span.astype(jnp.float32)
    convolved = jnp.zeros((sequences, proposals, group_count, group_width), jnp.float32)
    for conv_tap in range(tap_count):
        convolved = convolved + widened[
            :, conv_tap : conv_tap + proposals
        ] * convolution_tap_weight[conv_tap].astype(jnp.float32)
    activated = jax.nn.silu(convolved)
    ssm_inputs = activated[..., :group_inner].reshape(sequences, proposals, head_count, head_dim)
    inject = jnp.repeat(activated[..., group_inner : group_inner + state_size], per_group, axis=2)
    readout = jnp.repeat(activated[..., group_inner + state_size :], per_group, axis=2)
    head_step_size = jax.nn.softplus(unactivated_step + step_size_bias)
    log_decay_factor = proposal_extra_decay - jnp.exp(log_decay_rate) * head_step_size
    chosen = (accepted - 1)[:, None, None, None, None]
    start_state = jnp.take_along_axis(per_proposal_states, chosen, axis=1)[:, 0]
    running_state_rows = causal_states(
        log_decay_factor, head_step_size, ssm_inputs, inject, start_state
    )
    response = (
        jnp.einsum("sjhn,sjhpn->sjhp", readout, running_state_rows)
        + direct_path_weight[:, None] * ssm_inputs
    )
    gate_raw = gate_portion.astype(jnp.float32).reshape(sequences, proposals, head_count, head_dim)
    gate_applied_output = (response * jax.nn.silu(gate_raw)).reshape(
        sequences, proposals, group_count, group_inner
    )
    scaled = (
        gate_applied_output
        * rms_scale(gate_applied_output)
        * group_norm_scale.reshape(group_count, group_inner)
    )
    flat_gated = scaled.astype(jnp.bfloat16).reshape(sequences, proposals, head_count * head_dim)
    return (flat_gated, running_state_rows, convolution_span)


def local(
    tokens,
    input_norm_scale,
    head_input_matrix,
    output_gate_matrix,
    group_input_matrix,
    group_readout_matrix,
    step_size_matrix,
    step_size_bias,
    log_decay_rate,
    direct_path_weight,
    convolution_tap_weight,
    convolution_history_rows,
    per_proposal_states,
    accepted,
    proposal_extra_decay,
    group_norm_scale,
    output_projection_matrix,
):
    local_seqs, proposals, width = tokens.shape
    head_local = step_size_bias.shape[0]
    group_local = convolution_tap_weight.shape[1]
    head_dim = per_proposal_states.shape[3]
    state_size = per_proposal_states.shape[4]
    group_inner = head_local // group_local * head_dim
    widened = tokens.astype(jnp.float32)
    normed = (widened * rms_scale(widened) * input_norm_scale).astype(jnp.bfloat16)
    unactivated_step = jnp.einsum(
        "sjd,dh->sjh", normed, step_size_matrix, preferred_element_type=jnp.float32
    )
    pieces = lax.all_to_all(normed, "kv", split_axis=2, concat_axis=0, tiled=True)
    joined = jnp.concatenate(
        [head_input_matrix, group_input_matrix, group_readout_matrix, output_gate_matrix], axis=1
    )
    summed = lax.psum_scatter(
        jnp.einsum("sjd,dc->sjc", pieces, joined, preferred_element_type=jnp.float32),
        "kv",
        scatter_dimension=0,
        tiled=True,
    )
    projected = summed.astype(jnp.bfloat16)
    input_width = head_local * head_dim
    inject_width = group_local * state_size
    part_input = projected[..., :input_width].reshape(
        local_seqs, proposals, group_local, group_inner
    )
    part_inject = projected[..., input_width : input_width + inject_width].reshape(
        local_seqs, proposals, group_local, state_size
    )
    part_readout = projected[
        ..., input_width + inject_width : input_width + 2 * inject_width
    ].reshape(local_seqs, proposals, group_local, state_size)
    gate_portion = projected[..., input_width + 2 * inject_width :]
    incoming_token_rows = jnp.concatenate([part_input, part_inject, part_readout], axis=-1)
    gate_applied_output, running_state_rows, convolution_span = combine_head_outputs(
        incoming_token_rows,
        gate_portion,
        unactivated_step,
        step_size_bias,
        log_decay_rate,
        direct_path_weight,
        convolution_tap_weight,
        convolution_history_rows,
        per_proposal_states,
        accepted,
        proposal_extra_decay,
        group_norm_scale,
    )
    terms = jnp.einsum(
        "sjc,cd->sjd",
        lax.all_gather(gate_applied_output, "kv", axis=0, tiled=True),
        output_projection_matrix,
        preferred_element_type=jnp.float32,
    )
    mixed = lax.psum_scatter(terms.astype(jnp.bfloat16), "tp", scatter_dimension=0, tiled=True)
    return (mixed, running_state_rows, convolution_span)


def solution(mesh):
    return jax.shard_map(
        local,
        mesh=mesh,
        in_specs=(
            P(("grp", "kv"), None, None),
            P(),
            P("kv", "tp"),
            P("kv", "tp"),
            P("kv", "tp"),
            P("kv", "tp"),
            P(None, "tp"),
            P("tp"),
            P("tp"),
            P("tp"),
            P(None, "tp", None),
            P(("grp", "kv"), None, "tp", None),
            P(("grp", "kv"), None, "tp", None, None),
            P(("grp", "kv")),
            P(("grp", "kv"), None, "tp"),
            P("tp"),
            P("tp", "kv"),
        ),
        out_specs=(
            P(("grp", "tp"), None, "kv"),
            P(("grp", "kv"), None, "tp", None, None),
            P(("grp", "kv"), None, "tp", None),
        ),
        check_vma=False,
    )
```

profile of v0, /device:TPU:0, one launch (start us, length us, event | category | flops | bytes accessed | tf_op | source)
XLA Modules:
  0.0 112.8 jit_solution(2285924247131712935)
XLA Ops:
  0.6 0.0 copy-start
  0.6 0.0 copy-start.7
  0.7 0.0 copy-start.5
  0.7 0.9 fusion.12
  1.6 0.9 fusion.14
  2.5 2.8 %copy.69 = bf16[1,3,4096]{1,0,2:T(2,128)(2,1)S(1)} copy(bf16[1,3,4096]{2,1,0:T(4,128)(2,1)S(1)} %fusion.14) | data formatting | bytes 49152 | tf_op jit(solution)/shard_map/convert_element_type | solution.py:108
  5.3 0.5 broadcast.303
  5.8 22.4 %reduce.15 = bf16[4096,3]{1,0:T(8,128)(2,1)S(1)} reduce(bf16[4096,1,3]{2,1,0:T(2,128)(2,1)S(1)} %bitcast.84, bf16[]{:T(256)} %broadcast.303), dimensions={1}, to_apply=%bitcast.74.reduce_sub_computation | reduce | bytes 49154
  28.3 2.1 %reshape.441 = bf16[4,2,1536]{2,1,0:T(2,128)(2,1)} reshape(bf16[4096,3]{1,0:T(8,128)(2,1)S(1)} %reduce.15) | data formatting | bytes 49152
  30.4 6.3 %all-to-all-start = ((bf16[4,2,1536]{2,1,0:T(2,128)(2,1)}), bf16[4,2,1536]{2,1,0:T(2,128)(2,1)S(1)}, u32[]{:S(2)}, u32[]{:S(2)}) async-start(bf16[4,2,1536]{2,1,0:T(2,128)(2,1)} %reshape.441), calls=%async_computation | async-start | bytes 49152 | tf_op jit(solution)/shard_map/all_to_all | solution.py:112
  37.4 0.0 copy-done.7
  37.4 0.6 gather_fusion
  38.0 0.1 broadcast_select_fusion
  38.1 0.1 fusion.22
  38.2 0.0 copy-done.5
  38.2 0.6 bitcast_convert_fusion.3
  38.8 0.7 exp.33
  39.5 0.0 copy-done
  39.5 0.8 compare_select_fusion
  40.3 0.1 copy.76
  40.4 0.7 fusion.23
  41.1 0.1 copy.74
  41.2 0.1 multiply_bitcast_fusion
  41.4 1.3 %fusion.8 = f32[32,64,64]{2,1,0:T(8,128)S(1)} fusion(f32[1,3,32,64,64]{4,3,2,1,0:T(8,128)} %param.29, s32[]{:T(128)} %bitcast.20, pred[]{:T(512)} %bitcast.19), kind=kLoop, calls=%fused_computation.11 | loop fusion | flops 131072 | bytes 1048581 | tf_op jit(solution)/shard_map/jit(take_along_axis)/select_n | solution.py:61
  42.7 0.1 copy.72
  42.8 1.2 %dynamic-slice.4 = u32[1]{0:T(128)} dynamic-slice(u32[32]{0:T(128)} %constant.86, u32[]{:T(128)S(6)} %add.157), dynamic_slice_sizes={1} | dynamic-slice | bytes 12
  44.0 1.3 %dynamic-slice.6 = u32[1]{0:T(128)} dynamic-slice(u32[32]{0:T(128)} %constant.90, u32[]{:T(128)S(6)} %add.157), dynamic_slice_sizes={1} | dynamic-slice | bytes 12
  45.3 0.0 all-to-all-done
  45.3 2.1 %reshape.442 = bf16[4096,1,3]{2,1,0:T(2,128)(2,1)S(1)} reshape(bf16[4,2,1536]{2,1,0:T(2,128)(2,1)S(1)} %all-to-all-done) | data formatting | bytes 49152
  47.4 2.0 %copy.70 = bf16[1,3,4096]{2,1,0:T(4,128)(2,1)S(1)} copy(bf16[1,3,4096]{1,0,2:T(2,128)(2,1)S(1)} %bitcast.85) | data formatting | bytes 49152 | tf_op jit(solution)/shard_map/all_to_all | solution.py:112
  49.5 0.0 copy-start.1
  49.5 0.0 copy-start.2
  49.5 0.0 copy-start.3
  49.5 0.0 copy-start.4
  49.5 5.0 %fusion = f32[4,3,4352]{2,0,1:T(4,128)S(1)} fusion(bf16[1024,2048]{1,0:T(8,128)(2,1)} %param.20, bf16[1024,128]{1,0:T(8,128)(2,1)} %param.22, bf16[1024,128]{1,0:T(8,128)(2,1)} %param.21, bf16[1024,2048]{1,0:T(8,128)(2,1)} %param.19, bf16[1,3,4,1024]{3,2,1,0:T(4,128)(2,1)S(1)} %all_to_all.14), kind=kOutput, calls=%fused_computation.2 | convolution fusion | flops 142606336 | bytes 9146368 | tf_op jit(solution)/shard_map/sjd,dc->sjc/dot_general | solution.py:117
  54.5 23.6 %all-reduce.3 = bf16[4,3,4352]{2,0,1:T(4,128)(2,1)S(1)} all-reduce(f32[4,3,4352]{2,0,1:T(4,128)S(1)} %fusion), channel_id=2, replica_groups=mesh['grp'=2,'kv'=4,'tp'=4] {'kv'}, use_global_device_ids=true, to_apply=%region_1.0.clone | all-reduce | flops 52224 | bytes 313344
  78.1 0.7 dynamic-slice_convert_fusion
  78.8 0.1 fusion.20
  78.9 0.1 slice_reduce_fusion
  79.0 0.1 reshape.366
  79.1 0.1 reshape.367
  79.2 0.1 concatenate.23
  79.3 0.7 pad_maximum_fusion
  80.0 0.0 copy-done.1
  80.0 0.0 copy-done.2
  80.0 0.0 copy-done.4
  80.0 0.1 divide_multiply_fusion
  80.0 0.1 slice_bitcast_fusion.1
  80.1 0.1 reshape.406
  80.2 0.1 reshape.370
  80.4 1.4 %bitcast_add_fusion = f32[1,3,32,64,64]{4,3,1,2,0:T(8,128)S(1)} fusion(bf16[3,32,64,1]{2,0,3,1:T(4,128)(2,1)S(1)} %bitcast.88, f32[32,64,64]{2,1,0:T(8,128)S(1)} %fusion.8, f32[3,32]{0,1:T(8,128)S(1)} %copy.72, f32[3,32,3]{0,2,1:T(4,128)S(1)} %multiply_bitcast_fusion, f32[3,32,64]{2,0,1:T(4,128)S(1)} %copy.73), kind=kOutput, calls=%fused_computation.5 | convolution fusion | flops 3164160 | bytes 2135552 | tf_op jit(solution)/shard_map/sjih,sihp,sihn->sjhpn/dot_general | solution.py:21
  81.8 0.0 copy-start.8
  81.8 0.0 copy-start.6
  81.8 1.9 %copy.80 = f32[1,3,32,64,64]{4,3,2,1,0:T(8,128)} copy(f32[1,3,32,64,64]{4,3,1,2,0:T(8,128)S(1)} %bitcast_add_fusion) | data formatting | bytes 3145728
  83.7 0.9 fusion.3
  84.6 0.2 multiply_reduce_fusion
  84.8 0.1 reshape.374
  84.9 0.1 reduce_sum.27
  85.0 0.1 reduce_sum.28
  85.1 0.1 mul.189
  85.2 13.1 %all_gather.3 = bf16[4,3,2048]{2,1,0:T(4,128)(2,1)S(1)} all-gather(bf16[1,3,2048]{2,1,0:T(4,128)(2,1)S(1)} %multiply_convert_fusion), channel_id=1, replica_groups=mesh['grp'=2,'kv'=4,'tp'=4] {'kv'}, dimensions={0}, use_global_device_ids=true | all-gather | bytes 61440 | tf_op jit(solution)/shard_map/all_gather | solution.py:152
  98.4 2.8 %fusion.5 = bf16[4,3,1024]{2,0,1:T(4,128)(2,1)S(1)} fusion(bf16[2048,1024]{1,0:T(8,128)(2,1)} %param.33, bf16[4,3,2048]{2,1,0:T(4,128)(2,1)S(1)} %all_gather.3), kind=kOutput, calls=%fused_computation.8 | convolution fusion | flops 50343936 | bytes 4268032 | tf_op jit(solution)/shard_map/sjc,cd->sjd/dot_general | solution.py:150
  101.2 10.3 %all-reduce.1 = bf16[4,3,1024]{2,1,0:T(4,128)(2,1)S(1)} all-reduce(bf16[4,3,1024]{2,1,0:T(4,128)(2,1)S(1)} %copy.79), channel_id=3, replica_groups=mesh['grp'=2,'kv'=4,'tp'=4] {'tp'}, use_global_device_ids=true, to_apply=%region_5.6.clone | all-reduce | flops 12288 | bytes 49152
  111.5 1.2 %constant_dynamic-slice_fusion = bf16[1,3,1024]{2,1,0:T(4,128)(2,1)} fusion(bf16[4,3,1024]{2,1,0:T(4,128)(2,1)S(1)} %all-reduce.1, u32[]{:T(128)} %bitcast.45), kind=kLoop, calls=%fused_computation.61 | loop fusion | bytes 12292
  (23 shorter events, 0.3 us)
Async XLA Ops:
  0.6 38.8 %copy-start = (bf16[4096,32]{0,1:T(8,128)(2,1)S(1)}, bf16[4096,32]{0,1:T(8,128)(2,1)}, u32[]{:S(2)}) copy-start(bf16[4096,32]{0,1:T(8,128)(2,1)} %param.23) | copy-start | bytes 786436
  0.6 36.8 %copy-start.7 = (bf16[1,6,2,1152]{3,2,1,0:T(2,128)(2,1)S(1)}, bf16[1,6,2,1152]{3,2,1,0:T(2,128)(2,1)}, u32[]{:S(2)}) copy-start(bf16[1,6,2,1152]{3,2,1,0:T(2,128)(2,1)} %param.28) | copy-start | bytes 82948
  0.7 37.5 %copy-start.5 = (bf16[4,2,1152]{2,1,0:T(2,128)(2,1)S(1)}, bf16[4,2,1152]{2,1,0:T(2,128)(2,1)}, u32[]{:S(2)}) copy-start(bf16[4,2,1152]{2,1,0:T(2,128)(2,1)} %param.27) | copy-start | bytes 55300
  30.4 15.0 %all-to-all-start = ((bf16[4,2,1536]{2,1,0:T(2,128)(2,1)}), bf16[4,2,1536]{2,1,0:T(2,128)(2,1)S(1)}, u32[]{:S(2)}, u32[]{:S(2)}) async-start(bf16[4,2,1536]{2,1,0:T(2,128)(2,1)} %reshape.441), calls=%async_computation | async-start | bytes 49152 | tf_op jit(solution)/shard_map/all_to_all | solution.py:112
  49.5 30.5 %copy-start.1 = (f32[2,1152]{1,0:T(2,128)S(1)}, f32[2,1152]{1,0:T(2,128)}, u32[]{:S(2)}) copy-start(f32[2,1152]{1,0:T(2,128)} %get-tuple-element.33) | copy-start | bytes 27652
  49.5 30.5 %copy-start.2 = (f32[2,1152]{1,0:T(2,128)S(1)}, f32[2,1152]{1,0:T(2,128)}, u32[]{:S(2)}) copy-start(f32[2,1152]{1,0:T(2,128)} %get-tuple-element.34) | copy-start | bytes 27652
  49.5 30.5 %copy-start.3 = (f32[2,1152]{1,0:T(2,128)S(1)}, f32[2,1152]{1,0:T(2,128)}, u32[]{:S(2)}) copy-start(f32[2,1152]{1,0:T(2,128)} %get-tuple-element.35) | copy-start | bytes 27652
  49.5 30.5 %copy-start.4 = (f32[2,1152]{1,0:T(2,128)S(1)}, f32[2,1152]{1,0:T(2,128)}, u32[]{:S(2)}) copy-start(f32[2,1152]{1,0:T(2,128)} %get-tuple-element.36) | copy-start | bytes 27652
  81.8 2.8 %copy-start.8 = (f32[32]{0:T(128)S(1)}, f32[32]{0:T(128)}, u32[]{:S(2)}) copy-start(f32[32]{0:T(128)} %param.26) | copy-start | bytes 388
  81.8 3.4 %copy-start.6 = (f32[2048]{0:T(1024)S(1)}, f32[2048]{0:T(1024)}, u32[]{:S(2)}) copy-start(f32[2048]{0:T(1024)} %param.32) | copy-start | bytes 24580
where the time goes:
time: 113 us
  blocking collectives  47 us (42%)
  other arithmetic  28.3 us (25%)
  local copies, waits for them, and re-layouts  18.6 us (16%)
  matrix products  11 us (10%)
  starting transfers between devices  6.35 us (6%)
  between operations  1.59 us (1%)
    unnamed x2, blocking collectives  33.9 us
    unnamed x1, other arithmetic  22.4 us
    all_gather x1, blocking collectives, local(): lax.all_gather(gate_applied_output, 'kv', axis=0, tiled=True)  13.1 us
    unnamed x25, local copies, waits for them, and re-layouts  10.4 us
    all_to_all x1, starting transfers between devices, local(): lax.all_to_all(normed, 'kv', split_axis=2, concat_axis=0, tiled=True)  6.35 us
    dot_general x1, matrix products, local(): jnp.einsum('sjd,dc->sjc', pieces, joined, preferred_element_type=jnp.floa...  4.97 us
    dot_general x1, matrix products, local(): jnp.einsum('sjc,cd->sjd', lax.all_gather(gate_applied_output, 'kv', axis=...  2.85 us
    convert_element_type x1, local copies, waits for them, and re-layouts, local(): (widened * rms_scale(widened) * input_norm_scale).astype(jnp.bfloat16)  2.84 us
  transfers between devices with their start and end apart: 1, of which 0 were waited for; matrix products, arithmetic and copies ran while one was open for 7% of the time, Pallas kernels for 0%

commit v1 on v0

--- a/solution.py
+++ b/solution.py
@@ -1,9 +1,462 @@
+import functools
+
 import jax
 import jax.numpy as jnp
 from jax import lax
+from jax.experimental import pallas as pl
+from jax.experimental.pallas import tpu as pltpu
 from jax.sharding import PartitionSpec as P
 
 epsilon = 1e-06
+F32 = jnp.float32
+BF16 = jnp.bfloat16
+ROWS = 8
+
+
+def vmem(x):
+    return pltpu.with_memory_space_constraint(x, pltpu.VMEM)
+
+
+VMEM_SPEC = pl.BlockSpec(memory_space=pltpu.VMEM)
+SMEM_SPEC = pl.BlockSpec(memory_space=pltpu.SMEM)
+HBM_SPEC = pl.BlockSpec(memory_space=pl.ANY)
+
+
+def call(body, outs, ins, specs, name, flops=0, scratch=(), out_specs=None, limit=20 << 20):
+    return pl.pallas_call(
+        body,
+        out_shape=outs,
+        in_specs=specs,
+        out_specs=out_specs or [VMEM_SPEC] * len(outs),
+        scratch_shapes=list(scratch),
+        cost_estimate=pl.CostEstimate(flops=flops, transcendentals=0, bytes_accessed=0),
+        compiler_params=pltpu.CompilerParams(vmem_limit_bytes=limit),
+        name=name,
+    )(*ins)
+
+
+def exchange(blocks, axis, count):
+    got = []
+    for step in range(1, count):
+        pairs = [(i, i ^ step) for i in range(count)]
+        got.append(lax.ppermute(blocks[step], axis, pairs))
+    return got
+
+
+def silu(v):
+    return v * jax.nn.sigmoid(v)
+
+
+def split(v):
+    high = v.astype(BF16)
+    return high, (v - high.astype(F32)).astype(BF16)
+
+
+def norm_body(count, tokens, scale, normed, *slices):
+    me = lax.axis_index("kv")
+    width = slices[0].shape[1]
+    values = tokens[0].astype(F32)
+    mean = jnp.mean(values * values, axis=-1, keepdims=True)
+    normed[...] = (values * lax.rsqrt(mean + epsilon) * scale[...]).astype(BF16)
+    for step in range(count):
+        start = pl.multiple_of(lax.bitwise_xor(me, step) * width, 128)
+        slices[step][...] = normed[:, pl.ds(start, width)]
+
+
+def step_body(head_dim, normed, step_t, bias, rate, direct, extra, coef, small, table):
+    props, heads = extra.shape
+    raw = lax.dot_general(
+        normed[...], step_t[...], (((1,), (1,)), ((), ())), preferred_element_type=F32
+    )
+    size = jax.nn.softplus(raw + bias[...])
+    decay = extra[...] - jnp.exp(rate[...]) * size
+    table[...] = jnp.zeros_like(table)
+    small[...] = jnp.zeros_like(small)
+    small[0:props, :] = jnp.exp(decay)
+    total = []
+    for j in range(props):
+        row = decay[j : j + 1]
+        total.append(row if j == 0 else total[-1] + row)
+        table[j : j + 1, :] = jnp.exp(total[j])
+    for i in range(props):
+        own = size[i : i + 1]
+        for j in range(i, props):
+            at = (1 + i) * ROWS + j
+            table[at : at + 1, :] = jnp.exp(total[j] - total[i]) * own
+    at = (1 + props) * ROWS
+    table[at : at + 1, :] = direct[...]
+    width = coef.shape[-1]
+    lane = lax.broadcasted_iota(jnp.int32, (heads, width), 1)
+    head = lax.broadcasted_iota(jnp.int32, (heads, width), 0)
+    spread = jnp.where(lane // head_dim == head, 1.0, 0.0).astype(F32)
+    wide = jnp.dot(
+        table[...], spread, preferred_element_type=F32, precision=lax.Precision.HIGHEST
+    )
+    for part in range(coef.shape[0]):
+        coef[part] = wide[part * ROWS : (part + 1) * ROWS]
+
+
+def state_body(accepted, states, history, taps, start, high, low, early, taps_wide, sem):
+    count = accepted[0]
+    copy = pltpu.make_async_copy(states.at[0, count - 1], start, sem)
+    copy.start()
+    heads, head_dim, size = start.shape
+    groups = taps.shape[1]
+    tap_count = taps.shape[0]
+    inner = heads // groups * head_dim
+    per = heads // groups
+
+    def widen(rows, target, at):
+        rows = rows.astype(F32)
+        for g in range(groups):
+            row = rows[g : g + 1]
+            target[at : at + 1, g * inner : (g + 1) * inner] = row[:, :inner]
+            for part in range(2):
+                base = groups * inner + part * groups * size + g * size
+                target[at : at + 1, base : base + size] = row[
+                    :, inner + part * size : inner + (part + 1) * size
+                ]
+
+    taps_wide[...] = jnp.zeros_like(taps_wide)
+    early[...] = jnp.zeros_like(early)
+    for k in range(tap_count):
+        widen(taps[k], taps_wide, k)
+    for k in range(tap_count - 1):
+        widen(history[0, count + k], early, k)
+    context = early[...]
+    before = tap_count - 1
+    total = context * taps_wide[0:1, :]
+    keep = lax.broadcasted_iota(jnp.int32, (ROWS, 1), 0) < before
+    for k in range(1, before):
+        total = total + jnp.where(keep, pltpu.roll(context, ROWS - k, 0), 0.0) * taps_wide[k : k + 1, :]
+    early[...] = jnp.where(keep, total, 0.0)
+
+    high[...] = jnp.zeros_like(high)
+    low[...] = jnp.zeros_like(low)
+    copy.wait()
+    pair = 128 // head_dim
+    for g in range(groups):
+        for block in range(per // pair):
+            at = g * per + block * pair
+            tile = start[at : at + pair].reshape(pair * head_dim, size).T
+            big, rest = split(tile)
+            cols = slice(at * head_dim, (at + pair) * head_dim)
+            high[g * size : (g + 1) * size, cols] = big
+            low[g * size : (g + 1) * size, cols] = rest
+
+
+def stack_rows(parts, lhs):
+    lhs[...] = jnp.zeros_like(lhs)
+    for j, part in enumerate(parts):
+        lhs[4 * j : 4 * j + part.shape[0], :] = part[...].astype(F32)
+    return lhs[...].astype(BF16)
+
+
+def project_body(count, *refs):
+    slices = refs[:count]
+    weights = refs[count : count + 4]
+    own = refs[count + 4]
+    outs = refs[count + 5 : count + 4 + count]
+    lhs = stack_rows(slices, refs[-1])
+    at = 0
+    for weight in weights:
+        width = weight.shape[1]
+        result = jnp.dot(lhs, weight[...], preferred_element_type=F32)
+        own[:, at : at + width] = result[0:4]
+        for j, out in enumerate(outs, 1):
+            out[:, at : at + width] = result[4 * j : 4 * j + 4].astype(BF16)
+        at += width
+
+
+def mixer_body(props, groups, *refs):
+    own, *rest = refs
+    count = len(rest) - 11
+    others = rest[:count]
+    coef, early, taps, high, low, gain, gated, fresh, act, summed, norms = rest[count:]
+    inner = gain.shape[1]
+    conv = early.shape[1]
+    per = inner // groups
+    both = (conv - inner) // 2
+    size = both // groups
+    summed[...] = jnp.zeros_like(summed)
+    total = own[...]
+    for other in others:
+        total = total + other[...].astype(F32)
+    summed[0:props, :] = total[0:props].astype(BF16).astype(F32)
+    rows = summed[:, :conv]
+    fresh[...] = rows
+    tap_count = 4
+    value = early[...] + rows * taps[tap_count - 1 : tap_count, :]
+    for k in range(1, props):
+        value = value + pltpu.roll(rows * taps[tap_count - 1 - k : tap_count - k, :], k, 0)
+    value = silu(value)
+    act[...] = value
+    x = value[:, :inner]
+    b = value[:, inner : inner + both]
+    c = value[:, inner + both :]
+    c_high, c_low = split(c)
+    left = jnp.concatenate([c_high.astype(F32), c_low.astype(F32)], axis=0).astype(BF16)
+    carried = jnp.dot(left, high[...], preferred_element_type=F32)
+    carried = carried[:ROWS] + carried[ROWS:]
+    carried = carried + jnp.dot(c_high, low[...], preferred_element_type=F32)
+    lane = lax.broadcasted_iota(jnp.int32, (ROWS, both), 1)
+    response = coef[0] * carried + coef[1 + props, 0:1, :] * x
+    pieces = []
+    weights = []
+    for i in range(props):
+        product = c * b[i : i + 1]
+        weights.append(
+            [
+                jnp.sum(jnp.where(lane // size == g, product, 0.0), axis=1, keepdims=True)
+                for g in range(groups)
+            ]
+        )
+    gate = summed[:, conv:]
+    gate = silu(gate)
+    for g in range(groups):
+        at = slice(g * per, (g + 1) * per)
+        part = response[:, at]
+        for i in range(props):
+            part = part + coef[1 + i, :, at] * weights[i][g] * x[i : i + 1, at]
+        part = part * gate[:, at]
+        mean = jnp.sum(part * part, axis=1, keepdims=True) * (1.0 / per)
+        pieces.append(part * lax.rsqrt(mean + epsilon) * gain[:, at])
+    norms[...] = jnp.concatenate(pieces, axis=1)
+    gated[...] = norms[0:4].astype(BF16)
+
+
+def tail_body(props, accepted, start, small, act, coef, fresh, history, states, tail, held, sem):
+    heads, head_dim, size = start.shape
+    groups = history.shape[2]
+    per = heads // groups
+    inner = per * head_dim
+    wide = heads * head_dim
+    count = accepted[0]
+    before = tail.shape[1] - props
+    for k in range(before):
+        tail[0, k] = history[0, count + k]
+    for j in range(props):
+        rows = []
+        for g in range(groups):
+            row = [fresh[j : j + 1, g * inner : (g + 1) * inner]]
+            for part in range(2):
+                base = wide + part * groups * size + g * size
+                row.append(fresh[j : j + 1, base : base + size])
+            rows.append(jnp.concatenate(row, axis=1))
+        tail[0, before + j] = jnp.concatenate(rows, axis=0).astype(BF16)
+    x = act[:, :wide]
+    row_at = lax.broadcasted_iota(jnp.int32, (ROWS, 1), 0)
+    steps = jnp.zeros((ROWS, wide), F32)
+    for j in range(props):
+        steps = jnp.where(row_at == j, coef[1 + j], steps)
+    dx = x * steps
+    dx_high, dx_low = split(dx)
+    dx_high, dx_low = dx_high.astype(F32), dx_low.astype(F32)
+    left = jnp.concatenate(
+        [dx_high, dx_low, dx_high, jnp.zeros_like(dx)], axis=0
+    ).astype(BF16)
+    b = act[:, wide : wide + groups * size]
+    b_high, b_low = split(b)
+    b_high, b_low = b_high.astype(F32), b_low.astype(F32)
+    copies = []
+    for g in range(groups):
+        blocks = []
+        for j in range(props):
+            hi = jnp.where(row_at == j, b_high, 0.0)
+            lo = jnp.where(row_at == j, b_low, 0.0)
+            full = jnp.concatenate([hi, hi, lo, jnp.zeros_like(hi)], axis=0)
+            if g:
+                full = pltpu.roll(full, groups * size - g * size, 1)
+            blocks.append(full)
+        right = jnp.concatenate(blocks, axis=1).astype(BF16)
+        update = lax.dot_general(
+            left[:, g * inner : (g + 1) * inner],
+            right,
+            (((0,), (0,)), ((), ())),
+            preferred_element_type=F32,
+        )
+        lanes = groups * size
+        for h in range(per):
+            at = g * per + h
+            state = start[at]
+            for j in range(props):
+                new = update[h * head_dim : (h + 1) * head_dim, j * lanes : j * lanes + size]
+                state = state * small[j : j + 1, at : at + 1] + new
+                held[j, at] = state
+        copy = pltpu.make_async_copy(
+            held.at[:, pl.ds(g * per, per)], states.at[0, :, pl.ds(g * per, per)], sem.at[g]
+        )
+        copy.start()
+        copies.append(copy)
+    for copy in copies:
+        copy.wait()
+
+
+def output_body(count, *refs):
+    parts = refs[:count]
+    weight = refs[count]
+    outs = refs[count + 1 : count + 1 + count]
+    result, lhs = refs[-2:]
+    which = lax.bitwise_xor(lax.axis_index("kv"), lax.axis_index("tp"))
+    product = jnp.dot(stack_rows(parts, lhs), weight[...], preferred_element_type=F32)
+    for j in range(count):
+        result[j, 0:4] = product[4 * j : 4 * j + 4]
+    for step in range(count):
+        outs[step][...] = result[lax.bitwise_xor(which, step), 0:4].astype(BF16)
+
+
+def final_body(*refs):
+    *parts, out = refs
+    total = parts[0][...].astype(F32)
+    for part in parts[1:]:
+        total = total + part[...].astype(F32)
+    out[0] = total[0 : out.shape[1]].astype(BF16)
+
+
+def fast_local(
+    count,
+    tokens,
+    input_norm_scale,
+    head_input_matrix,
+    output_gate_matrix,
+    group_input_matrix,
+    group_readout_matrix,
+    step_size_matrix,
+    step_size_bias,
+    log_decay_rate,
+    direct_path_weight,
+    convolution_tap_weight,
+    convolution_history_rows,
+    per_proposal_states,
+    accepted,
+    proposal_extra_decay,
+    group_norm_scale,
+    output_projection_matrix,
+):
+    _, props, width = tokens.shape
+    heads = step_size_bias.shape[0]
+    _, tail_rows, groups, channels = convolution_history_rows.shape
+    head_dim, size = per_proposal_states.shape[3:]
+    inner = heads * head_dim
+    conv = groups * channels
+    rows = head_input_matrix.shape[0]
+    total = conv + inner
+    out_cols = output_projection_matrix.shape[1]
+
+    normed, *slices = call(
+        functools.partial(norm_body, count),
+        [pltpu.VMEM((props, width), BF16)] + [pltpu.VMEM((props, rows), BF16)] * count,
+        [tokens, input_norm_scale.reshape(1, width)],
+        [VMEM_SPEC] * 2,
+        "norm",
+    )
+    received = exchange(slices, "kv", count)
+
+    coef, small = call(
+        functools.partial(step_body, head_dim),
+        [pltpu.VMEM((props + 2, ROWS, inner), F32), pltpu.VMEM((ROWS, heads), F32)],
+        [
+            vmem(normed),
+            vmem(step_size_matrix.T),
+            step_size_bias.reshape(1, heads),
+            log_decay_rate.reshape(1, heads),
+            direct_path_weight.reshape(1, heads),
+            proposal_extra_decay.reshape(props, heads),
+        ],
+        [VMEM_SPEC] * 6,
+        "steps",
+        flops=20_000_000,
+        scratch=[pltpu.VMEM(((props + 2) * ROWS, heads), F32)],
+    )
+    start, high, low, early, taps = call(
+        state_body,
+        [
+            pltpu.VMEM((heads, head_dim, size), F32),
+            pltpu.VMEM((groups * size, inner), BF16),
+            pltpu.VMEM((groups * size, inner), BF16),
+            pltpu.VMEM((ROWS, conv), F32),
+            pltpu.VMEM((ROWS, conv), F32),
+        ],
+        [accepted, per_proposal_states, convolution_history_rows, convolution_tap_weight],
+        [SMEM_SPEC, HBM_SPEC, VMEM_SPEC, VMEM_SPEC],
+        "start_state",
+        flops=20_000_000,
+        scratch=[pltpu.SemaphoreType.DMA],
+    )
+
+    own, *partials = call(
+        functools.partial(project_body, count),
+        [pltpu.VMEM((4, total), F32)] + [pltpu.VMEM((4, total), BF16)] * (count - 1),
+        [vmem(s) for s in [slices[0]] + received]
+        + [
+            vmem(w)
+            for w in (
+                head_input_matrix,
+                group_input_matrix,
+                group_readout_matrix,
+                output_gate_matrix,
+            )
+        ],
+        [VMEM_SPEC] * (count + 4),
+        "project",
+        flops=200_000_000,
+        scratch=[pltpu.VMEM((4 * count, rows), F32)],
+    )
+    sums = exchange([None] + partials, "kv", count)
+    gated, fresh, act = call(
+        functools.partial(mixer_body, props, groups),
+        [
+            pltpu.VMEM((4, inner), BF16),
+            pltpu.VMEM((ROWS, conv), F32),
+            pltpu.VMEM((ROWS, conv), F32),
+        ],
+        [vmem(v) for v in [own] + sums + [coef, early, taps, high, low]]
+        + [vmem(group_norm_scale.reshape(1, inner))],
+        [VMEM_SPEC] * (count + 6),
+        "mixer",
+        flops=20_000_000,
+        scratch=[pltpu.VMEM((ROWS, total), F32), pltpu.VMEM((ROWS, inner), F32)],
+    )
+    gathered = exchange([gated] * count, "kv", count)
+    new_states, new_tail = call(
+        functools.partial(tail_body, props),
+        [
+            jax.ShapeDtypeStruct((1, props, heads, head_dim, size), F32),
+            jax.ShapeDtypeStruct(convolution_history_rows.shape, BF16),
+        ],
+        [accepted]
+        + [vmem(v) for v in (start, small, act, coef, fresh)]
+        + [convolution_history_rows],
+        [SMEM_SPEC] + [VMEM_SPEC] * 6,
+        "states",
+        flops=60_000_000,
+        out_specs=[HBM_SPEC, VMEM_SPEC],
+        scratch=[
+            pltpu.VMEM((props, heads, head_dim, size), F32),
+            pltpu.SemaphoreType.DMA((groups,)),
+        ],
+    )
+    blocks = call(
+        functools.partial(output_body, count),
+        [pltpu.VMEM((4, out_cols), BF16)] * count,
+        [vmem(v) for v in [gated] + gathered + [output_projection_matrix]],
+        [VMEM_SPEC] * (count + 1),
+        "output",
+        flops=100_000_000,
+        scratch=[
+            pltpu.VMEM((count, ROWS, out_cols), F32),
+            pltpu.VMEM((4 * count, inner), F32),
+        ],
+    )
+    last = exchange(blocks, "tp", count)
+    (mixed,) = call(
+        final_body,
+        [jax.ShapeDtypeStruct((1, props, out_cols), BF16)],
+        [vmem(v) for v in [blocks[0]] + last],
+        [VMEM_SPEC] * count,
+        "final",
+    )
+    return (mixed, new_states, new_tail)
 
 
 def rms_scale(values):
@@ -157,9 +610,18 @@
     return (mixed, running_state_rows, convolution_span)
 
 
+def chosen(mesh, *arguments):
+    tokens, matrix = arguments[0], arguments[2]
+    kv, tp = mesh.shape["kv"], mesh.shape["tp"]
+    slim = tokens.shape[:2] == (1, 3) and matrix.shape[0] % 128 == 0
+    if slim and kv == tp and kv in (2, 4):
+        return fast_local(kv, *arguments)
+    return local(*arguments)
+
+
 def solution(mesh):
     return jax.shard_map(
-        local,
+        functools.partial(chosen, mesh),
         mesh=mesh,
         in_specs=(
             P(("grp", "kv"), None, None),

time: 113 us -> 42.7 us (0.38)
  blocking collectives: 47 us -> 0 us
  other arithmetic: 28.3 us -> 0 us
  matrix products: 11 us -> 0 us
  local copies, waits for them, and re-layouts: 18.6 us -> 7.79 us
  starting transfers between devices: 6.35 us -> 16.5 us
  waiting for transfers between devices: 0.01 us -> 9.38 us
  Pallas kernels: 0 us -> 7.16 us
    unnamed x2 -> x0, blocking collectives: 33.9 us -> none
    unnamed x1 -> x0, other arithmetic: 22.4 us -> none
    ppermute x0 -> x12, starting transfers between devices: none -> 16.5 us  [exchange(): got.append(lax.ppermute(blocks[step], axis, pairs))]
    all_gather x1 -> x0, blocking collectives: 13.1 us -> none  [local(): lax.all_gather(gate_applied_output, 'kv', axis=0, tiled=True)]
    dot_general x5 -> x0, matrix products: 11 us -> none  [the longest x1 4.97 us: local(): jnp.einsum('sjd,dc->sjc', pieces, joined, preferred_element_type=jnp.floa...]
    ppermute x0 -> x12, waiting for transfers between devices: none -> 9.38 us  [exchange(): got.append(lax.ppermute(blocks[step], axis, pairs))]
    pallas_call x0 -> x8, Pallas kernels: none -> 7.16 us  [call(): pl.pallas_call(body, out_shape=outs, in_specs=specs, out_specs=out_specs...]
    all_to_all x1 -> x0, starting transfers between devices: 6.35 us -> none  [local(): lax.all_to_all(normed, 'kv', split_axis=2, concat_axis=0, tiled=True)]
  transfers between devices with their start and end apart: 1 -> 12, of which waited for: 0 -> 5; matrix products, arithmetic and copies ran while one was open for 7% -> 0% of each run, Pallas kernels for 0% -> 10%
where the time goes in v1:
time: 42.7 us; the launch traced here: 42.3 us
  starting transfers between devices  16.5 us (39%)
  waiting for transfers between devices  9.38 us (22%)
  local copies, waits for them, and re-layouts  7.79 us (18%)
  Pallas kernels  7.16 us (17%)
  between operations  1.51 us (4%)
    ppermute x12, starting transfers between devices, exchange(): got.append(lax.ppermute(blocks[step], axis, pairs))  16.5 us
    ppermute x12, waiting for transfers between devices, exchange(): got.append(lax.ppermute(blocks[step], axis, pairs))  9.38 us
    unnamed x33, local copies, waits for them, and re-layouts  7.79 us
    pallas_call x8, Pallas kernels, call(): pl.pallas_call(body, out_shape=outs, in_specs=specs, out_specs=out_specs...  7.16 us
  transfers between devices with their start and end apart: 12, of which 5 were waited for; matrix products, arithmetic and copies ran while one was open for 0% of the time, Pallas kernels for 10%

profile of v1, /device:TPU:0, one launch (start us, length us, event | category | flops | bytes accessed | tf_op | source)
XLA Modules:
  0.0 42.3 jit_solution(16931597036250085279)
XLA Ops:
  0.6 0.0 copy-start.8
  0.6 0.7 %copy-done.8 = bf16[1,3,4096]{2,1,0:T(4,128)(2,1)S(1)} copy-done((bf16[1,3,4096]{2,1,0:T(4,128)(2,1)S(1)}, bf16[1,3,4096]{2,1,0:T(4,128)(2,1)}, u32[]{:S(2)}) %copy-start.8) | copy-done | bytes 24600
  1.4 0.0 copy-start.10
  1.4 0.7 %copy-done.10 = f32[4096]{0:T(1024)S(1)} copy-done((f32[4096]{0:T(1024)S(1)}, f32[4096]{0:T(1024)}, u32[]{:S(2)}) %copy-start.10) | copy-done | bytes 16408
  2.1 0.1 norm.1
  2.2 3.1 %collective-permute-start = (bf16[3,1024]{1,0:T(4,128)(2,1)S(1)}, bf16[3,1024]{1,0:T(4,128)(2,1)S(1)}, u32[]{:S(2)}, u32[]{:S(2)}) collective-permute-start(bf16[3,1024]{1,0:T(4,128)(2,1)S(1)} %get-tuple-element.29), channel_id=1, source_target_pairs={{0,4},{4,0},{8,12},{12,8},{1,5},{5,1},{9,13},{13,9},{2,6},{6,2},{1... | collective-permute-start | bytes 18440 | tf_op jit(solution)/shard_map/ppermute | solution.py:42
  5.4 2.6 %collective-permute-start.1 = (bf16[3,1024]{1,0:T(4,128)(2,1)S(1)}, bf16[3,1024]{1,0:T(4,128)(2,1)S(1)}, u32[]{:S(2)}, u32[]{:S(2)}) collective-permute-start(bf16[3,1024]{1,0:T(4,128)(2,1)S(1)} %get-tuple-element.30), channel_id=1, source_target_pairs={{0,8},{4,12},{8,0},{12,4},{1,9},{5,13},{9,1},{13,5},{2,10},{6,14},... | collective-permute-start | bytes 18440 | tf_op jit(solution)/shard_map/ppermute | solution.py:42
  8.0 0.0 collective-permute-start.2
  8.0 0.0 collective-permute-done.refs_1_
  8.0 2.0 %collective-permute-done.1.refs_2_ = bf16[3,1024]{1,0:T(4,128)(2,1)S(1)} collective-permute-done((bf16[3,1024]{1,0:T(4,128)(2,1)S(1)}, bf16[3,1024]{1,0:T(4,128)(2,1)S(1)}, u32[]{:S(2)}, u32[]{:S(2)}) %collective-permute-start.1) | collective-permute-done | bytes 6176 | tf_op jit(solution)/shard_map/ppermute | solution.py:42
  9.9 3.5 %collective-permute-done.2.refs_3_ = bf16[3,1024]{1,0:T(4,128)(2,1)S(1)} collective-permute-done((bf16[3,1024]{1,0:T(4,128)(2,1)S(1)}, bf16[3,1024]{1,0:T(4,128)(2,1)S(1)}, u32[]{:S(2)}, u32[]{:S(2)}) %collective-permute-start.2) | collective-permute-done | bytes 6176 | tf_op jit(solution)/shard_map/ppermute | solution.py:42
  13.4 0.0 copy-start
  13.4 2.2 %copy-done = bf16[1024,2048]{1,0:T(8,128)(2,1)S(1)} copy-done((bf16[1024,2048]{1,0:T(8,128)(2,1)S(1)}, bf16[1024,2048]{1,0:T(8,128)(2,1)}, u32[]{:S(2)}) %copy-start) | copy-done | bytes 4194328
  15.6 0.0 copy-start.1
  15.6 2.2 %copy-done.1 = bf16[1024,2048]{1,0:T(8,128)(2,1)S(1)} copy-done((bf16[1024,2048]{1,0:T(8,128)(2,1)S(1)}, bf16[1024,2048]{1,0:T(8,128)(2,1)}, u32[]{:S(2)}) %copy-start.1) | copy-done | bytes 4194328
  17.8 0.0 copy-start.4
  17.8 0.9 %copy-done.4 = bf16[1024,128]{1,0:T(8,128)(2,1)S(1)} copy-done((bf16[1024,128]{1,0:T(8,128)(2,1)S(1)}, bf16[1024,128]{1,0:T(8,128)(2,1)}, u32[]{:S(2)}) %copy-start.4) | copy-done | bytes 262168
  18.7 0.0 copy-start.5
  18.7 0.9 %copy-done.5 = bf16[1024,128]{1,0:T(8,128)(2,1)S(1)} copy-done((bf16[1024,128]{1,0:T(8,128)(2,1)S(1)}, bf16[1024,128]{1,0:T(8,128)(2,1)}, u32[]{:S(2)}) %copy-start.5) | copy-done | bytes 262168
  19.7 0.0 copy-start.15
  19.7 0.0 copy-start.3
  19.7 0.0 copy-start.7
  19.7 0.0 copy-start.9
  19.7 0.0 copy-start.6
  19.7 0.0 copy-start.12
  19.7 0.0 copy-start.13
  19.7 0.0 copy-start.14
  19.7 0.0 copy-start.11
  19.8 1.3 %project.1 = (f32[4,4352]{1,0:T(4,128)S(1)}, bf16[4,4352]{1,0:T(4,128)(2,1)S(1)}, bf16[4,4352]{1,0:T(4,128)(2,1)S(1)}, bf16[4,4352]{1,0:T(4,128)(2,1)S(1)}) custom-call(bf16[3,1024]{1,0:T(4,128)(2,1)S(1)} %get-tuple-element.28.refs_0_, bf16[3,1024]{1,0:T(4,128)(2,1)S(1)} %collective-permute-done.refs_1_, bf16[3,1024]{1,0:T(4,128)(2,1)S(1)} %collective-permute-done.1.refs_2_, ...), custom_call_target="tpu_custom_call" | custom-call | flops 200000000 | tf_op jit(solution)/shard_map/project/pallas_call | solution.py:26
  21.0 0.0 copy-start.2
  21.0 0.0 collective-permute-start.3
  21.0 0.6 %collective-permute-start.4 = (bf16[4,4352]{1,0:T(4,128)(2,1)S(1)}, bf16[4,4352]{1,0:T(4,128)(2,1)S(1)}, u32[]{:S(2)}, u32[]{:S(2)}) collective-permute-start(bf16[4,4352]{1,0:T(4,128)(2,1)S(1)} %get-tuple-element.34), channel_id=1, source_target_pairs={{0,8},{4,12},{8,0},{12,4},{1,9},{5,13},{9,1},{13,5},{2,10},{6,14},... | collective-permute-start | bytes 104456 | tf_op jit(solution)/shard_map/ppermute | solution.py:42
  21.7 3.7 %collective-permute-start.5 = (bf16[4,4352]{1,0:T(4,128)(2,1)S(1)}, bf16[4,4352]{1,0:T(4,128)(2,1)S(1)}, u32[]{:S(2)}, u32[]{:S(2)}) collective-permute-start(bf16[4,4352]{1,0:T(4,128)(2,1)S(1)} %get-tuple-element.35), channel_id=1, source_target_pairs={{0,12},{4,8},{8,4},{12,0},{1,13},{5,9},{9,5},{13,1},{2,14},{6,10},... | collective-permute-start | bytes 104456 | tf_op jit(solution)/shard_map/ppermute | solution.py:42
  26.1 0.0 copy-done.15
  26.1 0.0 copy-done.3
  26.1 0.0 copy-done.7
  26.1 0.0 copy-done.9
  26.1 0.5 %start_state.1 = (f32[32,64,64]{2,1,0:T(8,128)S(1)}, bf16[128,2048]{1,0:T(8,128)(2,1)S(1)}, bf16[128,2048]{1,0:T(8,128)(2,1)S(1)}, f32[8,2304]{1,0:T(8,128)S(1)}, f32[8,2304]{1,0:T(8,128)S(1)}) custom-call(s32[1]{0:T(128)S(6)} %copy.23.accepted, f32[1,3,32,64,64]{4,3,2,1,0:T(8,128)S(1)} %copy-done.3, bf16[1,6,2,1152]{3,2,1,0:T(2,128)(2,1)S(1)} %copy-done.7, ...), custom_call_target="tpu_custom_call" | custom-call | flops 20000000 | tf_op jit(solution)/shard_map/start_state/pallas_call | solution.py:26
  26.7 0.0 copy-done.6
  26.7 0.0 copy-done.12
  26.7 0.0 copy-done.13
  26.7 0.0 copy-done.14
  26.7 0.7 %steps.1 = (f32[5,8,2048]{2,1,0:T(8,128)S(1)}, f32[8,32]{1,0:T(8,128)S(1)}) custom-call(bf16[3,4096]{1,0:T(4,128)(2,1)S(1)} %get-tuple-element.36.normed, bf16[32,4096]{1,0:T(8,128)(2,1)S(1)} %bitcast.9, f32[1,32]{1,0:T(1,128)S(1)} %bitcast.13, f32[1,32]{1,0:T(1,128)S(1)} %bitcast.14, f32[1,32]{1,0:T(1,128)S(1)} %bitcast.15, f32[3,32]{1,0:T(4,128)S(1)} %bitcast.11), custom_call_target="tpu_custom_call" | custom-call | flops 20000000 | tf_op jit(solution)/shard_map/steps/pallas_call | solution.py:26
  27.5 0.0 collective-permute-done.3.refs_1_
  27.5 0.0 collective-permute-done.4.refs_2_
  27.5 0.3 collective-permute-done.5.refs_3_
  27.8 0.0 copy-done.11
  27.8 0.4 mixer.1
  28.2 3.5 %collective-permute-start.8 = (bf16[4,2048]{1,0:T(4,128)(2,1)S(1)}, bf16[4,2048]{1,0:T(4,128)(2,1)S(1)}, u32[]{:S(2)}, u32[]{:S(2)}) collective-permute-start(bf16[4,2048]{1,0:T(4,128)(2,1)S(1)} %get-tuple-element.42.refs_0_), channel_id=1, source_target_pairs={{0,12},{4,8},{8,4},{12,0},{1,13},{5,9},{9,5},{13,1},{2,14},{6,10},... | collective-permute-start | bytes 49160 | tf_op jit(solution)/shard_map/ppermute | solution.py:42
  31.6 0.0 collective-permute-start.7
  31.6 1.0 %collective-permute-start.6 = (bf16[4,2048]{1,0:T(4,128)(2,1)S(1)}, bf16[4,2048]{1,0:T(4,128)(2,1)S(1)}, u32[]{:S(2)}, u32[]{:S(2)}) collective-permute-start(bf16[4,2048]{1,0:T(4,128)(2,1)S(1)} %get-tuple-element.42.refs_0_), channel_id=1, source_target_pairs={{0,4},{4,0},{8,12},{12,8},{1,5},{5,1},{9,13},{13,9},{2,6},{6,2},{1... | collective-permute-start | bytes 49160 | tf_op jit(solution)/shard_map/ppermute | solution.py:42
  32.6 1.1 %collective-permute-done.8.refs_3_ = bf16[4,2048]{1,0:T(4,128)(2,1)S(1)} collective-permute-done((bf16[4,2048]{1,0:T(4,128)(2,1)S(1)}, bf16[4,2048]{1,0:T(4,128)(2,1)S(1)}, u32[]{:S(2)}, u32[]{:S(2)}) %collective-permute-start.8) | collective-permute-done | bytes 16416 | tf_op jit(solution)/shard_map/ppermute | solution.py:42
  33.8 2.5 %collective-permute-done.7.refs_2_ = bf16[4,2048]{1,0:T(4,128)(2,1)S(1)} collective-permute-done((bf16[4,2048]{1,0:T(4,128)(2,1)S(1)}, bf16[4,2048]{1,0:T(4,128)(2,1)S(1)}, u32[]{:S(2)}, u32[]{:S(2)}) %collective-permute-start.7) | collective-permute-done | bytes 16416 | tf_op jit(solution)/shard_map/ppermute | solution.py:42
  36.3 0.0 collective-permute-done.6.refs_1_
  36.3 0.0 copy-done.2
  36.3 0.7 %output.1 = (bf16[4,1024]{1,0:T(4,128)(2,1)S(1)}, bf16[4,1024]{1,0:T(4,128)(2,1)S(1)}, bf16[4,1024]{1,0:T(4,128)(2,1)S(1)}, bf16[4,1024]{1,0:T(4,128)(2,1)S(1)}) custom-call(bf16[4,2048]{1,0:T(4,128)(2,1)S(1)} %get-tuple-element.42.refs_0_, bf16[4,2048]{1,0:T(4,128)(2,1)S(1)} %collective-permute-done.6.refs_1_, ...), custom_call_target="tpu_custom_call" | custom-call | flops 100000000 | tf_op jit(solution)/shard_map/output/pallas_call | solution.py:26
  36.9 0.1 collective-permute-start.9
  37.0 1.6 %collective-permute-start.10 = (bf16[4,1024]{1,0:T(4,128)(2,1)S(1)}, bf16[4,1024]{1,0:T(4,128)(2,1)S(1)}, u32[]{:S(2)}, u32[]{:S(2)}) collective-permute-start(bf16[4,1024]{1,0:T(4,128)(2,1)S(1)} %get-tuple-element.45), channel_id=1, source_target_pairs={{0,2},{1,3},{2,0},{3,1},{4,6},{5,7},{6,4},{7,5},{8,10},{9,11},{10,... | collective-permute-start | bytes 24584 | tf_op jit(solution)/shard_map/ppermute | solution.py:42
  38.6 0.3 collective-permute-start.11
  38.9 2.8 %states.3 = (f32[1,3,32,64,64]{4,3,2,1,0:T(8,128)}, bf16[1,6,2,1152]{3,2,1,0:T(2,128)(2,1)}) custom-call(s32[1]{0:T(128)S(6)} %copy.23.accepted, f32[32,64,64]{2,1,0:T(8,128)S(1)} %get-tuple-element.47.start, f32[8,32]{1,0:T(8,128)S(1)} %get-tuple-element.48.small, f32[8,2304]{1,0:T(8,128)S(1)} %get-tuple-element.49.act, ...), custom_call_target="tpu_custom_call" | custom-call | flops 60000000 | tf_op jit(solution)/shard_map/states/pallas_call | solution.py:26
  41.7 0.0 collective-permute-done.9.refs_1_
  41.7 0.0 collective-permute-done.10.refs_2_
  41.7 0.0 collective-permute-done.11.refs_3_
  41.7 0.6 %final.1 = bf16[1,3,1024]{2,1,0:T(4,128)(2,1)} custom-call(bf16[4,1024]{1,0:T(4,128)(2,1)S(1)} %get-tuple-element.43.refs_0_, bf16[4,1024]{1,0:T(4,128)(2,1)S(1)} %collective-permute-done.9.refs_1_, bf16[4,1024]{1,0:T(4,128)(2,1)S(1)} %collective-permute-done.10.refs_2_, bf16[4,1024]{1,0:T(4,128)(2,1)S(1)} %collective-permute-done.11.refs_3_), custom_call_target="tpu_custom_call" | custom-call | tf_op jit(solution)/shard_map/final/pallas_call | solution.py:26
  (1 shorter events, 0.0 us)
Async XLA Ops:
  0.6 0.8 %copy-start.8 = (bf16[1,3,4096]{2,1,0:T(4,128)(2,1)S(1)}, bf16[1,3,4096]{2,1,0:T(4,128)(2,1)}, u32[]{:S(2)}) copy-start(bf16[1,3,4096]{2,1,0:T(4,128)(2,1)} %tokens.1) | copy-start | bytes 73732
  1.4 0.7 %copy-start.10 = (f32[4096]{0:T(1024)S(1)}, f32[4096]{0:T(1024)}, u32[]{:S(2)}) copy-start(f32[4096]{0:T(1024)} %param.18) | copy-start | bytes 49156
  2.2 5.7 %collective-permute-start = (bf16[3,1024]{1,0:T(4,128)(2,1)S(1)}, bf16[3,1024]{1,0:T(4,128)(2,1)S(1)}, u32[]{:S(2)}, u32[]{:S(2)}) collective-permute-start(bf16[3,1024]{1,0:T(4,128)(2,1)S(1)} %get-tuple-element.29), channel_id=1, source_target_pairs={{0,4},{4,0},{8,12},{12,8},{1,5},{5,1},{9,13},{13,9},{2,6},{6,2},{1... | collective-permute-start | bytes 18440 | tf_op jit(solution)/shard_map/ppermute | solution.py:42
  5.4 4.5 %collective-permute-start.1 = (bf16[3,1024]{1,0:T(4,128)(2,1)S(1)}, bf16[3,1024]{1,0:T(4,128)(2,1)S(1)}, u32[]{:S(2)}, u32[]{:S(2)}) collective-permute-start(bf16[3,1024]{1,0:T(4,128)(2,1)S(1)} %get-tuple-element.30), channel_id=1, source_target_pairs={{0,8},{4,12},{8,0},{12,4},{1,9},{5,13},{9,1},{13,5},{2,10},{6,14},... | collective-permute-start | bytes 18440 | tf_op jit(solution)/shard_map/ppermute | solution.py:42
  8.0 5.4 %collective-permute-start.2 = (bf16[3,1024]{1,0:T(4,128)(2,1)S(1)}, bf16[3,1024]{1,0:T(4,128)(2,1)S(1)}, u32[]{:S(2)}, u32[]{:S(2)}) collective-permute-start(bf16[3,1024]{1,0:T(4,128)(2,1)S(1)} %get-tuple-element.31), channel_id=1, source_target_pairs={{0,12},{4,8},{8,4},{12,0},{1,13},{5,9},{9,5},{13,1},{2,14},{6,10},... | collective-permute-start | bytes 18440 | tf_op jit(solution)/shard_map/ppermute | solution.py:42
  13.4 2.2 %copy-start = (bf16[1024,2048]{1,0:T(8,128)(2,1)S(1)}, bf16[1024,2048]{1,0:T(8,128)(2,1)}, u32[]{:S(2)}) copy-start(bf16[1024,2048]{1,0:T(8,128)(2,1)} %refs_4_.2) | copy-start | bytes 12582916
  15.6 2.2 %copy-start.1 = (bf16[1024,2048]{1,0:T(8,128)(2,1)S(1)}, bf16[1024,2048]{1,0:T(8,128)(2,1)}, u32[]{:S(2)}) copy-start(bf16[1024,2048]{1,0:T(8,128)(2,1)} %refs_7_.1) | copy-start | bytes 12582916
  17.8 0.9 %copy-start.4 = (bf16[1024,128]{1,0:T(8,128)(2,1)S(1)}, bf16[1024,128]{1,0:T(8,128)(2,1)}, u32[]{:S(2)}) copy-start(bf16[1024,128]{1,0:T(8,128)(2,1)} %refs_5_.1) | copy-start | bytes 786436
  18.7 0.9 %copy-start.5 = (bf16[1024,128]{1,0:T(8,128)(2,1)S(1)}, bf16[1024,128]{1,0:T(8,128)(2,1)}, u32[]{:S(2)}) copy-start(bf16[1024,128]{1,0:T(8,128)(2,1)} %refs_6_.1) | copy-start | bytes 786436
  19.7 6.4 %copy-start.15 = (f32[1,3,32]{2,0,1:T(1,128)S(1)}, f32[1,3,32]{2,0,1:T(1,128)}, u32[]{:S(2)}) copy-start(f32[1,3,32]{2,0,1:T(1,128)} %param.31) | copy-start | bytes 1156
  19.7 6.4 %copy-start.3 = (f32[1,3,32,64,64]{4,3,2,1,0:T(8,128)S(1)}, f32[1,3,32,64,64]{4,3,2,1,0:T(8,128)}, u32[]{:S(2)}) copy-start(f32[1,3,32,64,64]{4,3,2,1,0:T(8,128)} %states.2) | copy-start | bytes 4718596
  19.7 6.4 %copy-start.7 = (bf16[1,6,2,1152]{3,2,1,0:T(2,128)(2,1)S(1)}, bf16[1,6,2,1152]{3,2,1,0:T(2,128)(2,1)}, u32[]{:S(2)}) copy-start(bf16[1,6,2,1152]{3,2,1,0:T(2,128)(2,1)} %history.3) | copy-start | bytes 82948
  19.7 6.4 %copy-start.9 = (bf16[4,2,1152]{2,1,0:T(2,128)(2,1)S(1)}, bf16[4,2,1152]{2,1,0:T(2,128)(2,1)}, u32[]{:S(2)}) copy-start(bf16[4,2,1152]{2,1,0:T(2,128)(2,1)} %taps.1) | copy-start | bytes 55300
  19.7 7.0 %copy-start.6 = (bf16[4096,32]{0,1:T(8,128)(2,1)S(1)}, bf16[4096,32]{0,1:T(8,128)(2,1)}, u32[]{:S(2)}) copy-start(bf16[4096,32]{0,1:T(8,128)(2,1)} %param.23) | copy-start | bytes 786436
  19.7 7.0 %copy-start.12 = (f32[32]{0:T(128)S(1)}, f32[32]{0:T(128)}, u32[]{:S(2)}) copy-start(f32[32]{0:T(128)} %param.24) | copy-start | bytes 388
  19.7 7.0 %copy-start.13 = (f32[32]{0:T(128)S(1)}, f32[32]{0:T(128)}, u32[]{:S(2)}) copy-start(f32[32]{0:T(128)} %param.25) | copy-start | bytes 388
  19.7 7.0 %copy-start.14 = (f32[32]{0:T(128)S(1)}, f32[32]{0:T(128)}, u32[]{:S(2)}) copy-start(f32[32]{0:T(128)} %param.26) | copy-start | bytes 388
  19.7 8.0 %copy-start.11 = (f32[2048]{0:T(1024)S(1)}, f32[2048]{0:T(1024)}, u32[]{:S(2)}) copy-start(f32[2048]{0:T(1024)} %param.32) | copy-start | bytes 24580
  21.0 15.2 %copy-start.2 = (bf16[2048,1024]{1,0:T(8,128)(2,1)S(1)}, bf16[2048,1024]{1,0:T(8,128)(2,1)}, u32[]{:S(2)}) copy-start(bf16[2048,1024]{1,0:T(8,128)(2,1)} %refs_4_.3) | copy-start | bytes 12582916
  21.0 6.4 %collective-permute-start.3 = (bf16[4,4352]{1,0:T(4,128)(2,1)S(1)}, bf16[4,4352]{1,0:T(4,128)(2,1)S(1)}, u32[]{:S(2)}, u32[]{:S(2)}) collective-permute-start(bf16[4,4352]{1,0:T(4,128)(2,1)S(1)} %get-tuple-element.33), channel_id=1, source_target_pairs={{0,4},{4,0},{8,12},{12,8},{1,5},{5,1},{9,13},{13,9},{2,6},{6,2},{1... | collective-permute-start | bytes 104456 | tf_op jit(solution)/shard_map/ppermute | solution.py:42
  21.0 6.4 %collective-permute-start.4 = (bf16[4,4352]{1,0:T(4,128)(2,1)S(1)}, bf16[4,4352]{1,0:T(4,128)(2,1)S(1)}, u32[]{:S(2)}, u32[]{:S(2)}) collective-permute-start(bf16[4,4352]{1,0:T(4,128)(2,1)S(1)} %get-tuple-element.34), channel_id=1, source_target_pairs={{0,8},{4,12},{8,0},{12,4},{1,9},{5,13},{9,1},{13,5},{2,10},{6,14},... | collective-permute-start | bytes 104456 | tf_op jit(solution)/shard_map/ppermute | solution.py:42
  21.7 6.1 %collective-permute-start.5 = (bf16[4,4352]{1,0:T(4,128)(2,1)S(1)}, bf16[4,4352]{1,0:T(4,128)(2,1)S(1)}, u32[]{:S(2)}, u32[]{:S(2)}) collective-permute-start(bf16[4,4352]{1,0:T(4,128)(2,1)S(1)} %get-tuple-element.35), channel_id=1, source_target_pairs={{0,12},{4,8},{8,4},{12,0},{1,13},{5,9},{9,5},{13,1},{2,14},{6,10},... | collective-permute-start | bytes 104456 | tf_op jit(solution)/shard_map/ppermute | solution.py:42
  28.2 5.6 %collective-permute-start.8 = (bf16[4,2048]{1,0:T(4,128)(2,1)S(1)}, bf16[4,2048]{1,0:T(4,128)(2,1)S(1)}, u32[]{:S(2)}, u32[]{:S(2)}) collective-permute-start(bf16[4,2048]{1,0:T(4,128)(2,1)S(1)} %get-tuple-element.42.refs_0_), channel_id=1, source_target_pairs={{0,12},{4,8},{8,4},{12,0},{1,13},{5,9},{9,5},{13,1},{2,14},{6,10},... | collective-permute-start | bytes 49160 | tf_op jit(solution)/shard_map/ppermute | solution.py:42
  31.6 4.6 %collective-permute-start.7 = (bf16[4,2048]{1,0:T(4,128)(2,1)S(1)}, bf16[4,2048]{1,0:T(4,128)(2,1)S(1)}, u32[]{:S(2)}, u32[]{:S(2)}) collective-permute-start(bf16[4,2048]{1,0:T(4,128)(2,1)S(1)} %get-tuple-element.42.refs_0_), channel_id=1, source_target_pairs={{0,8},{4,12},{8,0},{12,4},{1,9},{5,13},{9,1},{13,5},{2,10},{6,14},... | collective-permute-start | bytes 49160 | tf_op jit(solution)/shard_map/ppermute | solution.py:42
  31.6 4.6 %collective-permute-start.6 = (bf16[4,2048]{1,0:T(4,128)(2,1)S(1)}, bf16[4,2048]{1,0:T(4,128)(2,1)S(1)}, u32[]{:S(2)}, u32[]{:S(2)}) collective-permute-start(bf16[4,2048]{1,0:T(4,128)(2,1)S(1)} %get-tuple-element.42.refs_0_), channel_id=1, source_target_pairs={{0,4},{4,0},{8,12},{12,8},{1,5},{5,1},{9,13},{13,9},{2,6},{6,2},{1... | collective-permute-start | bytes 49160 | tf_op jit(solution)/shard_map/ppermute | solution.py:42
  36.9 4.7 %collective-permute-start.9 = (bf16[4,1024]{1,0:T(4,128)(2,1)S(1)}, bf16[4,1024]{1,0:T(4,128)(2,1)S(1)}, u32[]{:S(2)}, u32[]{:S(2)}) collective-permute-start(bf16[4,1024]{1,0:T(4,128)(2,1)S(1)} %get-tuple-element.44), channel_id=1, source_target_pairs={{0,1},{1,0},{2,3},{3,2},{4,5},{5,4},{6,7},{7,6},{8,9},{9,8},{10,11... | collective-permute-start | bytes 24584 | tf_op jit(solution)/shard_map/ppermute | solution.py:42
  37.0 4.7 %collective-permute-start.10 = (bf16[4,1024]{1,0:T(4,128)(2,1)S(1)}, bf16[4,1024]{1,0:T(4,128)(2,1)S(1)}, u32[]{:S(2)}, u32[]{:S(2)}) collective-permute-start(bf16[4,1024]{1,0:T(4,128)(2,1)S(1)} %get-tuple-element.45), channel_id=1, source_target_pairs={{0,2},{1,3},{2,0},{3,1},{4,6},{5,7},{6,4},{7,5},{8,10},{9,11},{10,... | collective-permute-start | bytes 24584 | tf_op jit(solution)/shard_map/ppermute | solution.py:42
  38.6 3.1 %collective-permute-start.11 = (bf16[4,1024]{1,0:T(4,128)(2,1)S(1)}, bf16[4,1024]{1,0:T(4,128)(2,1)S(1)}, u32[]{:S(2)}, u32[]{:S(2)}) collective-permute-start(bf16[4,1024]{1,0:T(4,128)(2,1)S(1)} %get-tuple-element.46), channel_id=1, source_target_pairs={{0,3},{1,2},{2,1},{3,0},{4,7},{5,6},{6,5},{7,4},{8,11},{9,10},{10,... | collective-permute-start | bytes 24584 | tf_op jit(solution)/shard_map/ppermute | solution.py:42

commit v2 on v1

--- a/solution.py
+++ b/solution.py
@@ -7,6 +7,7 @@
 from jax.experimental.pallas import tpu as pltpu
 from jax.sharding import PartitionSpec as P
 
+
 epsilon = 1e-06
 F32 = jnp.float32
 BF16 = jnp.bfloat16
@@ -17,30 +18,34 @@
     return pltpu.with_memory_space_constraint(x, pltpu.VMEM)
 
 
+def hbm(x):
+    return pltpu.with_memory_space_constraint(x, pltpu.HBM)
+
+
 VMEM_SPEC = pl.BlockSpec(memory_space=pltpu.VMEM)
 SMEM_SPEC = pl.BlockSpec(memory_space=pltpu.SMEM)
 HBM_SPEC = pl.BlockSpec(memory_space=pl.ANY)
 
 
-def call(body, outs, ins, specs, name, flops=0, scratch=(), out_specs=None, limit=20 << 20):
+def call(body, outs, ins, specs, flops=0, scratch=(), out_specs=None, limit=20 << 20, moved=0, aliases={}):
     return pl.pallas_call(
         body,
         out_shape=outs,
         in_specs=specs,
         out_specs=out_specs or [VMEM_SPEC] * len(outs),
         scratch_shapes=list(scratch),
-        cost_estimate=pl.CostEstimate(flops=flops, transcendentals=0, bytes_accessed=0),
+        input_output_aliases=aliases,
+        cost_estimate=pl.CostEstimate(flops=flops, transcendentals=0, bytes_accessed=moved),
         compiler_params=pltpu.CompilerParams(vmem_limit_bytes=limit),
-        name=name,
     )(*ins)
 
 
 def exchange(blocks, axis, count):
     got = []
-    for step in range(1, count):
+    for step in reversed(range(1, count)):
         pairs = [(i, i ^ step) for i in range(count)]
         got.append(lax.ppermute(blocks[step], axis, pairs))
-    return got
+    return got[::-1]
 
 
 def silu(v):
@@ -63,7 +68,7 @@
         slices[step][...] = normed[:, pl.ds(start, width)]
 
 
-def step_body(head_dim, normed, step_t, bias, rate, direct, extra, coef, small, table):
+def step_body(head_dim, accepted, normed, step_t, bias, rate, direct, extra, coef, small, table):
     props, heads = extra.shape
     raw = lax.dot_general(
         normed[...], step_t[...], (((1,), (1,)), ((), ())), preferred_element_type=F32
@@ -96,11 +101,9 @@
         coef[part] = wide[part * ROWS : (part + 1) * ROWS]
 
 
-def state_body(accepted, states, history, taps, start, high, low, early, taps_wide, sem):
+def state_body(accepted, states, history, taps, high, low, early, taps_wide):
     count = accepted[0]
-    copy = pltpu.make_async_copy(states.at[0, count - 1], start, sem)
-    copy.start()
-    heads, head_dim, size = start.shape
+    heads, head_dim, size = states.shape[2:]
     groups = taps.shape[1]
     tap_count = taps.shape[0]
     inner = heads // groups * head_dim
@@ -133,12 +136,11 @@
 
     high[...] = jnp.zeros_like(high)
     low[...] = jnp.zeros_like(low)
-    copy.wait()
     pair = 128 // head_dim
     for g in range(groups):
         for block in range(per // pair):
             at = g * per + block * pair
-            tile = start[at : at + pair].reshape(pair * head_dim, size).T
+            tile = states[0, count - 1, at : at + pair].reshape(pair * head_dim, size).T
             big, rest = split(tile)
             cols = slice(at * head_dim, (at + pair) * head_dim)
             high[g * size : (g + 1) * size, cols] = big
@@ -225,69 +227,75 @@
     gated[...] = norms[0:4].astype(BF16)
 
 
-def tail_body(props, accepted, start, small, act, coef, fresh, history, states, tail, held, sem):
-    heads, head_dim, size = start.shape
+def states_body(props, g, accepted, start, small, act, coef, fresh, history, *refs):
+    if g == 0:
+        states, tail, flag, held, sem = refs
+        flag[...] = jnp.zeros_like(flag)
+    else:
+        _, states, held, sem = refs
+    heads, head_dim, size = start.shape[2:]
     groups = history.shape[2]
     per = heads // groups
     inner = per * head_dim
     wide = heads * head_dim
     count = accepted[0]
-    before = tail.shape[1] - props
-    for k in range(before):
-        tail[0, k] = history[0, count + k]
+    lanes = slice(g * inner, (g + 1) * inner)
+    row_at = lax.broadcasted_iota(jnp.int32, (ROWS, 1), 0)
+    steps = jnp.zeros((ROWS, inner), F32)
     for j in range(props):
-        rows = []
-        for g in range(groups):
-            row = [fresh[j : j + 1, g * inner : (g + 1) * inner]]
-            for part in range(2):
-                base = wide + part * groups * size + g * size
-                row.append(fresh[j : j + 1, base : base + size])
-            rows.append(jnp.concatenate(row, axis=1))
-        tail[0, before + j] = jnp.concatenate(rows, axis=0).astype(BF16)
-    x = act[:, :wide]
-    row_at = lax.broadcasted_iota(jnp.int32, (ROWS, 1), 0)
-    steps = jnp.zeros((ROWS, wide), F32)
-    for j in range(props):
-        steps = jnp.where(row_at == j, coef[1 + j], steps)
-    dx = x * steps
+        steps = jnp.where(row_at == j, coef[1 + j, :, lanes], steps)
+    dx = act[:, lanes] * steps
     dx_high, dx_low = split(dx)
     dx_high, dx_low = dx_high.astype(F32), dx_low.astype(F32)
     left = jnp.concatenate(
         [dx_high, dx_low, dx_high, jnp.zeros_like(dx)], axis=0
     ).astype(BF16)
-    b = act[:, wide : wide + groups * size]
-    b_high, b_low = split(b)
+    b_high, b_low = split(act[:, wide : wide + groups * size])
     b_high, b_low = b_high.astype(F32), b_low.astype(F32)
+    blocks = []
+    for j in range(props):
+        hi = jnp.where(row_at == j, b_high, 0.0)
+        lo = jnp.where(row_at == j, b_low, 0.0)
+        full = jnp.concatenate([hi, hi, lo, jnp.zeros_like(hi)], axis=0)
+        if g:
+            full = pltpu.roll(full, groups * size - g * size, 1)
+        blocks.append(full)
+    right = jnp.concatenate(blocks, axis=1).astype(BF16)
+    update = lax.dot_general(
+        left, right, (((0,), (0,)), ((), ())), preferred_element_type=F32
+    )
+    block = groups * size
     copies = []
-    for g in range(groups):
-        blocks = []
+    half = per // 2
+    for h in range(per):
+        at = g * per + h
+        state = start[0, count - 1, at]
         for j in range(props):
-            hi = jnp.where(row_at == j, b_high, 0.0)
-            lo = jnp.where(row_at == j, b_low, 0.0)
-            full = jnp.concatenate([hi, hi, lo, jnp.zeros_like(hi)], axis=0)
-            if g:
-                full = pltpu.roll(full, groups * size - g * size, 1)
-            blocks.append(full)
-        right = jnp.concatenate(blocks, axis=1).astype(BF16)
-        update = lax.dot_general(
-            left[:, g * inner : (g + 1) * inner],
-            right,
-            (((0,), (0,)), ((), ())),
-            preferred_element_type=F32,
-        )
-        lanes = groups * size
-        for h in range(per):
-            at = g * per + h
-            state = start[at]
-            for j in range(props):
-                new = update[h * head_dim : (h + 1) * head_dim, j * lanes : j * lanes + size]
-                state = state * small[j : j + 1, at : at + 1] + new
-                held[j, at] = state
-        copy = pltpu.make_async_copy(
-            held.at[:, pl.ds(g * per, per)], states.at[0, :, pl.ds(g * per, per)], sem.at[g]
-        )
-        copy.start()
-        copies.append(copy)
+            new = update[h * head_dim : (h + 1) * head_dim, j * block : j * block + size]
+            state = state * small[j : j + 1, at : at + 1] + new
+            held[j, h] = state
+        if (h + 1) % half == 0:
+            first = h + 1 - half
+            copy = pltpu.make_async_copy(
+                held.at[:, pl.ds(first, half)],
+                states.at[0, :, pl.ds(g * per + first, half)],
+                sem.at[len(copies)],
+            )
+            copy.start()
+            copies.append(copy)
+    if g == 0:
+        before = tail.shape[1] - props
+        for k in range(before):
+            tail[0, k] = history[0, count + k]
+        for j in range(props):
+            rows = []
+            for q in range(groups):
+                row = [fresh[j : j + 1, q * inner : (q + 1) * inner]]
+                for part in range(2):
+                    base = wide + part * groups * size + q * size
+                    row.append(fresh[j : j + 1, base : base + size])
+                rows.append(jnp.concatenate(row, axis=1))
+            tail[0, before + j] = jnp.concatenate(rows, axis=0).astype(BF16)
     for copy in copies:
         copy.wait()
 
@@ -295,7 +303,7 @@
 def output_body(count, *refs):
     parts = refs[:count]
     weight = refs[count]
-    outs = refs[count + 1 : count + 1 + count]
+    outs = refs[count + 2 : count + 2 + count]
     result, lhs = refs[-2:]
     which = lax.bitwise_xor(lax.axis_index("kv"), lax.axis_index("tp"))
     product = jnp.dot(stack_rows(parts, lhs), weight[...], preferred_element_type=F32)
@@ -335,7 +343,7 @@
 ):
     _, props, width = tokens.shape
     heads = step_size_bias.shape[0]
-    _, tail_rows, groups, channels = convolution_history_rows.shape
+    _, _, groups, channels = convolution_history_rows.shape
     head_dim, size = per_proposal_states.shape[3:]
     inner = heads * head_dim
     conv = groups * channels
@@ -346,16 +354,18 @@
     normed, *slices = call(
         functools.partial(norm_body, count),
         [pltpu.VMEM((props, width), BF16)] + [pltpu.VMEM((props, rows), BF16)] * count,
-        [tokens, input_norm_scale.reshape(1, width)],
+        [hbm(tokens), hbm(input_norm_scale.reshape(1, width))],
         [VMEM_SPEC] * 2,
-        "norm",
+        flops=1_000_000_000_000, moved=10_000_000_000,
     )
     received = exchange(slices, "kv", count)
+    matrices = [head_input_matrix, group_input_matrix, group_readout_matrix, output_gate_matrix]
 
     coef, small = call(
         functools.partial(step_body, head_dim),
         [pltpu.VMEM((props + 2, ROWS, inner), F32), pltpu.VMEM((ROWS, heads), F32)],
         [
+            accepted,
             vmem(normed),
             vmem(step_size_matrix.T),
             step_size_bias.reshape(1, heads),
@@ -363,42 +373,30 @@
             direct_path_weight.reshape(1, heads),
             proposal_extra_decay.reshape(props, heads),
         ],
-        [VMEM_SPEC] * 6,
-        "steps",
+        [SMEM_SPEC] + [VMEM_SPEC] * 6,
         flops=20_000_000,
         scratch=[pltpu.VMEM(((props + 2) * ROWS, heads), F32)],
     )
-    start, high, low, early, taps = call(
+    states = vmem(per_proposal_states)
+    high, low, early, taps = call(
         state_body,
         [
-            pltpu.VMEM((heads, head_dim, size), F32),
             pltpu.VMEM((groups * size, inner), BF16),
             pltpu.VMEM((groups * size, inner), BF16),
             pltpu.VMEM((ROWS, conv), F32),
             pltpu.VMEM((ROWS, conv), F32),
         ],
-        [accepted, per_proposal_states, convolution_history_rows, convolution_tap_weight],
-        [SMEM_SPEC, HBM_SPEC, VMEM_SPEC, VMEM_SPEC],
-        "start_state",
+        [accepted, states, convolution_history_rows, convolution_tap_weight],
+        [SMEM_SPEC] + [VMEM_SPEC] * 3,
         flops=20_000_000,
-        scratch=[pltpu.SemaphoreType.DMA],
     )
 
     own, *partials = call(
         functools.partial(project_body, count),
         [pltpu.VMEM((4, total), F32)] + [pltpu.VMEM((4, total), BF16)] * (count - 1),
         [vmem(s) for s in [slices[0]] + received]
-        + [
-            vmem(w)
-            for w in (
-                head_input_matrix,
-                group_input_matrix,
-                group_readout_matrix,
-                output_gate_matrix,
-            )
-        ],
+        + matrices,
         [VMEM_SPEC] * (count + 4),
-        "project",
         flops=200_000_000,
         scratch=[pltpu.VMEM((4 * count, rows), F32)],
     )
@@ -413,35 +411,42 @@
         [vmem(v) for v in [own] + sums + [coef, early, taps, high, low]]
         + [vmem(group_norm_scale.reshape(1, inner))],
         [VMEM_SPEC] * (count + 6),
-        "mixer",
         flops=20_000_000,
         scratch=[pltpu.VMEM((ROWS, total), F32), pltpu.VMEM((ROWS, inner), F32)],
     )
     gathered = exchange([gated] * count, "kv", count)
-    new_states, new_tail = call(
-        functools.partial(tail_body, props),
-        [
-            jax.ShapeDtypeStruct((1, props, heads, head_dim, size), F32),
-            jax.ShapeDtypeStruct(convolution_history_rows.shape, BF16),
-        ],
-        [accepted]
-        + [vmem(v) for v in (start, small, act, coef, fresh)]
-        + [convolution_history_rows],
-        [SMEM_SPEC] + [VMEM_SPEC] * 6,
-        "states",
-        flops=60_000_000,
-        out_specs=[HBM_SPEC, VMEM_SPEC],
-        scratch=[
-            pltpu.VMEM((props, heads, head_dim, size), F32),
-            pltpu.SemaphoreType.DMA((groups,)),
-        ],
-    )
+    new_states = None
+    for g in range(groups):
+        shape = jax.ShapeDtypeStruct((1, props, heads, head_dim, size), F32)
+        outs = [shape]
+        if g == 0:
+            outs += [
+                jax.ShapeDtypeStruct(convolution_history_rows.shape, BF16),
+                pltpu.VMEM((ROWS, 128), F32),
+            ]
+        result = call(
+            functools.partial(states_body, props, g),
+            outs,
+            [accepted, states]
+            + [vmem(v) for v in (small, act, coef, fresh, convolution_history_rows)]
+            + ([hbm(new_states)] if g else []),
+            [SMEM_SPEC] + [VMEM_SPEC] * 6 + ([HBM_SPEC] if g else []),
+            flops=30_000_000,
+            out_specs=[HBM_SPEC] + [VMEM_SPEC] * (len(outs) - 1),
+            scratch=[
+                pltpu.VMEM((props, heads // groups, head_dim, size), F32),
+                pltpu.SemaphoreType.DMA((2,)),
+            ],
+            aliases={7: 0} if g else {},
+        )
+        new_states = result[0]
+        if g == 0:
+            new_tail, flag = result[1:]
     blocks = call(
         functools.partial(output_body, count),
         [pltpu.VMEM((4, out_cols), BF16)] * count,
-        [vmem(v) for v in [gated] + gathered + [output_projection_matrix]],
-        [VMEM_SPEC] * (count + 1),
-        "output",
+        [vmem(v) for v in [gated] + gathered + [output_projection_matrix, flag]],
+        [VMEM_SPEC] * (count + 2),
         flops=100_000_000,
         scratch=[
             pltpu.VMEM((count, ROWS, out_cols), F32),
@@ -454,7 +459,6 @@
         [jax.ShapeDtypeStruct((1, props, out_cols), BF16)],
         [vmem(v) for v in [blocks[0]] + last],
         [VMEM_SPEC] * count,
-        "final",
     )
     return (mixed, new_states, new_tail)
 
@@ -551,7 +555,7 @@
     group_norm_scale,
     output_projection_matrix,
 ):
-    local_seqs, proposals, width = tokens.shape
+    local_seqs, proposals, _ = tokens.shape
     head_local = step_size_bias.shape[0]
     group_local = convolution_tap_weight.shape[1]
     head_dim = per_proposal_states.shape[3]

time: 42.7 us -> 35.7 us (0.84)
  local copies, waits for them, and re-layouts: 7.79 us -> 0.08 us
  Pallas kernels: 7.16 us -> 8.78 us
  waiting for transfers between devices: 9.38 us -> 8.61 us
    unnamed x33 -> x29, local copies, waits for them, and re-layouts: 7.79 us -> 0.08 us
    pallas_call x8 -> x9, Pallas kernels: 7.16 us -> 8.78 us  [call(): pl.pallas_call(body, out_shape=outs, in_specs=specs, out_specs=out_specs...]
    ppermute x12, waiting for transfers between devices: 9.38 us -> 8.61 us  [exchange(): got.append(lax.ppermute(blocks[step], axis, pairs))]
  transfers between devices with their start and end apart: 12 -> 12, of which waited for: 5 -> 6; matrix products, arithmetic and copies ran while one was open for 0% -> 0% of each run, Pallas kernels for 10% -> 14%
where the time goes in v2:
time: 35.7 us; the launch traced here: 35.5 us
  starting transfers between devices  16.5 us (46%)
  Pallas kernels  8.78 us (25%)
  waiting for transfers between devices  8.61 us (24%)
  between operations  1.57 us (4%)
    ppermute x12, starting transfers between devices, exchange(): got.append(lax.ppermute(blocks[step], axis, pairs))  16.5 us
    pallas_call x9, Pallas kernels, call(): pl.pallas_call(body, out_shape=outs, in_specs=specs, out_specs=out_specs...  8.78 us
    ppermute x12, waiting for transfers between devices, exchange(): got.append(lax.ppermute(blocks[step], axis, pairs))  8.61 us
  transfers between devices with their start and end apart: 12, of which 6 were waited for; matrix products, arithmetic and copies ran while one was open for 0% of the time, Pallas kernels for 14%

profile of v2, /device:TPU:0, one launch (start us, length us, event | category | flops | bytes accessed | tf_op | source)
XLA Modules:
  0.0 35.5 jit_solution(7215326063388576636)
XLA Ops:
  0.6 0.0 copy-start.2
  0.6 0.0 copy-start.3
  0.7 0.0 copy-start.4
  0.7 0.0 copy-start.5
  0.7 1.0 %shard_map.184 = (bf16[3,4096]{1,0:T(4,128)(2,1)S(1)}, bf16[3,1024]{1,0:T(4,128)(2,1)S(1)}, bf16[3,1024]{1,0:T(4,128)(2,1)S(1)}, bf16[3,1024]{1,0:T(4,128)(2,1)S(1)}, bf16[3,1024]{1,0:T(4,128)(2,1)S(1)}) custom-call(bf16[1,3,4096]{2,1,0:T(4,128)(2,1)} %tokens.1, f32[1,4096]{1,0:T(1,128)} %bitcast.15), custom_call_target="tpu_custom_call" | custom-call | flops 999999995904 | bytes 10000000000 | tf_op jit(solution)/shard_map/pallas_call | solution.py:31
  1.7 3.1 %collective-permute-start = (bf16[3,1024]{1,0:T(4,128)(2,1)S(1)}, bf16[3,1024]{1,0:T(4,128)(2,1)S(1)}, u32[]{:S(2)}, u32[]{:S(2)}) collective-permute-start(bf16[3,1024]{1,0:T(4,128)(2,1)S(1)} %get-tuple-element.29), channel_id=1, source_target_pairs={{0,4},{4,0},{8,12},{12,8},{1,5},{5,1},{9,13},{13,9},{2,6},{6,2},{1... | collective-permute-start | bytes 18440 | tf_op jit(solution)/shard_map/ppermute | solution.py:47
  4.8 2.6 %collective-permute-start.1 = (bf16[3,1024]{1,0:T(4,128)(2,1)S(1)}, bf16[3,1024]{1,0:T(4,128)(2,1)S(1)}, u32[]{:S(2)}, u32[]{:S(2)}) collective-permute-start(bf16[3,1024]{1,0:T(4,128)(2,1)S(1)} %get-tuple-element.30), channel_id=1, source_target_pairs={{0,8},{4,12},{8,0},{12,4},{1,9},{5,13},{9,1},{13,5},{2,10},{6,14},... | collective-permute-start | bytes 18440 | tf_op jit(solution)/shard_map/ppermute | solution.py:47
  7.4 0.0 collective-permute-start.2
  7.4 0.0 collective-permute-done.refs_1_
  7.4 2.0 %collective-permute-done.1.refs_2_ = bf16[3,1024]{1,0:T(4,128)(2,1)S(1)} collective-permute-done((bf16[3,1024]{1,0:T(4,128)(2,1)S(1)}, bf16[3,1024]{1,0:T(4,128)(2,1)S(1)}, u32[]{:S(2)}, u32[]{:S(2)}) %collective-permute-start.1) | collective-permute-done | bytes 6176 | tf_op jit(solution)/shard_map/ppermute | solution.py:47
  9.4 3.5 %collective-permute-done.2.refs_3_ = bf16[3,1024]{1,0:T(4,128)(2,1)S(1)} collective-permute-done((bf16[3,1024]{1,0:T(4,128)(2,1)S(1)}, bf16[3,1024]{1,0:T(4,128)(2,1)S(1)}, u32[]{:S(2)}, u32[]{:S(2)}) %collective-permute-start.2) | collective-permute-done | bytes 6176 | tf_op jit(solution)/shard_map/ppermute | solution.py:47
  12.9 0.0 copy-done.2
  12.9 0.0 copy-done.3
  12.9 0.0 copy-done.4
  12.9 0.0 copy-done.5
  12.9 0.0 copy-start.13
  12.9 0.0 copy-start
  12.9 0.0 copy-start.7
  12.9 0.0 copy-start.8
  13.0 0.0 copy-start.6
  13.0 0.0 copy-start.10
  13.0 0.0 copy-start.11
  13.0 0.0 copy-start.12
  13.0 0.0 copy-start.9
  13.0 1.3 %shard_map.185 = (f32[4,4352]{1,0:T(4,128)S(1)}, bf16[4,4352]{1,0:T(4,128)(2,1)S(1)}, bf16[4,4352]{1,0:T(4,128)(2,1)S(1)}, bf16[4,4352]{1,0:T(4,128)(2,1)S(1)}) custom-call(bf16[3,1024]{1,0:T(4,128)(2,1)S(1)} %get-tuple-element.28.refs_0_, bf16[3,1024]{1,0:T(4,128)(2,1)S(1)} %collective-permute-done.refs_1_, ...), custom_call_target="tpu_custom_call" | custom-call | flops 200000000 | tf_op jit(solution)/shard_map/pallas_call | solution.py:31
  14.3 0.0 collective-permute-start.3
  14.3 0.7 %collective-permute-start.4 = (bf16[4,4352]{1,0:T(4,128)(2,1)S(1)}, bf16[4,4352]{1,0:T(4,128)(2,1)S(1)}, u32[]{:S(2)}, u32[]{:S(2)}) collective-permute-start(bf16[4,4352]{1,0:T(4,128)(2,1)S(1)} %get-tuple-element.34), channel_id=1, source_target_pairs={{0,8},{4,12},{8,0},{12,4},{1,9},{5,13},{9,1},{13,5},{2,10},{6,14},... | collective-permute-start | bytes 104456 | tf_op jit(solution)/shard_map/ppermute | solution.py:47
  14.9 3.7 %collective-permute-start.5 = (bf16[4,4352]{1,0:T(4,128)(2,1)S(1)}, bf16[4,4352]{1,0:T(4,128)(2,1)S(1)}, u32[]{:S(2)}, u32[]{:S(2)}) collective-permute-start(bf16[4,4352]{1,0:T(4,128)(2,1)S(1)} %get-tuple-element.35), channel_id=1, source_target_pairs={{0,12},{4,8},{8,4},{12,0},{1,13},{5,9},{9,5},{13,1},{2,14},{6,10},... | collective-permute-start | bytes 104456 | tf_op jit(solution)/shard_map/ppermute | solution.py:47
  19.3 0.0 copy-done.13
  19.4 0.0 copy-done
  19.4 0.0 copy-done.7
  19.4 0.0 copy-done.8
  19.4 0.0 copy-start.1
  19.4 0.4 %shard_map.187 = (bf16[128,2048]{1,0:T(8,128)(2,1)S(1)}, bf16[128,2048]{1,0:T(8,128)(2,1)S(1)}, f32[8,2304]{1,0:T(8,128)S(1)}, f32[8,2304]{1,0:T(8,128)S(1)}) custom-call(s32[1]{0:T(128)S(6)} %copy.25.accepted, f32[1,3,32,64,64]{4,3,2,1,0:T(8,128)S(1)} %copy-done, bf16[1,6,2,1152]{3,2,1,0:T(2,128)(2,1)S(1)} %copy-done.7, bf16[4,2,1152]{2,1,0:T(2,128)(2,1)S(1)} %copy-done.8), custom_call_target="tpu_custom_call" | custom-call | flops 20000000 | tf_op jit(solution)/shard_map/pallas_call | solution.py:31
  19.8 0.0 copy-done.6
  19.8 0.0 copy-done.10
  19.8 0.0 copy-done.11
  19.8 0.0 copy-done.12
  19.8 0.7 %shard_map.186 = (f32[5,8,2048]{2,1,0:T(8,128)S(1)}, f32[8,32]{1,0:T(8,128)S(1)}) custom-call(s32[1]{0:T(128)S(6)} %copy.25.accepted, bf16[3,4096]{1,0:T(4,128)(2,1)S(1)} %get-tuple-element.36.normed, bf16[32,4096]{1,0:T(8,128)(2,1)S(1)} %bitcast.9, f32[1,32]{1,0:T(1,128)S(1)} %bitcast.12, f32[1,32]{1,0:T(1,128)S(1)} %bitcast.13, f32[1,32]{1,0:T(1,128)S(1)} %bitcast.14, ...), custom_call_target="tpu_custom_call" | custom-call | flops 20000000 | tf_op jit(solution)/shard_map/pallas_call | solution.py:31
  20.6 0.0 collective-permute-done.3.refs_1_
  20.6 0.0 collective-permute-done.4.refs_2_
  20.6 0.4 %collective-permute-done.5.refs_3_ = bf16[4,4352]{1,0:T(4,128)(2,1)S(1)} collective-permute-done((bf16[4,4352]{1,0:T(4,128)(2,1)S(1)}, bf16[4,4352]{1,0:T(4,128)(2,1)S(1)}, u32[]{:S(2)}, u32[]{:S(2)}) %collective-permute-start.5) | collective-permute-done | bytes 34848 | tf_op jit(solution)/shard_map/ppermute | solution.py:47
  21.0 0.0 copy-done.9
  21.0 0.4 %shard_map.188 = (bf16[4,2048]{1,0:T(4,128)(2,1)S(1)}, f32[8,2304]{1,0:T(8,128)S(1)}, f32[8,2304]{1,0:T(8,128)S(1)}) custom-call(f32[4,4352]{1,0:T(4,128)S(1)} %get-tuple-element.32.refs_0_, bf16[4,4352]{1,0:T(4,128)(2,1)S(1)} %collective-permute-done.3.refs_1_, bf16[4,4352]{1,0:T(4,128)(2,1)S(1)} %collective-permute-done.4.refs_2_, ...), custom_call_target="tpu_custom_call" | custom-call | flops 20000000 | tf_op jit(solution)/shard_map/pallas_call | solution.py:31
  21.4 3.5 %collective-permute-start.8 = (bf16[4,2048]{1,0:T(4,128)(2,1)S(1)}, bf16[4,2048]{1,0:T(4,128)(2,1)S(1)}, u32[]{:S(2)}, u32[]{:S(2)}) collective-permute-start(bf16[4,2048]{1,0:T(4,128)(2,1)S(1)} %get-tuple-element.42.refs_0_), channel_id=1, source_target_pairs={{0,12},{4,8},{8,4},{12,0},{1,13},{5,9},{9,5},{13,1},{2,14},{6,10},... | collective-permute-start | bytes 49160 | tf_op jit(solution)/shard_map/ppermute | solution.py:47
  24.9 0.0 collective-permute-start.7
  24.9 1.0 %collective-permute-start.6 = (bf16[4,2048]{1,0:T(4,128)(2,1)S(1)}, bf16[4,2048]{1,0:T(4,128)(2,1)S(1)}, u32[]{:S(2)}, u32[]{:S(2)}) collective-permute-start(bf16[4,2048]{1,0:T(4,128)(2,1)S(1)} %get-tuple-element.42.refs_0_), channel_id=1, source_target_pairs={{0,4},{4,0},{8,12},{12,8},{1,5},{5,1},{9,13},{13,9},{2,6},{6,2},{1... | collective-permute-start | bytes 49160 | tf_op jit(solution)/shard_map/ppermute | solution.py:47
  25.9 2.1 %shard_map.189 = (f32[1,3,32,64,64]{4,3,2,1,0:T(8,128)}, bf16[1,6,2,1152]{3,2,1,0:T(2,128)(2,1)}, f32[8,128]{1,0:T(8,128)S(1)}) custom-call(s32[1]{0:T(128)S(6)} %copy.25.accepted, f32[1,3,32,64,64]{4,3,2,1,0:T(8,128)S(1)} %copy-done, f32[8,32]{1,0:T(8,128)S(1)} %get-tuple-element.43.small, f32[8,2304]{1,0:T(8,128)S(1)} %get-tuple-element.44.act, ...), custom_call_target="tpu_custom_call" | custom-call | flops 30000000 | tf_op jit(solution)/shard_map/pallas_call | solution.py:31
  28.0 0.0 collective-permute-done.8.refs_3_
  28.0 1.5 %collective-permute-done.7.refs_2_ = bf16[4,2048]{1,0:T(4,128)(2,1)S(1)} collective-permute-done((bf16[4,2048]{1,0:T(4,128)(2,1)S(1)}, bf16[4,2048]{1,0:T(4,128)(2,1)S(1)}, u32[]{:S(2)}, u32[]{:S(2)}) %collective-permute-start.7) | collective-permute-done | bytes 16416 | tf_op jit(solution)/shard_map/ppermute | solution.py:47
  29.5 0.0 collective-permute-done.6.refs_1_
  29.5 0.0 copy-done.1
  29.5 0.7 %shard_map.190 = (bf16[4,1024]{1,0:T(4,128)(2,1)S(1)}, bf16[4,1024]{1,0:T(4,128)(2,1)S(1)}, bf16[4,1024]{1,0:T(4,128)(2,1)S(1)}, bf16[4,1024]{1,0:T(4,128)(2,1)S(1)}) custom-call(bf16[4,2048]{1,0:T(4,128)(2,1)S(1)} %get-tuple-element.42.refs_0_, bf16[4,2048]{1,0:T(4,128)(2,1)S(1)} %collective-permute-done.6.refs_1_, ...), custom_call_target="tpu_custom_call" | custom-call | flops 100000000 | tf_op jit(solution)/shard_map/pallas_call | solution.py:31
  30.2 0.1 collective-permute-start.9
  30.3 1.6 %collective-permute-start.10 = (bf16[4,1024]{1,0:T(4,128)(2,1)S(1)}, bf16[4,1024]{1,0:T(4,128)(2,1)S(1)}, u32[]{:S(2)}, u32[]{:S(2)}) collective-permute-start(bf16[4,1024]{1,0:T(4,128)(2,1)S(1)} %get-tuple-element.49), channel_id=1, source_target_pairs={{0,2},{1,3},{2,0},{3,1},{4,6},{5,7},{6,4},{7,5},{8,10},{9,11},{10,... | collective-permute-start | bytes 24584 | tf_op jit(solution)/shard_map/ppermute | solution.py:47
  31.8 0.3 collective-permute-start.11
  32.1 1.5 %shard_map.192 = f32[1,3,32,64,64]{4,3,2,1,0:T(8,128)} custom-call(s32[1]{0:T(128)S(6)} %copy.25.accepted, f32[1,3,32,64,64]{4,3,2,1,0:T(8,128)S(1)} %copy-done, f32[8,32]{1,0:T(8,128)S(1)} %get-tuple-element.43.small, f32[8,2304]{1,0:T(8,128)S(1)} %get-tuple-element.44.act, ...), custom_call_target="tpu_custom_call", output_to_operand_aliasing={{}: (7, {})} | custom-call | flops 30000000 | tf_op jit(solution)/shard_map/pallas_call | solution.py:31
  33.7 0.0 collective-permute-done.9.refs_1_
  33.7 0.3 collective-permute-done.10.refs_2_
  34.0 0.9 %collective-permute-done.11.refs_3_ = bf16[4,1024]{1,0:T(4,128)(2,1)S(1)} collective-permute-done((bf16[4,1024]{1,0:T(4,128)(2,1)S(1)}, bf16[4,1024]{1,0:T(4,128)(2,1)S(1)}, u32[]{:S(2)}, u32[]{:S(2)}) %collective-permute-start.11) | collective-permute-done | bytes 8224 | tf_op jit(solution)/shard_map/ppermute | solution.py:47
  34.9 0.6 %shard_map.191 = bf16[1,3,1024]{2,1,0:T(4,128)(2,1)} custom-call(bf16[4,1024]{1,0:T(4,128)(2,1)S(1)} %get-tuple-element.47.refs_0_, bf16[4,1024]{1,0:T(4,128)(2,1)S(1)} %collective-permute-done.9.refs_1_, bf16[4,1024]{1,0:T(4,128)(2,1)S(1)} %collective-permute-done.10.refs_2_, bf16[4,1024]{1,0:T(4,128)(2,1)S(1)} %collective-permute-done.11.refs_3_), custom_call_target="tpu_custom_call" | custom-call | tf_op jit(solution)/shard_map/pallas_call | solution.py:31
  (1 shorter events, 0.0 us)
Async XLA Ops:
  0.6 12.3 %copy-start.2 = (bf16[1024,2048]{1,0:T(8,128)(2,1)S(1)}, bf16[1024,2048]{1,0:T(8,128)(2,1)}, u32[]{:S(2)}) copy-start(bf16[1024,2048]{1,0:T(8,128)(2,1)} %refs_4_.2) | copy-start | bytes 12582916
  0.6 12.2 %copy-start.3 = (bf16[1024,2048]{1,0:T(8,128)(2,1)S(1)}, bf16[1024,2048]{1,0:T(8,128)(2,1)}, u32[]{:S(2)}) copy-start(bf16[1024,2048]{1,0:T(8,128)(2,1)} %refs_7_.1) | copy-start | bytes 12582916
  0.7 12.2 %copy-start.4 = (bf16[1024,128]{1,0:T(8,128)(2,1)S(1)}, bf16[1024,128]{1,0:T(8,128)(2,1)}, u32[]{:S(2)}) copy-start(bf16[1024,128]{1,0:T(8,128)(2,1)} %refs_5_.1) | copy-start | bytes 786436
  0.7 12.2 %copy-start.5 = (bf16[1024,128]{1,0:T(8,128)(2,1)S(1)}, bf16[1024,128]{1,0:T(8,128)(2,1)}, u32[]{:S(2)}) copy-start(bf16[1024,128]{1,0:T(8,128)(2,1)} %refs_6_.1) | copy-start | bytes 786436
  1.7 5.7 %collective-permute-start = (bf16[3,1024]{1,0:T(4,128)(2,1)S(1)}, bf16[3,1024]{1,0:T(4,128)(2,1)S(1)}, u32[]{:S(2)}, u32[]{:S(2)}) collective-permute-start(bf16[3,1024]{1,0:T(4,128)(2,1)S(1)} %get-tuple-element.29), channel_id=1, source_target_pairs={{0,4},{4,0},{8,12},{12,8},{1,5},{5,1},{9,13},{13,9},{2,6},{6,2},{1... | collective-permute-start | bytes 18440 | tf_op jit(solution)/shard_map/ppermute | solution.py:47
  4.8 4.5 %collective-permute-start.1 = (bf16[3,1024]{1,0:T(4,128)(2,1)S(1)}, bf16[3,1024]{1,0:T(4,128)(2,1)S(1)}, u32[]{:S(2)}, u32[]{:S(2)}) collective-permute-start(bf16[3,1024]{1,0:T(4,128)(2,1)S(1)} %get-tuple-element.30), channel_id=1, source_target_pairs={{0,8},{4,12},{8,0},{12,4},{1,9},{5,13},{9,1},{13,5},{2,10},{6,14},... | collective-permute-start | bytes 18440 | tf_op jit(solution)/shard_map/ppermute | solution.py:47
  7.4 5.4 %collective-permute-start.2 = (bf16[3,1024]{1,0:T(4,128)(2,1)S(1)}, bf16[3,1024]{1,0:T(4,128)(2,1)S(1)}, u32[]{:S(2)}, u32[]{:S(2)}) collective-permute-start(bf16[3,1024]{1,0:T(4,128)(2,1)S(1)} %get-tuple-element.31), channel_id=1, source_target_pairs={{0,12},{4,8},{8,4},{12,0},{1,13},{5,9},{9,5},{13,1},{2,14},{6,10},... | collective-permute-start | bytes 18440 | tf_op jit(solution)/shard_map/ppermute | solution.py:47
  12.9 6.4 %copy-start.13 = (f32[1,3,32]{2,0,1:T(1,128)S(1)}, f32[1,3,32]{2,0,1:T(1,128)}, u32[]{:S(2)}) copy-start(f32[1,3,32]{2,0,1:T(1,128)} %param.31) | copy-start | bytes 1156
  12.9 6.4 %copy-start = (f32[1,3,32,64,64]{4,3,2,1,0:T(8,128)S(1)}, f32[1,3,32,64,64]{4,3,2,1,0:T(8,128)}, u32[]{:S(2)}) copy-start(f32[1,3,32,64,64]{4,3,2,1,0:T(8,128)} %start.3) | copy-start | bytes 4718596
  12.9 6.4 %copy-start.7 = (bf16[1,6,2,1152]{3,2,1,0:T(2,128)(2,1)S(1)}, bf16[1,6,2,1152]{3,2,1,0:T(2,128)(2,1)}, u32[]{:S(2)}) copy-start(bf16[1,6,2,1152]{3,2,1,0:T(2,128)(2,1)} %history.5) | copy-start | bytes 82948
  12.9 6.4 %copy-start.8 = (bf16[4,2,1152]{2,1,0:T(2,128)(2,1)S(1)}, bf16[4,2,1152]{2,1,0:T(2,128)(2,1)}, u32[]{:S(2)}) copy-start(bf16[4,2,1152]{2,1,0:T(2,128)(2,1)} %taps.1) | copy-start | bytes 55300
  13.0 6.9 %copy-start.6 = (bf16[4096,32]{0,1:T(8,128)(2,1)S(1)}, bf16[4096,32]{0,1:T(8,128)(2,1)}, u32[]{:S(2)}) copy-start(bf16[4096,32]{0,1:T(8,128)(2,1)} %param.23) | copy-start | bytes 786436
  13.0 6.9 %copy-start.10 = (f32[32]{0:T(128)S(1)}, f32[32]{0:T(128)}, u32[]{:S(2)}) copy-start(f32[32]{0:T(128)} %param.24) | copy-start | bytes 388
  13.0 6.9 %copy-start.11 = (f32[32]{0:T(128)S(1)}, f32[32]{0:T(128)}, u32[]{:S(2)}) copy-start(f32[32]{0:T(128)} %param.25) | copy-start | bytes 388
  13.0 6.8 %copy-start.12 = (f32[32]{0:T(128)S(1)}, f32[32]{0:T(128)}, u32[]{:S(2)}) copy-start(f32[32]{0:T(128)} %param.26) | copy-start | bytes 388
  13.0 8.0 %copy-start.9 = (f32[2048]{0:T(1024)S(1)}, f32[2048]{0:T(1024)}, u32[]{:S(2)}) copy-start(f32[2048]{0:T(1024)} %param.32) | copy-start | bytes 24580
  14.3 6.3 %collective-permute-start.3 = (bf16[4,4352]{1,0:T(4,128)(2,1)S(1)}, bf16[4,4352]{1,0:T(4,128)(2,1)S(1)}, u32[]{:S(2)}, u32[]{:S(2)}) collective-permute-start(bf16[4,4352]{1,0:T(4,128)(2,1)S(1)} %get-tuple-element.33), channel_id=1, source_target_pairs={{0,4},{4,0},{8,12},{12,8},{1,5},{5,1},{9,13},{13,9},{2,6},{6,2},{1... | collective-permute-start | bytes 104456 | tf_op jit(solution)/shard_map/ppermute | solution.py:47
  14.3 6.3 %collective-permute-start.4 = (bf16[4,4352]{1,0:T(4,128)(2,1)S(1)}, bf16[4,4352]{1,0:T(4,128)(2,1)S(1)}, u32[]{:S(2)}, u32[]{:S(2)}) collective-permute-start(bf16[4,4352]{1,0:T(4,128)(2,1)S(1)} %get-tuple-element.34), channel_id=1, source_target_pairs={{0,8},{4,12},{8,0},{12,4},{1,9},{5,13},{9,1},{13,5},{2,10},{6,14},... | collective-permute-start | bytes 104456 | tf_op jit(solution)/shard_map/ppermute | solution.py:47
  14.9 6.1 %collective-permute-start.5 = (bf16[4,4352]{1,0:T(4,128)(2,1)S(1)}, bf16[4,4352]{1,0:T(4,128)(2,1)S(1)}, u32[]{:S(2)}, u32[]{:S(2)}) collective-permute-start(bf16[4,4352]{1,0:T(4,128)(2,1)S(1)} %get-tuple-element.35), channel_id=1, source_target_pairs={{0,12},{4,8},{8,4},{12,0},{1,13},{5,9},{9,5},{13,1},{2,14},{6,10},... | collective-permute-start | bytes 104456 | tf_op jit(solution)/shard_map/ppermute | solution.py:47
  19.4 10.1 %copy-start.1 = (bf16[2048,1024]{1,0:T(8,128)(2,1)S(1)}, bf16[2048,1024]{1,0:T(8,128)(2,1)}, u32[]{:S(2)}) copy-start(bf16[2048,1024]{1,0:T(8,128)(2,1)} %refs_4_.3) | copy-start | bytes 12582916
  21.4 6.6 %collective-permute-start.8 = (bf16[4,2048]{1,0:T(4,128)(2,1)S(1)}, bf16[4,2048]{1,0:T(4,128)(2,1)S(1)}, u32[]{:S(2)}, u32[]{:S(2)}) collective-permute-start(bf16[4,2048]{1,0:T(4,128)(2,1)S(1)} %get-tuple-element.42.refs_0_), channel_id=1, source_target_pairs={{0,12},{4,8},{8,4},{12,0},{1,13},{5,9},{9,5},{13,1},{2,14},{6,10},... | collective-permute-start | bytes 49160 | tf_op jit(solution)/shard_map/ppermute | solution.py:47
  24.9 4.6 %collective-permute-start.7 = (bf16[4,2048]{1,0:T(4,128)(2,1)S(1)}, bf16[4,2048]{1,0:T(4,128)(2,1)S(1)}, u32[]{:S(2)}, u32[]{:S(2)}) collective-permute-start(bf16[4,2048]{1,0:T(4,128)(2,1)S(1)} %get-tuple-element.42.refs_0_), channel_id=1, source_target_pairs={{0,8},{4,12},{8,0},{12,4},{1,9},{5,13},{9,1},{13,5},{2,10},{6,14},... | collective-permute-start | bytes 49160 | tf_op jit(solution)/shard_map/ppermute | solution.py:47
  24.9 4.6 %collective-permute-start.6 = (bf16[4,2048]{1,0:T(4,128)(2,1)S(1)}, bf16[4,2048]{1,0:T(4,128)(2,1)S(1)}, u32[]{:S(2)}, u32[]{:S(2)}) collective-permute-start(bf16[4,2048]{1,0:T(4,128)(2,1)S(1)} %get-tuple-element.42.refs_0_), channel_id=1, source_target_pairs={{0,4},{4,0},{8,12},{12,8},{1,5},{5,1},{9,13},{13,9},{2,6},{6,2},{1... | collective-permute-start | bytes 49160 | tf_op jit(solution)/shard_map/ppermute | solution.py:47
  30.2 3.5 %collective-permute-start.9 = (bf16[4,1024]{1,0:T(4,128)(2,1)S(1)}, bf16[4,1024]{1,0:T(4,128)(2,1)S(1)}, u32[]{:S(2)}, u32[]{:S(2)}) collective-permute-start(bf16[4,1024]{1,0:T(4,128)(2,1)S(1)} %get-tuple-element.48), channel_id=1, source_target_pairs={{0,1},{1,0},{2,3},{3,2},{4,5},{5,4},{6,7},{7,6},{8,9},{9,8},{10,11... | collective-permute-start | bytes 24584 | tf_op jit(solution)/shard_map/ppermute | solution.py:47
  30.3 3.7 %collective-permute-start.10 = (bf16[4,1024]{1,0:T(4,128)(2,1)S(1)}, bf16[4,1024]{1,0:T(4,128)(2,1)S(1)}, u32[]{:S(2)}, u32[]{:S(2)}) collective-permute-start(bf16[4,1024]{1,0:T(4,128)(2,1)S(1)} %get-tuple-element.49), channel_id=1, source_target_pairs={{0,2},{1,3},{2,0},{3,1},{4,6},{5,7},{6,4},{7,5},{8,10},{9,11},{10,... | collective-permute-start | bytes 24584 | tf_op jit(solution)/shard_map/ppermute | solution.py:47
  31.8 3.1 %collective-permute-start.11 = (bf16[4,1024]{1,0:T(4,128)(2,1)S(1)}, bf16[4,1024]{1,0:T(4,128)(2,1)S(1)}, u32[]{:S(2)}, u32[]{:S(2)}) collective-permute-start(bf16[4,1024]{1,0:T(4,128)(2,1)S(1)} %get-tuple-element.50), channel_id=1, source_target_pairs={{0,3},{1,2},{2,1},{3,0},{4,7},{5,6},{6,5},{7,4},{8,11},{9,10},{10,... | collective-permute-start | bytes 24584 | tf_op jit(solution)/shard_map/ppermute | solution.py:47

commit v3 on v2

--- a/solution.py
+++ b/solution.py
@@ -57,21 +57,31 @@
     return high, (v - high.astype(F32)).astype(BF16)
 
 
-def norm_body(count, tokens, scale, normed, *slices):
+def slice_body(count, tokens, *refs):
+    slices, sem = refs[:count], refs[-1]
     me = lax.axis_index("kv")
     width = slices[0].shape[1]
+    copies = []
+    for step in reversed(range(count)):
+        start = pl.multiple_of(lax.bitwise_xor(me, step) * width, 128)
+        copy = pltpu.make_async_copy(
+            tokens.at[0, :, pl.ds(start, width)], slices[step], sem.at[step]
+        )
+        copy.start()
+        copies.append(copy)
+    for copy in copies:
+        copy.wait()
+
+
+def step_body(head_dim, accepted, tokens, scale, step_t, bias, rate, direct, extra, coef, small, norm, table):
+    props, heads = extra.shape
     values = tokens[0].astype(F32)
-    mean = jnp.mean(values * values, axis=-1, keepdims=True)
-    normed[...] = (values * lax.rsqrt(mean + epsilon) * scale[...]).astype(BF16)
-    for step in range(count):
-        start = pl.multiple_of(lax.bitwise_xor(me, step) * width, 128)
-        slices[step][...] = normed[:, pl.ds(start, width)]
-
-
-def step_body(head_dim, accepted, normed, step_t, bias, rate, direct, extra, coef, small, table):
-    props, heads = extra.shape
+    norm_rows = lax.rsqrt(jnp.mean(values * values, axis=-1, keepdims=True) + epsilon)
+    norm[...] = jnp.ones_like(norm)
+    norm[0:props, :] = jnp.broadcast_to(norm_rows, (props, norm.shape[1]))
+    normed = (values * norm_rows * scale[...]).astype(BF16)
     raw = lax.dot_general(
-        normed[...], step_t[...], (((1,), (1,)), ((), ())), preferred_element_type=F32
+        normed, step_t[...], (((1,), (1,)), ((), ())), preferred_element_type=F32
     )
     size = jax.nn.softplus(raw + bias[...])
     decay = extra[...] - jnp.exp(rate[...]) * size
@@ -154,27 +164,47 @@
     return lhs[...].astype(BF16)
 
 
-def project_body(count, *refs):
+def packed_width(props, width):
+    return -(-props * width // 4 // 128) * 128
+
+
+def project_body(count, props, *refs):
     slices = refs[:count]
-    weights = refs[count : count + 4]
-    own = refs[count + 4]
-    outs = refs[count + 5 : count + 4 + count]
-    lhs = stack_rows(slices, refs[-1])
-    at = 0
-    for weight in weights:
-        width = weight.shape[1]
-        result = jnp.dot(lhs, weight[...], preferred_element_type=F32)
-        own[:, at : at + width] = result[0:4]
-        for j, out in enumerate(outs, 1):
-            out[:, at : at + width] = result[4 * j : 4 * j + 4].astype(BF16)
-        at += width
+    inputs, inject, readout, gates, scale = refs[count : count + 5]
+    own = refs[count + 5]
+    outs = refs[count + 6 : count + 5 + count]
+    stage, rows = refs[-2:]
+    depth = rows.shape[1]
+    start = pl.multiple_of(lax.axis_index("kv") * depth, 128)
+    stack_rows(slices, rows)
+    lhs = (rows[...] * scale[:, pl.ds(start, depth)]).astype(BF16)
+    wide = stage.shape[1]
+    first = inputs.shape[1]
+    both = inject.shape[1] + readout.shape[1]
+    left = wide - first - both
+    rest = gates.shape[1] - left
+
+    result = jnp.dot(lhs, gates[...], preferred_element_type=F32)
+    stage[:, first + both :] = result[:, :left]
+    extra = result[:, left:]
+    result = jnp.dot(lhs, inputs[...], preferred_element_type=F32)
+    stage[:, :first] = result
+    pair = jnp.concatenate([inject[...], readout[...]], axis=1)
+    stage[:, first : first + both] = jnp.dot(lhs, pair, preferred_element_type=F32)
+    for j in range(count):
+        for r in range(props):
+            at = 4 * j + r
+            stage[4 * j + 3 : 4 * j + 4, r * rest : (r + 1) * rest] = extra[at : at + 1]
+    own[...] = stage[0:4, :]
+    for j, out in enumerate(outs, 1):
+        out[...] = stage[4 * j : 4 * j + 4, :].astype(BF16)
 
 
 def mixer_body(props, groups, *refs):
     own, *rest = refs
-    count = len(rest) - 11
+    count = len(rest) - 12
     others = rest[:count]
-    coef, early, taps, high, low, gain, gated, fresh, act, summed, norms = rest[count:]
+    norm, coef, early, taps, high, low, gain, gated, fresh, act, summed, norms = rest[count:]
     inner = gain.shape[1]
     conv = early.shape[1]
     per = inner // groups
@@ -184,7 +214,12 @@
     total = own[...]
     for other in others:
         total = total + other[...].astype(F32)
-    summed[0:props, :] = total[0:props].astype(BF16).astype(F32)
+    wide = total.shape[1]
+    rest = summed.shape[1] - wide
+    summed[0:props, :wide] = total[0:props]
+    for r in range(props):
+        summed[r : r + 1, wide:] = total[3:4, r * rest : (r + 1) * rest]
+    summed[...] = (summed[...] * norm[:, 0:1]).astype(BF16).astype(F32)
     rows = summed[:, :conv]
     fresh[...] = rows
     tap_count = 4
@@ -227,75 +262,78 @@
     gated[...] = norms[0:4].astype(BF16)
 
 
-def states_body(props, g, accepted, start, small, act, coef, fresh, history, *refs):
-    if g == 0:
-        states, tail, flag, held, sem = refs
+def states_body(props, groups, pieces, accepted, start, small, act, coef, *refs):
+    heads, head_dim, size = start.shape[2:]
+    per = heads // groups
+    last = pieces[-1][2] == per and pieces[-1][0] == groups - 1
+    if last:
+        fresh, history, _, states, tail, held, sem = refs
+    else:
+        states, flag, held, sem = refs
         flag[...] = jnp.zeros_like(flag)
-    else:
-        _, states, held, sem = refs
-    heads, head_dim, size = start.shape[2:]
-    groups = history.shape[2]
-    per = heads // groups
+    copies = []
     inner = per * head_dim
     wide = heads * head_dim
+    block = groups * size
     count = accepted[0]
-    lanes = slice(g * inner, (g + 1) * inner)
     row_at = lax.broadcasted_iota(jnp.int32, (ROWS, 1), 0)
-    steps = jnp.zeros((ROWS, inner), F32)
+    b_high, b_low = split(act[:, wide : wide + block])
+    b_high, b_low = b_high.astype(F32), b_low.astype(F32)
+    filled = 0
+    for g, low, high in pieces:
+        lanes = slice(g * inner + low * head_dim, g * inner + high * head_dim)
+        steps = jnp.zeros((ROWS, (high - low) * head_dim), F32)
+        for j in range(props):
+            steps = jnp.where(row_at == j, coef[1 + j, :, lanes], steps)
+        dx = act[:, lanes] * steps
+        dx_high, dx_low = split(dx)
+        dx_high, dx_low = dx_high.astype(F32), dx_low.astype(F32)
+        left = jnp.concatenate(
+            [dx_high, dx_low, dx_high, jnp.zeros_like(dx)], axis=0
+        ).astype(BF16)
+        blocks = []
+        for j in range(props):
+            hi = jnp.where(row_at == j, b_high, 0.0)
+            lo = jnp.where(row_at == j, b_low, 0.0)
+            full = jnp.concatenate([hi, hi, lo, jnp.zeros_like(hi)], axis=0)
+            if g:
+                full = pltpu.roll(full, block - g * size, 1)
+            blocks.append(full)
+        right = jnp.concatenate(blocks, axis=1).astype(BF16)
+        update = lax.dot_general(
+            left, right, (((0,), (0,)), ((), ())), preferred_element_type=F32
+        )
+        for h in range(high - low):
+            at = g * per + low + h
+            state = start[0, count - 1, at]
+            for j in range(props):
+                new = update[h * head_dim : (h + 1) * head_dim, j * block : j * block + size]
+                state = state * small[j : j + 1, at : at + 1] + new
+                held[j, filled + h] = state
+        copy = pltpu.make_async_copy(
+            held.at[:, pl.ds(filled, high - low)],
+            states.at[0, :, pl.ds(g * per + low, high - low)],
+            sem.at[len(copies)],
+        )
+        copy.start()
+        copies.append(copy)
+        filled += high - low
+    if not last:
+        for copy in copies:
+            copy.wait()
+        return
+    before = tail.shape[1] - props
+    for k in range(before):
+        tail[0, k] = history[0, count + k]
     for j in range(props):
-        steps = jnp.where(row_at == j, coef[1 + j, :, lanes], steps)
-    dx = act[:, lanes] * steps
-    dx_high, dx_low = split(dx)
-    dx_high, dx_low = dx_high.astype(F32), dx_low.astype(F32)
-    left = jnp.concatenate(
-        [dx_high, dx_low, dx_high, jnp.zeros_like(dx)], axis=0
-    ).astype(BF16)
-    b_high, b_low = split(act[:, wide : wide + groups * size])
-    b_high, b_low = b_high.astype(F32), b_low.astype(F32)
-    blocks = []
-    for j in range(props):
-        hi = jnp.where(row_at == j, b_high, 0.0)
-        lo = jnp.where(row_at == j, b_low, 0.0)
-        full = jnp.concatenate([hi, hi, lo, jnp.zeros_like(hi)], axis=0)
-        if g:
-            full = pltpu.roll(full, groups * size - g * size, 1)
-        blocks.append(full)
-    right = jnp.concatenate(blocks, axis=1).astype(BF16)
-    update = lax.dot_general(
-        left, right, (((0,), (0,)), ((), ())), preferred_element_type=F32
-    )
-    block = groups * size
-    copies = []
-    half = per // 2
-    for h in range(per):
-        at = g * per + h
-        state = start[0, count - 1, at]
-        for j in range(props):
-            new = update[h * head_dim : (h + 1) * head_dim, j * block : j * block + size]
-            state = state * small[j : j + 1, at : at + 1] + new
-            held[j, h] = state
-        if (h + 1) % half == 0:
-            first = h + 1 - half
-            copy = pltpu.make_async_copy(
-                held.at[:, pl.ds(first, half)],
-                states.at[0, :, pl.ds(g * per + first, half)],
-                sem.at[len(copies)],
-            )
-            copy.start()
-            copies.append(copy)
-    if g == 0:
-        before = tail.shape[1] - props
-        for k in range(before):
-            tail[0, k] = history[0, count + k]
-        for j in range(props):
-            rows = []
-            for q in range(groups):
-                row = [fresh[j : j + 1, q * inner : (q + 1) * inner]]
-                for part in range(2):
-                    base = wide + part * groups * size + q * size
-                    row.append(fresh[j : j + 1, base : base + size])
-                rows.append(jnp.concatenate(row, axis=1))
-            tail[0, before + j] = jnp.concatenate(rows, axis=0).astype(BF16)
+        rows = []
+        for q in range(groups):
+            row = [fresh[j : j + 1, q * inner : (q + 1) * inner]]
+            for part in range(2):
+                base = wide + part * block + q * size
+                row.append(fresh[j : j + 1, base : base + size])
+            rows.append(jnp.concatenate(row, axis=1))
+        tail[0, before + j] = jnp.concatenate(rows, axis=0).astype(BF16)
     for copy in copies:
         copy.wait()
 
@@ -349,31 +387,40 @@
     conv = groups * channels
     rows = head_input_matrix.shape[0]
     total = conv + inner
+    packed = packed_width(props, total)
     out_cols = output_projection_matrix.shape[1]
 
-    normed, *slices = call(
-        functools.partial(norm_body, count),
-        [pltpu.VMEM((props, width), BF16)] + [pltpu.VMEM((props, rows), BF16)] * count,
-        [hbm(tokens), hbm(input_norm_scale.reshape(1, width))],
-        [VMEM_SPEC] * 2,
-        flops=1_000_000_000_000, moved=10_000_000_000,
+    slices = call(
+        functools.partial(slice_body, count),
+        [pltpu.VMEM((props, rows), BF16)] * count,
+        [hbm(tokens)],
+        [HBM_SPEC],
+        flops=1_000_000_000_000,
+        moved=10_000_000_000,
+        scratch=[pltpu.SemaphoreType.DMA((count,))],
     )
     received = exchange(slices, "kv", count)
     matrices = [head_input_matrix, group_input_matrix, group_readout_matrix, output_gate_matrix]
 
-    coef, small = call(
+    scale = input_norm_scale.reshape(1, width)
+    coef, small, norm = call(
         functools.partial(step_body, head_dim),
-        [pltpu.VMEM((props + 2, ROWS, inner), F32), pltpu.VMEM((ROWS, heads), F32)],
+        [
+            pltpu.VMEM((props + 2, ROWS, inner), F32),
+            pltpu.VMEM((ROWS, heads), F32),
+            pltpu.VMEM((ROWS, 128), F32),
+        ],
         [
             accepted,
-            vmem(normed),
+            vmem(tokens),
+            vmem(scale),
             vmem(step_size_matrix.T),
             step_size_bias.reshape(1, heads),
             log_decay_rate.reshape(1, heads),
             direct_path_weight.reshape(1, heads),
             proposal_extra_decay.reshape(props, heads),
         ],
-        [SMEM_SPEC] + [VMEM_SPEC] * 6,
+        [SMEM_SPEC] + [VMEM_SPEC] * 7,
         flops=20_000_000,
         scratch=[pltpu.VMEM(((props + 2) * ROWS, heads), F32)],
     )
@@ -392,13 +439,14 @@
     )
 
     own, *partials = call(
-        functools.partial(project_body, count),
-        [pltpu.VMEM((4, total), F32)] + [pltpu.VMEM((4, total), BF16)] * (count - 1),
+        functools.partial(project_body, count, props),
+        [pltpu.VMEM((4, packed), F32)] + [pltpu.VMEM((4, packed), BF16)] * (count - 1),
         [vmem(s) for s in [slices[0]] + received]
-        + matrices,
-        [VMEM_SPEC] * (count + 4),
+        + matrices
+        + [vmem(scale)],
+        [VMEM_SPEC] * (count + 5),
         flops=200_000_000,
-        scratch=[pltpu.VMEM((4 * count, rows), F32)],
+        scratch=[pltpu.VMEM((4 * count, packed), F32), pltpu.VMEM((4 * count, rows), F32)],
     )
     sums = exchange([None] + partials, "kv", count)
     gated, fresh, act = call(
@@ -408,40 +456,44 @@
             pltpu.VMEM((ROWS, conv), F32),
             pltpu.VMEM((ROWS, conv), F32),
         ],
-        [vmem(v) for v in [own] + sums + [coef, early, taps, high, low]]
+        [vmem(v) for v in [own] + sums + [norm, coef, early, taps, high, low]]
         + [vmem(group_norm_scale.reshape(1, inner))],
-        [VMEM_SPEC] * (count + 6),
+        [VMEM_SPEC] * (count + 7),
         flops=20_000_000,
         scratch=[pltpu.VMEM((ROWS, total), F32), pltpu.VMEM((ROWS, inner), F32)],
     )
     gathered = exchange([gated] * count, "kv", count)
-    new_states = None
-    for g in range(groups):
-        shape = jax.ShapeDtypeStruct((1, props, heads, head_dim, size), F32)
-        outs = [shape]
-        if g == 0:
-            outs += [
-                jax.ShapeDtypeStruct(convolution_history_rows.shape, BF16),
-                pltpu.VMEM((ROWS, 128), F32),
-            ]
-        result = call(
-            functools.partial(states_body, props, g),
-            outs,
-            [accepted, states]
-            + [vmem(v) for v in (small, act, coef, fresh, convolution_history_rows)]
-            + ([hbm(new_states)] if g else []),
-            [SMEM_SPEC] + [VMEM_SPEC] * 6 + ([HBM_SPEC] if g else []),
-            flops=30_000_000,
-            out_specs=[HBM_SPEC] + [VMEM_SPEC] * (len(outs) - 1),
-            scratch=[
-                pltpu.VMEM((props, heads // groups, head_dim, size), F32),
-                pltpu.SemaphoreType.DMA((2,)),
-            ],
-            aliases={7: 0} if g else {},
-        )
-        new_states = result[0]
-        if g == 0:
-            new_tail, flag = result[1:]
+    per = heads // groups
+    half = per // 2
+    pieces = [(g, at, at + half) for g in range(groups) for at in (0, half)]
+    first = 3 * len(pieces) // 4
+    all_states = jax.ShapeDtypeStruct((1, props, heads, head_dim, size), F32)
+
+    def scratch(number):
+        shape = (props, number * half, head_dim, size)
+        return [pltpu.VMEM(shape, F32), pltpu.SemaphoreType.DMA((number,))]
+
+    new_states, flag = call(
+        functools.partial(states_body, props, groups, pieces[:first]),
+        [all_states, pltpu.VMEM((ROWS, 128), F32)],
+        [accepted, states] + [vmem(v) for v in (small, act, coef)],
+        [SMEM_SPEC] + [VMEM_SPEC] * 4,
+        flops=30_000_000,
+        out_specs=[HBM_SPEC, VMEM_SPEC],
+        scratch=scratch(first),
+    )
+    new_states, new_tail = call(
+        functools.partial(states_body, props, groups, pieces[first:]),
+        [all_states, jax.ShapeDtypeStruct(convolution_history_rows.shape, BF16)],
+        [accepted, states]
+        + [vmem(v) for v in (small, act, coef, fresh, convolution_history_rows)]
+        + [hbm(new_states)],
+        [SMEM_SPEC] + [VMEM_SPEC] * 6 + [HBM_SPEC],
+        flops=30_000_000,
+        out_specs=[HBM_SPEC, VMEM_SPEC],
+        scratch=scratch(len(pieces) - first),
+        aliases={7: 0},
+    )
     blocks = call(
         functools.partial(output_body, count),
         [pltpu.VMEM((4, out_cols), BF16)] * count,
@@ -618,6 +670,7 @@
     tokens, matrix = arguments[0], arguments[2]
     kv, tp = mesh.shape["kv"], mesh.shape["tp"]
     slim = tokens.shape[:2] == (1, 3) and matrix.shape[0] % 128 == 0
+    slim = slim and arguments[10].shape[1] == 2
     if slim and kv == tp and kv in (2, 4):
         return fast_local(kv, *arguments)
     return local(*arguments)

time: 35.7 us -> 35.7 us (level)
  transfers between devices with their start and end apart: 12 -> 12, of which waited for: 6 -> 5; matrix products, arithmetic and copies ran while one was open for 0% -> 0% of each run, Pallas kernels for 14% -> 14%
where the time goes in v3:
time: 35.7 us; the launch traced here: 35.5 us
  starting transfers between devices  16.5 us (46%)
  Pallas kernels  8.82 us (25%)
  waiting for transfers between devices  8.45 us (24%)
  between operations  1.62 us (5%)
    ppermute x12, starting transfers between devices, exchange(): got.append(lax.ppermute(blocks[step], axis, pairs))  16.5 us
    pallas_call x9, Pallas kernels, call(): pl.pallas_call(body, out_shape=outs, in_specs=specs, out_specs=out_specs...  8.82 us
    ppermute x12, waiting for transfers between devices, exchange(): got.append(lax.ppermute(blocks[step], axis, pairs))  8.45 us
  transfers between devices with their start and end apart: 12, of which 5 were waited for; matrix products, arithmetic and copies ran while one was open for 0% of the time, Pallas kernels for 14%

profile of v3, /device:TPU:0, one launch (start us, length us, event | category | flops | bytes accessed | tf_op | source)
XLA Modules:
  0.0 35.5 jit_solution(10066453575004430125)
XLA Ops:
  0.6 0.0 copy-start.2
  0.6 0.0 copy-start.3
  0.7 0.0 copy-start.4
  0.7 0.0 copy-start.5
  0.7 0.0 copy-start.8
  0.7 0.9 %shard_map.184 = (bf16[3,1024]{1,0:T(4,128)(2,1)S(1)}, bf16[3,1024]{1,0:T(4,128)(2,1)S(1)}, bf16[3,1024]{1,0:T(4,128)(2,1)S(1)}, bf16[3,1024]{1,0:T(4,128)(2,1)S(1)}) custom-call(bf16[1,3,4096]{2,1,0:T(4,128)(2,1)} %tokens.3), custom_call_target="tpu_custom_call" | custom-call | flops 999999995904 | bytes 10000000000 | tf_op jit(solution)/shard_map/pallas_call | solution.py:31
  1.6 3.1 %collective-permute-start = (bf16[3,1024]{1,0:T(4,128)(2,1)S(1)}, bf16[3,1024]{1,0:T(4,128)(2,1)S(1)}, u32[]{:S(2)}, u32[]{:S(2)}) collective-permute-start(bf16[3,1024]{1,0:T(4,128)(2,1)S(1)} %get-tuple-element.30), channel_id=1, source_target_pairs={{0,4},{4,0},{8,12},{12,8},{1,5},{5,1},{9,13},{13,9},{2,6},{6,2},{1... | collective-permute-start | bytes 18440 | tf_op jit(solution)/shard_map/ppermute | solution.py:47
  4.8 2.6 %collective-permute-start.1 = (bf16[3,1024]{1,0:T(4,128)(2,1)S(1)}, bf16[3,1024]{1,0:T(4,128)(2,1)S(1)}, u32[]{:S(2)}, u32[]{:S(2)}) collective-permute-start(bf16[3,1024]{1,0:T(4,128)(2,1)S(1)} %get-tuple-element.31), channel_id=1, source_target_pairs={{0,8},{4,12},{8,0},{12,4},{1,9},{5,13},{9,1},{13,5},{2,10},{6,14},... | collective-permute-start | bytes 18440 | tf_op jit(solution)/shard_map/ppermute | solution.py:47
  7.3 0.0 collective-permute-start.2
  7.3 0.0 collective-permute-done.refs_1_
  7.3 2.0 %collective-permute-done.1.refs_2_ = bf16[3,1024]{1,0:T(4,128)(2,1)S(1)} collective-permute-done((bf16[3,1024]{1,0:T(4,128)(2,1)S(1)}, bf16[3,1024]{1,0:T(4,128)(2,1)S(1)}, u32[]{:S(2)}, u32[]{:S(2)}) %collective-permute-start.1) | collective-permute-done | bytes 6176 | tf_op jit(solution)/shard_map/ppermute | solution.py:47
  9.3 3.5 %collective-permute-done.2.refs_3_ = bf16[3,1024]{1,0:T(4,128)(2,1)S(1)} collective-permute-done((bf16[3,1024]{1,0:T(4,128)(2,1)S(1)}, bf16[3,1024]{1,0:T(4,128)(2,1)S(1)}, u32[]{:S(2)}, u32[]{:S(2)}) %collective-permute-start.2) | collective-permute-done | bytes 6176 | tf_op jit(solution)/shard_map/ppermute | solution.py:47
  12.8 0.0 copy-done.2
  12.8 0.0 copy-done.3
  12.8 0.0 copy-done.4
  12.8 0.0 copy-done.5
  12.8 0.0 copy-done.8
  12.8 0.0 copy-start.15
  12.8 0.0 copy-start
  12.8 0.0 copy-start.7
  12.9 0.0 copy-start.10
  12.9 0.0 copy-start.6
  12.9 0.0 copy-start.9
  12.9 0.0 copy-start.12
  12.9 0.0 copy-start.13
  12.9 0.0 copy-start.14
  12.9 0.0 copy-start.11
  12.9 1.3 %shard_map.185 = (f32[4,3328]{1,0:T(4,128)S(1)}, bf16[4,3328]{1,0:T(4,128)(2,1)S(1)}, bf16[4,3328]{1,0:T(4,128)(2,1)S(1)}, bf16[4,3328]{1,0:T(4,128)(2,1)S(1)}) custom-call(bf16[3,1024]{1,0:T(4,128)(2,1)S(1)} %get-tuple-element.29.refs_0_, bf16[3,1024]{1,0:T(4,128)(2,1)S(1)} %collective-permute-done.refs_1_, ...), custom_call_target="tpu_custom_call" | custom-call | flops 200000000 | tf_op jit(solution)/shard_map/pallas_call | solution.py:31
  14.3 0.1 collective-permute-start.3
  14.3 0.6 %collective-permute-start.4 = (bf16[4,3328]{1,0:T(4,128)(2,1)S(1)}, bf16[4,3328]{1,0:T(4,128)(2,1)S(1)}, u32[]{:S(2)}, u32[]{:S(2)}) collective-permute-start(bf16[4,3328]{1,0:T(4,128)(2,1)S(1)} %get-tuple-element.35), channel_id=1, source_target_pairs={{0,8},{4,12},{8,0},{12,4},{1,9},{5,13},{9,1},{13,5},{2,10},{6,14},... | collective-permute-start | bytes 79880 | tf_op jit(solution)/shard_map/ppermute | solution.py:47
  15.0 3.7 %collective-permute-start.5 = (bf16[4,3328]{1,0:T(4,128)(2,1)S(1)}, bf16[4,3328]{1,0:T(4,128)(2,1)S(1)}, u32[]{:S(2)}, u32[]{:S(2)}) collective-permute-start(bf16[4,3328]{1,0:T(4,128)(2,1)S(1)} %get-tuple-element.36), channel_id=1, source_target_pairs={{0,12},{4,8},{8,4},{12,0},{1,13},{5,9},{9,5},{13,1},{2,14},{6,10},... | collective-permute-start | bytes 79880 | tf_op jit(solution)/shard_map/ppermute | solution.py:47
  19.4 0.0 copy-done.15
  19.4 0.0 copy-done
  19.4 0.0 copy-done.7
  19.4 0.0 copy-done.10
  19.4 0.0 copy-start.1
  19.4 0.4 %shard_map.187 = (bf16[128,2048]{1,0:T(8,128)(2,1)S(1)}, bf16[128,2048]{1,0:T(8,128)(2,1)S(1)}, f32[8,2304]{1,0:T(8,128)S(1)}, f32[8,2304]{1,0:T(8,128)S(1)}) custom-call(s32[1]{0:T(128)S(6)} %copy.25.accepted, f32[1,3,32,64,64]{4,3,2,1,0:T(8,128)S(1)} %copy-done, bf16[1,6,2,1152]{3,2,1,0:T(2,128)(2,1)S(1)} %copy-done.7, bf16[4,2,1152]{2,1,0:T(2,128)(2,1)S(1)} %copy-done.10), custom_call_target="tpu_custom_call" | custom-call | flops 20000000 | tf_op jit(solution)/shard_map/pallas_call | solution.py:31
  19.8 0.0 copy-done.6
  19.8 0.0 copy-done.9
  19.8 0.0 copy-done.12
  19.9 0.0 copy-done.13
  19.9 0.0 copy-done.14
  19.9 0.9 %shard_map.186 = (f32[5,8,2048]{2,1,0:T(8,128)S(1)}, f32[8,32]{1,0:T(8,128)S(1)}, f32[8,128]{1,0:T(8,128)S(1)}) custom-call(s32[1]{0:T(128)S(6)} %copy.25.accepted, bf16[1,3,4096]{2,1,0:T(4,128)(2,1)S(1)} %copy-done.9, f32[1,4096]{1,0:T(1,128)S(1)} %bitcast.11, bf16[32,4096]{1,0:T(8,128)(2,1)S(1)} %bitcast.9, f32[1,32]{1,0:T(1,128)S(1)} %bitcast.14, ...), custom_call_target="tpu_custom_call" | custom-call | flops 20000000 | tf_op jit(solution)/shard_map/pallas_call | solution.py:31
  20.7 0.0 collective-permute-done.3.refs_1_
  20.8 0.0 collective-permute-done.4.refs_2_
  20.8 0.1 collective-permute-done.5.refs_3_
  20.9 0.0 copy-done.11
  20.9 0.4 %shard_map.188 = (bf16[4,2048]{1,0:T(4,128)(2,1)S(1)}, f32[8,2304]{1,0:T(8,128)S(1)}, f32[8,2304]{1,0:T(8,128)S(1)}) custom-call(f32[4,3328]{1,0:T(4,128)S(1)} %get-tuple-element.33.refs_0_, bf16[4,3328]{1,0:T(4,128)(2,1)S(1)} %collective-permute-done.3.refs_1_, bf16[4,3328]{1,0:T(4,128)(2,1)S(1)} %collective-permute-done.4.refs_2_, ...), custom_call_target="tpu_custom_call" | custom-call | flops 20000000 | tf_op jit(solution)/shard_map/pallas_call | solution.py:31
  21.3 3.6 %collective-permute-start.8 = (bf16[4,2048]{1,0:T(4,128)(2,1)S(1)}, bf16[4,2048]{1,0:T(4,128)(2,1)S(1)}, u32[]{:S(2)}, u32[]{:S(2)}) collective-permute-start(bf16[4,2048]{1,0:T(4,128)(2,1)S(1)} %get-tuple-element.43.refs_0_), channel_id=1, source_target_pairs={{0,12},{4,8},{8,4},{12,0},{1,13},{5,9},{9,5},{13,1},{2,14},{6,10},... | collective-permute-start | bytes 49160 | tf_op jit(solution)/shard_map/ppermute | solution.py:47
  24.8 0.0 collective-permute-start.7
  24.8 0.9 %collective-permute-start.6 = (bf16[4,2048]{1,0:T(4,128)(2,1)S(1)}, bf16[4,2048]{1,0:T(4,128)(2,1)S(1)}, u32[]{:S(2)}, u32[]{:S(2)}) collective-permute-start(bf16[4,2048]{1,0:T(4,128)(2,1)S(1)} %get-tuple-element.43.refs_0_), channel_id=1, source_target_pairs={{0,4},{4,0},{8,12},{12,8},{1,5},{5,1},{9,13},{13,9},{2,6},{6,2},{1... | collective-permute-start | bytes 49160 | tf_op jit(solution)/shard_map/ppermute | solution.py:47
  25.7 1.8 %shard_map.189 = (f32[1,3,32,64,64]{4,3,2,1,0:T(8,128)}, f32[8,128]{1,0:T(8,128)S(1)}) custom-call(s32[1]{0:T(128)S(6)} %copy.25.accepted, f32[1,3,32,64,64]{4,3,2,1,0:T(8,128)S(1)} %copy-done, f32[8,32]{1,0:T(8,128)S(1)} %get-tuple-element.44.small, f32[8,2304]{1,0:T(8,128)S(1)} %get-tuple-element.45.act, f32[5,8,2048]{2,1,0:T(8,128)S(1)} %get-tuple-element.38.refs_5_.coef), custom_call_target="tpu_custom_call" | custom-call | flops 30000000 | tf_op jit(solution)/shard_map/pallas_call | solution.py:31
  27.5 0.0 collective-permute-done.8.refs_3_
  27.5 2.0 %collective-permute-done.7.refs_2_ = bf16[4,2048]{1,0:T(4,128)(2,1)S(1)} collective-permute-done((bf16[4,2048]{1,0:T(4,128)(2,1)S(1)}, bf16[4,2048]{1,0:T(4,128)(2,1)S(1)}, u32[]{:S(2)}, u32[]{:S(2)}) %collective-permute-start.7) | collective-permute-done | bytes 16416 | tf_op jit(solution)/shard_map/ppermute | solution.py:47
  29.5 0.0 collective-permute-done.6.refs_1_
  29.5 0.7 %shard_map.190 = (bf16[4,1024]{1,0:T(4,128)(2,1)S(1)}, bf16[4,1024]{1,0:T(4,128)(2,1)S(1)}, bf16[4,1024]{1,0:T(4,128)(2,1)S(1)}, bf16[4,1024]{1,0:T(4,128)(2,1)S(1)}) custom-call(bf16[4,2048]{1,0:T(4,128)(2,1)S(1)} %get-tuple-element.43.refs_0_, bf16[4,2048]{1,0:T(4,128)(2,1)S(1)} %collective-permute-done.6.refs_1_, ...), custom_call_target="tpu_custom_call" | custom-call | flops 100000000 | tf_op jit(solution)/shard_map/pallas_call | solution.py:31
  30.2 0.1 collective-permute-start.9
  30.2 1.6 %collective-permute-start.10 = (bf16[4,1024]{1,0:T(4,128)(2,1)S(1)}, bf16[4,1024]{1,0:T(4,128)(2,1)S(1)}, u32[]{:S(2)}, u32[]{:S(2)}) collective-permute-start(bf16[4,1024]{1,0:T(4,128)(2,1)S(1)} %get-tuple-element.49), channel_id=1, source_target_pairs={{0,2},{1,3},{2,0},{3,1},{4,6},{5,7},{6,4},{7,5},{8,10},{9,11},{10,... | collective-permute-start | bytes 24584 | tf_op jit(solution)/shard_map/ppermute | solution.py:47
  31.8 0.3 collective-permute-start.11
  32.1 1.8 %shard_map.192 = (f32[1,3,32,64,64]{4,3,2,1,0:T(8,128)}, bf16[1,6,2,1152]{3,2,1,0:T(2,128)(2,1)}) custom-call(s32[1]{0:T(128)S(6)} %copy.25.accepted, f32[1,3,32,64,64]{4,3,2,1,0:T(8,128)S(1)} %copy-done, f32[8,32]{1,0:T(8,128)S(1)} %get-tuple-element.44.small, f32[8,2304]{1,0:T(8,128)S(1)} %get-tuple-element.45.act, ...), custom_call_target="tpu_custom_call", output_to_operand_aliasing={{0}: (7, {})} | custom-call | flops 30000000 | tf_op jit(solution)/shard_map/pallas_call | solution.py:31
  33.9 0.0 collective-permute-done.9.refs_1_
  33.9 0.0 collective-permute-done.10.refs_2_
  34.0 0.9 %collective-permute-done.11.refs_3_ = bf16[4,1024]{1,0:T(4,128)(2,1)S(1)} collective-permute-done((bf16[4,1024]{1,0:T(4,128)(2,1)S(1)}, bf16[4,1024]{1,0:T(4,128)(2,1)S(1)}, u32[]{:S(2)}, u32[]{:S(2)}) %collective-permute-start.11) | collective-permute-done | bytes 8224 | tf_op jit(solution)/shard_map/ppermute | solution.py:47
  34.9 0.6 %shard_map.191 = bf16[1,3,1024]{2,1,0:T(4,128)(2,1)} custom-call(bf16[4,1024]{1,0:T(4,128)(2,1)S(1)} %get-tuple-element.47.refs_0_, bf16[4,1024]{1,0:T(4,128)(2,1)S(1)} %collective-permute-done.9.refs_1_, bf16[4,1024]{1,0:T(4,128)(2,1)S(1)} %collective-permute-done.10.refs_2_, bf16[4,1024]{1,0:T(4,128)(2,1)S(1)} %collective-permute-done.11.refs_3_), custom_call_target="tpu_custom_call" | custom-call | tf_op jit(solution)/shard_map/pallas_call | solution.py:31
  (2 shorter events, 0.0 us)
Async XLA Ops:
  0.6 12.2 %copy-start.2 = (bf16[1024,2048]{1,0:T(8,128)(2,1)S(1)}, bf16[1024,2048]{1,0:T(8,128)(2,1)}, u32[]{:S(2)}) copy-start(bf16[1024,2048]{1,0:T(8,128)(2,1)} %refs_4_.2) | copy-start | bytes 12582916
  0.6 12.2 %copy-start.3 = (bf16[1024,2048]{1,0:T(8,128)(2,1)S(1)}, bf16[1024,2048]{1,0:T(8,128)(2,1)}, u32[]{:S(2)}) copy-start(bf16[1024,2048]{1,0:T(8,128)(2,1)} %refs_7_.1) | copy-start | bytes 12582916
  0.7 12.1 %copy-start.4 = (bf16[1024,128]{1,0:T(8,128)(2,1)S(1)}, bf16[1024,128]{1,0:T(8,128)(2,1)}, u32[]{:S(2)}) copy-start(bf16[1024,128]{1,0:T(8,128)(2,1)} %refs_5_.1) | copy-start | bytes 786436
  0.7 12.1 %copy-start.5 = (bf16[1024,128]{1,0:T(8,128)(2,1)S(1)}, bf16[1024,128]{1,0:T(8,128)(2,1)}, u32[]{:S(2)}) copy-start(bf16[1024,128]{1,0:T(8,128)(2,1)} %refs_6_.1) | copy-start | bytes 786436
  0.7 12.1 %copy-start.8 = (f32[4096]{0:T(1024)S(1)}, f32[4096]{0:T(1024)}, u32[]{:S(2)}) copy-start(f32[4096]{0:T(1024)} %param.18) | copy-start | bytes 49156
  1.6 5.7 %collective-permute-start = (bf16[3,1024]{1,0:T(4,128)(2,1)S(1)}, bf16[3,1024]{1,0:T(4,128)(2,1)S(1)}, u32[]{:S(2)}, u32[]{:S(2)}) collective-permute-start(bf16[3,1024]{1,0:T(4,128)(2,1)S(1)} %get-tuple-element.30), channel_id=1, source_target_pairs={{0,4},{4,0},{8,12},{12,8},{1,5},{5,1},{9,13},{13,9},{2,6},{6,2},{1... | collective-permute-start | bytes 18440 | tf_op jit(solution)/shard_map/ppermute | solution.py:47
  4.8 4.5 %collective-permute-start.1 = (bf16[3,1024]{1,0:T(4,128)(2,1)S(1)}, bf16[3,1024]{1,0:T(4,128)(2,1)S(1)}, u32[]{:S(2)}, u32[]{:S(2)}) collective-permute-start(bf16[3,1024]{1,0:T(4,128)(2,1)S(1)} %get-tuple-element.31), channel_id=1, source_target_pairs={{0,8},{4,12},{8,0},{12,4},{1,9},{5,13},{9,1},{13,5},{2,10},{6,14},... | collective-permute-start | bytes 18440 | tf_op jit(solution)/shard_map/ppermute | solution.py:47
  7.3 5.4 %collective-permute-start.2 = (bf16[3,1024]{1,0:T(4,128)(2,1)S(1)}, bf16[3,1024]{1,0:T(4,128)(2,1)S(1)}, u32[]{:S(2)}, u32[]{:S(2)}) collective-permute-start(bf16[3,1024]{1,0:T(4,128)(2,1)S(1)} %get-tuple-element.32), channel_id=1, source_target_pairs={{0,12},{4,8},{8,4},{12,0},{1,13},{5,9},{9,5},{13,1},{2,14},{6,10},... | collective-permute-start | bytes 18440 | tf_op jit(solution)/shard_map/ppermute | solution.py:47
  12.8 6.5 %copy-start.15 = (f32[1,3,32]{2,0,1:T(1,128)S(1)}, f32[1,3,32]{2,0,1:T(1,128)}, u32[]{:S(2)}) copy-start(f32[1,3,32]{2,0,1:T(1,128)} %param.31) | copy-start | bytes 1156
  12.8 6.5 %copy-start = (f32[1,3,32,64,64]{4,3,2,1,0:T(8,128)S(1)}, f32[1,3,32,64,64]{4,3,2,1,0:T(8,128)}, u32[]{:S(2)}) copy-start(f32[1,3,32,64,64]{4,3,2,1,0:T(8,128)} %start.3) | copy-start | bytes 4718596
  12.8 6.5 %copy-start.7 = (bf16[1,6,2,1152]{3,2,1,0:T(2,128)(2,1)S(1)}, bf16[1,6,2,1152]{3,2,1,0:T(2,128)(2,1)}, u32[]{:S(2)}) copy-start(bf16[1,6,2,1152]{3,2,1,0:T(2,128)(2,1)} %refs_1_.1) | copy-start | bytes 82948
  12.9 6.5 %copy-start.10 = (bf16[4,2,1152]{2,1,0:T(2,128)(2,1)S(1)}, bf16[4,2,1152]{2,1,0:T(2,128)(2,1)}, u32[]{:S(2)}) copy-start(bf16[4,2,1152]{2,1,0:T(2,128)(2,1)} %taps.1) | copy-start | bytes 55300
  12.9 7.0 %copy-start.6 = (bf16[4096,32]{0,1:T(8,128)(2,1)S(1)}, bf16[4096,32]{0,1:T(8,128)(2,1)}, u32[]{:S(2)}) copy-start(bf16[4096,32]{0,1:T(8,128)(2,1)} %param.23) | copy-start | bytes 786436
  12.9 7.0 %copy-start.9 = (bf16[1,3,4096]{2,1,0:T(4,128)(2,1)S(1)}, bf16[1,3,4096]{2,1,0:T(4,128)(2,1)}, u32[]{:S(2)}) copy-start(bf16[1,3,4096]{2,1,0:T(4,128)(2,1)} %tokens.3) | copy-start | bytes 73732
  12.9 7.0 %copy-start.12 = (f32[32]{0:T(128)S(1)}, f32[32]{0:T(128)}, u32[]{:S(2)}) copy-start(f32[32]{0:T(128)} %param.24) | copy-start | bytes 388
  12.9 7.0 %copy-start.13 = (f32[32]{0:T(128)S(1)}, f32[32]{0:T(128)}, u32[]{:S(2)}) copy-start(f32[32]{0:T(128)} %param.25) | copy-start | bytes 388
  12.9 7.0 %copy-start.14 = (f32[32]{0:T(128)S(1)}, f32[32]{0:T(128)}, u32[]{:S(2)}) copy-start(f32[32]{0:T(128)} %param.26) | copy-start | bytes 388
  12.9 7.9 %copy-start.11 = (f32[2048]{0:T(1024)S(1)}, f32[2048]{0:T(1024)}, u32[]{:S(2)}) copy-start(f32[2048]{0:T(1024)} %param.32) | copy-start | bytes 24580
  14.3 6.5 %collective-permute-start.3 = (bf16[4,3328]{1,0:T(4,128)(2,1)S(1)}, bf16[4,3328]{1,0:T(4,128)(2,1)S(1)}, u32[]{:S(2)}, u32[]{:S(2)}) collective-permute-start(bf16[4,3328]{1,0:T(4,128)(2,1)S(1)} %get-tuple-element.34), channel_id=1, source_target_pairs={{0,4},{4,0},{8,12},{12,8},{1,5},{5,1},{9,13},{13,9},{2,6},{6,2},{1... | collective-permute-start | bytes 79880 | tf_op jit(solution)/shard_map/ppermute | solution.py:47
  14.3 6.4 %collective-permute-start.4 = (bf16[4,3328]{1,0:T(4,128)(2,1)S(1)}, bf16[4,3328]{1,0:T(4,128)(2,1)S(1)}, u32[]{:S(2)}, u32[]{:S(2)}) collective-permute-start(bf16[4,3328]{1,0:T(4,128)(2,1)S(1)} %get-tuple-element.35), channel_id=1, source_target_pairs={{0,8},{4,12},{8,0},{12,4},{1,9},{5,13},{9,1},{13,5},{2,10},{6,14},... | collective-permute-start | bytes 79880 | tf_op jit(solution)/shard_map/ppermute | solution.py:47
  15.0 5.9 %collective-permute-start.5 = (bf16[4,3328]{1,0:T(4,128)(2,1)S(1)}, bf16[4,3328]{1,0:T(4,128)(2,1)S(1)}, u32[]{:S(2)}, u32[]{:S(2)}) collective-permute-start(bf16[4,3328]{1,0:T(4,128)(2,1)S(1)} %get-tuple-element.36), channel_id=1, source_target_pairs={{0,12},{4,8},{8,4},{12,0},{1,13},{5,9},{9,5},{13,1},{2,14},{6,10},... | collective-permute-start | bytes 79880 | tf_op jit(solution)/shard_map/ppermute | solution.py:47
  19.4 10.1 %copy-start.1 = (bf16[2048,1024]{1,0:T(8,128)(2,1)S(1)}, bf16[2048,1024]{1,0:T(8,128)(2,1)}, u32[]{:S(2)}) copy-start(bf16[2048,1024]{1,0:T(8,128)(2,1)} %refs_4_.3) | copy-start | bytes 12582916
  21.3 6.2 %collective-permute-start.8 = (bf16[4,2048]{1,0:T(4,128)(2,1)S(1)}, bf16[4,2048]{1,0:T(4,128)(2,1)S(1)}, u32[]{:S(2)}, u32[]{:S(2)}) collective-permute-start(bf16[4,2048]{1,0:T(4,128)(2,1)S(1)} %get-tuple-element.43.refs_0_), channel_id=1, source_target_pairs={{0,12},{4,8},{8,4},{12,0},{1,13},{5,9},{9,5},{13,1},{2,14},{6,10},... | collective-permute-start | bytes 49160 | tf_op jit(solution)/shard_map/ppermute | solution.py:47
  24.8 4.6 %collective-permute-start.7 = (bf16[4,2048]{1,0:T(4,128)(2,1)S(1)}, bf16[4,2048]{1,0:T(4,128)(2,1)S(1)}, u32[]{:S(2)}, u32[]{:S(2)}) collective-permute-start(bf16[4,2048]{1,0:T(4,128)(2,1)S(1)} %get-tuple-element.43.refs_0_), channel_id=1, source_target_pairs={{0,8},{4,12},{8,0},{12,4},{1,9},{5,13},{9,1},{13,5},{2,10},{6,14},... | collective-permute-start | bytes 49160 | tf_op jit(solution)/shard_map/ppermute | solution.py:47
  24.8 4.6 %collective-permute-start.6 = (bf16[4,2048]{1,0:T(4,128)(2,1)S(1)}, bf16[4,2048]{1,0:T(4,128)(2,1)S(1)}, u32[]{:S(2)}, u32[]{:S(2)}) collective-permute-start(bf16[4,2048]{1,0:T(4,128)(2,1)S(1)} %get-tuple-element.43.refs_0_), channel_id=1, source_target_pairs={{0,4},{4,0},{8,12},{12,8},{1,5},{5,1},{9,13},{13,9},{2,6},{6,2},{1... | collective-permute-start | bytes 49160 | tf_op jit(solution)/shard_map/ppermute | solution.py:47
  30.2 3.8 %collective-permute-start.9 = (bf16[4,1024]{1,0:T(4,128)(2,1)S(1)}, bf16[4,1024]{1,0:T(4,128)(2,1)S(1)}, u32[]{:S(2)}, u32[]{:S(2)}) collective-permute-start(bf16[4,1024]{1,0:T(4,128)(2,1)S(1)} %get-tuple-element.48), channel_id=1, source_target_pairs={{0,1},{1,0},{2,3},{3,2},{4,5},{5,4},{6,7},{7,6},{8,9},{9,8},{10,11... | collective-permute-start | bytes 24584 | tf_op jit(solution)/shard_map/ppermute | solution.py:47
  30.2 3.7 %collective-permute-start.10 = (bf16[4,1024]{1,0:T(4,128)(2,1)S(1)}, bf16[4,1024]{1,0:T(4,128)(2,1)S(1)}, u32[]{:S(2)}, u32[]{:S(2)}) collective-permute-start(bf16[4,1024]{1,0:T(4,128)(2,1)S(1)} %get-tuple-element.49), channel_id=1, source_target_pairs={{0,2},{1,3},{2,0},{3,1},{4,6},{5,7},{6,4},{7,5},{8,10},{9,11},{10,... | collective-permute-start | bytes 24584 | tf_op jit(solution)/shard_map/ppermute | solution.py:47
  31.8 3.1 %collective-permute-start.11 = (bf16[4,1024]{1,0:T(4,128)(2,1)S(1)}, bf16[4,1024]{1,0:T(4,128)(2,1)S(1)}, u32[]{:S(2)}, u32[]{:S(2)}) collective-permute-start(bf16[4,1024]{1,0:T(4,128)(2,1)S(1)} %get-tuple-element.50), channel_id=1, source_target_pairs={{0,3},{1,2},{2,1},{3,0},{4,7},{5,6},{6,5},{7,4},{8,11},{9,10},{10,... | collective-permute-start | bytes 24584 | tf_op jit(solution)/shard_map/ppermute | solution.py:47

commit v4 on v3

--- a/solution.py
+++ b/solution.py
@@ -38,6 +38,18 @@
         cost_estimate=pl.CostEstimate(flops=flops, transcendentals=0, bytes_accessed=moved),
         compiler_params=pltpu.CompilerParams(vmem_limit_bytes=limit),
     )(*ins)
+
+
+def exchange_tokens(blocks, count):
+    got = []
+    for step in range(1, count):
+        pairs = [
+            (i * count + j, (i ^ step) * count + (j ^ 1))
+            for i in range(count)
+            for j in range(count)
+        ]
+        got.append(lax.ppermute(blocks[step], ("kv", "tp"), pairs))
+    return got
 
 
 def exchange(blocks, axis, count):
@@ -267,7 +279,7 @@
     per = heads // groups
     last = pieces[-1][2] == per and pieces[-1][0] == groups - 1
     if last:
-        fresh, history, _, states, tail, held, sem = refs
+        fresh, history, _, states, tail_out, held, tail, sem = refs
     else:
         states, flag, held, sem = refs
         flag[...] = jnp.zeros_like(flag)
@@ -276,6 +288,22 @@
     wide = heads * head_dim
     block = groups * size
     count = accepted[0]
+    if last:
+        before = tail.shape[1] - props
+        for k in range(before):
+            tail[0, k] = history[0, count + k]
+        for j in range(props):
+            rows = []
+            for q in range(groups):
+                row = [fresh[j : j + 1, q * inner : (q + 1) * inner]]
+                for part in range(2):
+                    base = wide + part * block + q * size
+                    row.append(fresh[j : j + 1, base : base + size])
+                rows.append(jnp.concatenate(row, axis=1))
+            tail[0, before + j] = jnp.concatenate(rows, axis=0).astype(BF16)
+        copy = pltpu.make_async_copy(tail, tail_out, sem.at[len(pieces)])
+        copy.start()
+        copies.append(copy)
     row_at = lax.broadcasted_iota(jnp.int32, (ROWS, 1), 0)
     b_high, b_low = split(act[:, wide : wide + block])
     b_high, b_low = b_high.astype(F32), b_low.astype(F32)
@@ -313,27 +341,11 @@
         copy = pltpu.make_async_copy(
             held.at[:, pl.ds(filled, high - low)],
             states.at[0, :, pl.ds(g * per + low, high - low)],
-            sem.at[len(copies)],
+            sem.at[pieces.index((g, low, high))],
         )
         copy.start()
         copies.append(copy)
         filled += high - low
-    if not last:
-        for copy in copies:
-            copy.wait()
-        return
-    before = tail.shape[1] - props
-    for k in range(before):
-        tail[0, k] = history[0, count + k]
-    for j in range(props):
-        rows = []
-        for q in range(groups):
-            row = [fresh[j : j + 1, q * inner : (q + 1) * inner]]
-            for part in range(2):
-                base = wide + part * block + q * size
-                row.append(fresh[j : j + 1, base : base + size])
-            rows.append(jnp.concatenate(row, axis=1))
-        tail[0, before + j] = jnp.concatenate(rows, axis=0).astype(BF16)
     for copy in copies:
         copy.wait()
 
@@ -399,7 +411,7 @@
         moved=10_000_000_000,
         scratch=[pltpu.SemaphoreType.DMA((count,))],
     )
-    received = exchange(slices, "kv", count)
+    received = exchange_tokens(slices, count)
     matrices = [head_input_matrix, group_input_matrix, group_readout_matrix, output_gate_matrix]
 
     scale = input_norm_scale.reshape(1, width)
@@ -469,9 +481,9 @@
     first = 3 * len(pieces) // 4
     all_states = jax.ShapeDtypeStruct((1, props, heads, head_dim, size), F32)
 
-    def scratch(number):
+    def scratch(number, *more):
         shape = (props, number * half, head_dim, size)
-        return [pltpu.VMEM(shape, F32), pltpu.SemaphoreType.DMA((number,))]
+        return [pltpu.VMEM(shape, F32), *more, pltpu.SemaphoreType.DMA((number + 1,))]
 
     new_states, flag = call(
         functools.partial(states_body, props, groups, pieces[:first]),
@@ -490,8 +502,10 @@
         + [hbm(new_states)],
         [SMEM_SPEC] + [VMEM_SPEC] * 6 + [HBM_SPEC],
         flops=30_000_000,
-        out_specs=[HBM_SPEC, VMEM_SPEC],
-        scratch=scratch(len(pieces) - first),
+        out_specs=[HBM_SPEC, HBM_SPEC],
+        scratch=scratch(
+            len(pieces) - first, pltpu.VMEM(convolution_history_rows.shape, BF16)
+        ),
         aliases={7: 0},
     )
     blocks = call(

time: 35.7 us -> 35 us (0.980)
  Pallas kernels: 8.82 us -> 8.22 us
    ppermute x12 -> x9, starting transfers between devices: 16.5 us -> 10.8 us  [exchange(): got.append(lax.ppermute(blocks[step], axis, pairs))]
    ppermute x0 -> x3, starting transfers between devices: none -> 5.43 us  [exchange_tokens(): got.append(lax.ppermute(blocks[step], ('kv', 'tp'), pairs))]
    ppermute x0 -> x3, waiting for transfers between devices: none -> 4.94 us  [exchange_tokens(): got.append(lax.ppermute(blocks[step], ('kv', 'tp'), pairs))]
    ppermute x12 -> x9, waiting for transfers between devices: 8.45 us -> 3.7 us  [exchange(): got.append(lax.ppermute(blocks[step], axis, pairs))]
    pallas_call x9, Pallas kernels: 8.82 us -> 8.22 us  [call(): pl.pallas_call(body, out_shape=outs, in_specs=specs, out_specs=out_specs...]
  transfers between devices with their start and end apart: 12 -> 12, of which waited for: 5 -> 5; matrix products, arithmetic and copies ran while one was open for 0% -> 0% of each run, Pallas kernels for 14% -> 12%
where the time goes in v4:
time: 35 us; the launch traced here: 34.8 us
  starting transfers between devices  16.2 us (46%)
  waiting for transfers between devices  8.64 us (25%)
  Pallas kernels  8.22 us (23%)
  between operations  1.62 us (5%)
    ppermute x9, starting transfers between devices, exchange(): got.append(lax.ppermute(blocks[step], axis, pairs))  10.8 us
    pallas_call x9, Pallas kernels, call(): pl.pallas_call(body, out_shape=outs, in_specs=specs, out_specs=out_specs...  8.22 us
    ppermute x3, starting transfers between devices, exchange_tokens(): got.append(lax.ppermute(blocks[step], ('kv', 'tp'), pairs))  5.43 us
    ppermute x3, waiting for transfers between devices, exchange_tokens(): got.append(lax.ppermute(blocks[step], ('kv', 'tp'), pairs))  4.94 us
    ppermute x9, waiting for transfers between devices, exchange(): got.append(lax.ppermute(blocks[step], axis, pairs))  3.7 us
  transfers between devices with their start and end apart: 12, of which 5 were waited for; matrix products, arithmetic and copies ran while one was open for 0% of the time, Pallas kernels for 12%

profile of v4, /device:TPU:0, one launch (start us, length us, event | category | flops | bytes accessed | tf_op | source)
XLA Modules:
  0.0 34.8 jit_solution(12041528426449109235)
XLA Ops:
  0.6 0.0 copy-start.2
  0.6 0.0 copy-start.3
  0.7 0.0 copy-start.4
  0.7 0.0 copy-start.5
  0.7 0.0 copy-start.8
  0.7 0.9 %shard_map.184 = (bf16[3,1024]{1,0:T(4,128)(2,1)S(1)}, bf16[3,1024]{1,0:T(4,128)(2,1)S(1)}, bf16[3,1024]{1,0:T(4,128)(2,1)S(1)}, bf16[3,1024]{1,0:T(4,128)(2,1)S(1)}) custom-call(bf16[1,3,4096]{2,1,0:T(4,128)(2,1)} %tokens.3), custom_call_target="tpu_custom_call" | custom-call | flops 999999995904 | bytes 10000000000 | tf_op jit(solution)/shard_map/pallas_call | solution.py:31
  1.6 2.6 %collective-permute-start = (bf16[3,1024]{1,0:T(4,128)(2,1)S(1)}, bf16[3,1024]{1,0:T(4,128)(2,1)S(1)}, u32[]{:S(2)}, u32[]{:S(2)}) collective-permute-start(bf16[3,1024]{1,0:T(4,128)(2,1)S(1)} %get-tuple-element.30), channel_id=1, source_target_pairs={{0,5},{1,4},{2,7},{3,6},{4,1},{5,0},{6,3},{7,2},{8,13},{9,12},{10,... | collective-permute-start | bytes 18440 | tf_op jit(solution)/shard_map/ppermute | solution.py:51
  4.2 2.9 %collective-permute-start.1 = (bf16[3,1024]{1,0:T(4,128)(2,1)S(1)}, bf16[3,1024]{1,0:T(4,128)(2,1)S(1)}, u32[]{:S(2)}, u32[]{:S(2)}) collective-permute-start(bf16[3,1024]{1,0:T(4,128)(2,1)S(1)} %get-tuple-element.31), channel_id=1, source_target_pairs={{0,9},{1,8},{2,11},{3,10},{4,13},{5,12},{6,15},{7,14},{8,1},{9,0},... | collective-permute-start | bytes 18440 | tf_op jit(solution)/shard_map/ppermute | solution.py:51
  7.1 0.0 collective-permute-start.2
  7.1 0.0 collective-permute-done.refs_1_
  7.1 1.4 %collective-permute-done.1.refs_2_ = bf16[3,1024]{1,0:T(4,128)(2,1)S(1)} collective-permute-done((bf16[3,1024]{1,0:T(4,128)(2,1)S(1)}, bf16[3,1024]{1,0:T(4,128)(2,1)S(1)}, u32[]{:S(2)}, u32[]{:S(2)}) %collective-permute-start.1) | collective-permute-done | bytes 6176 | tf_op jit(solution)/shard_map/ppermute | solution.py:51
  8.5 3.6 %collective-permute-done.2.refs_3_ = bf16[3,1024]{1,0:T(4,128)(2,1)S(1)} collective-permute-done((bf16[3,1024]{1,0:T(4,128)(2,1)S(1)}, bf16[3,1024]{1,0:T(4,128)(2,1)S(1)}, u32[]{:S(2)}, u32[]{:S(2)}) %collective-permute-start.2) | collective-permute-done | bytes 6176 | tf_op jit(solution)/shard_map/ppermute | solution.py:51
  12.0 0.0 copy-done.2
  12.0 0.0 copy-done.3
  12.0 0.0 copy-done.4
  12.0 0.0 copy-done.5
  12.0 0.0 copy-done.8
  12.0 0.0 copy-start.15
  12.0 0.0 copy-start
  12.1 0.0 copy-start.7
  12.1 0.0 copy-start.10
  12.1 0.0 copy-start.6
  12.1 0.0 copy-start.9
  12.1 0.0 copy-start.12
  12.1 0.0 copy-start.13
  12.1 0.0 copy-start.14
  12.1 0.0 copy-start.11
  12.2 1.3 %shard_map.185 = (f32[4,3328]{1,0:T(4,128)S(1)}, bf16[4,3328]{1,0:T(4,128)(2,1)S(1)}, bf16[4,3328]{1,0:T(4,128)(2,1)S(1)}, bf16[4,3328]{1,0:T(4,128)(2,1)S(1)}) custom-call(bf16[3,1024]{1,0:T(4,128)(2,1)S(1)} %get-tuple-element.29.refs_0_, bf16[3,1024]{1,0:T(4,128)(2,1)S(1)} %collective-permute-done.refs_1_, ...), custom_call_target="tpu_custom_call" | custom-call | flops 200000000 | tf_op jit(solution)/shard_map/pallas_call | solution.py:31
  13.5 0.1 collective-permute-start.3
  13.5 0.4 %collective-permute-start.4 = (bf16[4,3328]{1,0:T(4,128)(2,1)S(1)}, bf16[4,3328]{1,0:T(4,128)(2,1)S(1)}, u32[]{:S(2)}, u32[]{:S(2)}) collective-permute-start(bf16[4,3328]{1,0:T(4,128)(2,1)S(1)} %get-tuple-element.35), channel_id=1, source_target_pairs={{0,8},{4,12},{8,0},{12,4},{1,9},{5,13},{9,1},{13,5},{2,10},{6,14},... | collective-permute-start | bytes 79880 | tf_op jit(solution)/shard_map/ppermute | solution.py:59
  13.9 4.0 %collective-permute-start.5 = (bf16[4,3328]{1,0:T(4,128)(2,1)S(1)}, bf16[4,3328]{1,0:T(4,128)(2,1)S(1)}, u32[]{:S(2)}, u32[]{:S(2)}) collective-permute-start(bf16[4,3328]{1,0:T(4,128)(2,1)S(1)} %get-tuple-element.36), channel_id=1, source_target_pairs={{0,12},{4,8},{8,4},{12,0},{1,13},{5,9},{9,5},{13,1},{2,14},{6,10},... | collective-permute-start | bytes 79880 | tf_op jit(solution)/shard_map/ppermute | solution.py:59
  18.6 0.0 copy-done.15
  18.6 0.0 copy-done
  18.6 0.0 copy-done.7
  18.6 0.0 copy-done.10
  18.6 0.0 copy-start.1
  18.6 0.4 %shard_map.187 = (bf16[128,2048]{1,0:T(8,128)(2,1)S(1)}, bf16[128,2048]{1,0:T(8,128)(2,1)S(1)}, f32[8,2304]{1,0:T(8,128)S(1)}, f32[8,2304]{1,0:T(8,128)S(1)}) custom-call(s32[1]{0:T(128)S(6)} %copy.25.accepted, f32[1,3,32,64,64]{4,3,2,1,0:T(8,128)S(1)} %copy-done, bf16[1,6,2,1152]{3,2,1,0:T(2,128)(2,1)S(1)} %copy-done.7, bf16[4,2,1152]{2,1,0:T(2,128)(2,1)S(1)} %copy-done.10), custom_call_target="tpu_custom_call" | custom-call | flops 20000000 | tf_op jit(solution)/shard_map/pallas_call | solution.py:31
  19.0 0.0 copy-done.6
  19.1 0.0 copy-done.9
  19.1 0.0 copy-done.12
  19.1 0.0 copy-done.13
  19.1 0.0 copy-done.14
  19.1 0.9 %shard_map.186 = (f32[5,8,2048]{2,1,0:T(8,128)S(1)}, f32[8,32]{1,0:T(8,128)S(1)}, f32[8,128]{1,0:T(8,128)S(1)}) custom-call(s32[1]{0:T(128)S(6)} %copy.25.accepted, bf16[1,3,4096]{2,1,0:T(4,128)(2,1)S(1)} %copy-done.9, f32[1,4096]{1,0:T(1,128)S(1)} %bitcast.11, bf16[32,4096]{1,0:T(8,128)(2,1)S(1)} %bitcast.9, f32[1,32]{1,0:T(1,128)S(1)} %bitcast.14, ...), custom_call_target="tpu_custom_call" | custom-call | flops 20000000 | tf_op jit(solution)/shard_map/pallas_call | solution.py:31
  20.0 0.0 collective-permute-done.3.refs_1_
  20.0 0.0 collective-permute-done.4.refs_2_
  20.0 0.0 collective-permute-done.5.refs_3_
  20.0 0.0 copy-done.11
  20.0 0.4 %shard_map.188 = (bf16[4,2048]{1,0:T(4,128)(2,1)S(1)}, f32[8,2304]{1,0:T(8,128)S(1)}, f32[8,2304]{1,0:T(8,128)S(1)}) custom-call(f32[4,3328]{1,0:T(4,128)S(1)} %get-tuple-element.33.refs_0_, bf16[4,3328]{1,0:T(4,128)(2,1)S(1)} %collective-permute-done.3.refs_1_, bf16[4,3328]{1,0:T(4,128)(2,1)S(1)} %collective-permute-done.4.refs_2_, ...), custom_call_target="tpu_custom_call" | custom-call | flops 20000000 | tf_op jit(solution)/shard_map/pallas_call | solution.py:31
  20.5 3.6 %collective-permute-start.8 = (bf16[4,2048]{1,0:T(4,128)(2,1)S(1)}, bf16[4,2048]{1,0:T(4,128)(2,1)S(1)}, u32[]{:S(2)}, u32[]{:S(2)}) collective-permute-start(bf16[4,2048]{1,0:T(4,128)(2,1)S(1)} %get-tuple-element.43.refs_0_), channel_id=1, source_target_pairs={{0,12},{4,8},{8,4},{12,0},{1,13},{5,9},{9,5},{13,1},{2,14},{6,10},... | collective-permute-start | bytes 49160 | tf_op jit(solution)/shard_map/ppermute | solution.py:59
  24.1 0.0 collective-permute-start.7
  24.1 0.8 %collective-permute-start.6 = (bf16[4,2048]{1,0:T(4,128)(2,1)S(1)}, bf16[4,2048]{1,0:T(4,128)(2,1)S(1)}, u32[]{:S(2)}, u32[]{:S(2)}) collective-permute-start(bf16[4,2048]{1,0:T(4,128)(2,1)S(1)} %get-tuple-element.43.refs_0_), channel_id=1, source_target_pairs={{0,4},{4,0},{8,12},{12,8},{1,5},{5,1},{9,13},{13,9},{2,6},{6,2},{1... | collective-permute-start | bytes 49160 | tf_op jit(solution)/shard_map/ppermute | solution.py:59
  24.9 1.8 %shard_map.189 = (f32[1,3,32,64,64]{4,3,2,1,0:T(8,128)}, f32[8,128]{1,0:T(8,128)S(1)}) custom-call(s32[1]{0:T(128)S(6)} %copy.25.accepted, f32[1,3,32,64,64]{4,3,2,1,0:T(8,128)S(1)} %copy-done, f32[8,32]{1,0:T(8,128)S(1)} %get-tuple-element.44.small, f32[8,2304]{1,0:T(8,128)S(1)} %get-tuple-element.45.act, f32[5,8,2048]{2,1,0:T(8,128)S(1)} %get-tuple-element.38.refs_5_.coef), custom_call_target="tpu_custom_call" | custom-call | flops 30000000 | tf_op jit(solution)/shard_map/pallas_call | solution.py:31
  26.7 0.0 collective-permute-done.8.refs_3_
  26.7 2.0 %collective-permute-done.7.refs_2_ = bf16[4,2048]{1,0:T(4,128)(2,1)S(1)} collective-permute-done((bf16[4,2048]{1,0:T(4,128)(2,1)S(1)}, bf16[4,2048]{1,0:T(4,128)(2,1)S(1)}, u32[]{:S(2)}, u32[]{:S(2)}) %collective-permute-start.7) | collective-permute-done | bytes 16416 | tf_op jit(solution)/shard_map/ppermute | solution.py:59
  28.7 0.0 collective-permute-done.6.refs_1_
  28.7 0.7 %shard_map.190 = (bf16[4,1024]{1,0:T(4,128)(2,1)S(1)}, bf16[4,1024]{1,0:T(4,128)(2,1)S(1)}, bf16[4,1024]{1,0:T(4,128)(2,1)S(1)}, bf16[4,1024]{1,0:T(4,128)(2,1)S(1)}) custom-call(bf16[4,2048]{1,0:T(4,128)(2,1)S(1)} %get-tuple-element.43.refs_0_, bf16[4,2048]{1,0:T(4,128)(2,1)S(1)} %collective-permute-done.6.refs_1_, ...), custom_call_target="tpu_custom_call" | custom-call | flops 100000000 | tf_op jit(solution)/shard_map/pallas_call | solution.py:31
  29.4 0.1 collective-permute-start.9
  29.5 1.7 %collective-permute-start.10 = (bf16[4,1024]{1,0:T(4,128)(2,1)S(1)}, bf16[4,1024]{1,0:T(4,128)(2,1)S(1)}, u32[]{:S(2)}, u32[]{:S(2)}) collective-permute-start(bf16[4,1024]{1,0:T(4,128)(2,1)S(1)} %get-tuple-element.49), channel_id=1, source_target_pairs={{0,2},{1,3},{2,0},{3,1},{4,6},{5,7},{6,4},{7,5},{8,10},{9,11},{10,... | collective-permute-start | bytes 24584 | tf_op jit(solution)/shard_map/ppermute | solution.py:59
  31.1 0.2 collective-permute-start.11
  31.3 1.2 %shard_map.192 = (f32[1,3,32,64,64]{4,3,2,1,0:T(8,128)}, bf16[1,6,2,1152]{3,2,1,0:T(2,128)(2,1)}) custom-call(s32[1]{0:T(128)S(6)} %copy.25.accepted, f32[1,3,32,64,64]{4,3,2,1,0:T(8,128)S(1)} %copy-done, f32[8,32]{1,0:T(8,128)S(1)} %get-tuple-element.44.small, f32[8,2304]{1,0:T(8,128)S(1)} %get-tuple-element.45.act, ...), custom_call_target="tpu_custom_call", output_to_operand_aliasing={{0}: (7, {})} | custom-call | flops 30000000 | tf_op jit(solution)/shard_map/pallas_call | solution.py:31
  32.6 0.0 collective-permute-done.9.refs_1_
  32.6 0.6 %collective-permute-done.10.refs_2_ = bf16[4,1024]{1,0:T(4,128)(2,1)S(1)} collective-permute-done((bf16[4,1024]{1,0:T(4,128)(2,1)S(1)}, bf16[4,1024]{1,0:T(4,128)(2,1)S(1)}, u32[]{:S(2)}, u32[]{:S(2)}) %collective-permute-start.10) | collective-permute-done | bytes 8224 | tf_op jit(solution)/shard_map/ppermute | solution.py:59
  33.2 1.0 %collective-permute-done.11.refs_3_ = bf16[4,1024]{1,0:T(4,128)(2,1)S(1)} collective-permute-done((bf16[4,1024]{1,0:T(4,128)(2,1)S(1)}, bf16[4,1024]{1,0:T(4,128)(2,1)S(1)}, u32[]{:S(2)}, u32[]{:S(2)}) %collective-permute-start.11) | collective-permute-done | bytes 8224 | tf_op jit(solution)/shard_map/ppermute | solution.py:59
  34.2 0.6 %shard_map.191 = bf16[1,3,1024]{2,1,0:T(4,128)(2,1)} custom-call(bf16[4,1024]{1,0:T(4,128)(2,1)S(1)} %get-tuple-element.47.refs_0_, bf16[4,1024]{1,0:T(4,128)(2,1)S(1)} %collective-permute-done.9.refs_1_, bf16[4,1024]{1,0:T(4,128)(2,1)S(1)} %collective-permute-done.10.refs_2_, bf16[4,1024]{1,0:T(4,128)(2,1)S(1)} %collective-permute-done.11.refs_3_), custom_call_target="tpu_custom_call" | custom-call | tf_op jit(solution)/shard_map/pallas_call | solution.py:31
  (2 shorter events, 0.0 us)
Async XLA Ops:
  0.6 11.4 %copy-start.2 = (bf16[1024,2048]{1,0:T(8,128)(2,1)S(1)}, bf16[1024,2048]{1,0:T(8,128)(2,1)}, u32[]{:S(2)}) copy-start(bf16[1024,2048]{1,0:T(8,128)(2,1)} %refs_4_.2) | copy-start | bytes 12582916
  0.6 11.4 %copy-start.3 = (bf16[1024,2048]{1,0:T(8,128)(2,1)S(1)}, bf16[1024,2048]{1,0:T(8,128)(2,1)}, u32[]{:S(2)}) copy-start(bf16[1024,2048]{1,0:T(8,128)(2,1)} %refs_7_.1) | copy-start | bytes 12582916
  0.7 11.4 %copy-start.4 = (bf16[1024,128]{1,0:T(8,128)(2,1)S(1)}, bf16[1024,128]{1,0:T(8,128)(2,1)}, u32[]{:S(2)}) copy-start(bf16[1024,128]{1,0:T(8,128)(2,1)} %refs_5_.1) | copy-start | bytes 786436
  0.7 11.4 %copy-start.5 = (bf16[1024,128]{1,0:T(8,128)(2,1)S(1)}, bf16[1024,128]{1,0:T(8,128)(2,1)}, u32[]{:S(2)}) copy-start(bf16[1024,128]{1,0:T(8,128)(2,1)} %refs_6_.1) | copy-start | bytes 786436
  0.7 11.4 %copy-start.8 = (f32[4096]{0:T(1024)S(1)}, f32[4096]{0:T(1024)}, u32[]{:S(2)}) copy-start(f32[4096]{0:T(1024)} %param.18) | copy-start | bytes 49156
  1.6 5.4 %collective-permute-start = (bf16[3,1024]{1,0:T(4,128)(2,1)S(1)}, bf16[3,1024]{1,0:T(4,128)(2,1)S(1)}, u32[]{:S(2)}, u32[]{:S(2)}) collective-permute-start(bf16[3,1024]{1,0:T(4,128)(2,1)S(1)} %get-tuple-element.30), channel_id=1, source_target_pairs={{0,5},{1,4},{2,7},{3,6},{4,1},{5,0},{6,3},{7,2},{8,13},{9,12},{10,... | collective-permute-start | bytes 18440 | tf_op jit(solution)/shard_map/ppermute | solution.py:51
  4.2 4.3 %collective-permute-start.1 = (bf16[3,1024]{1,0:T(4,128)(2,1)S(1)}, bf16[3,1024]{1,0:T(4,128)(2,1)S(1)}, u32[]{:S(2)}, u32[]{:S(2)}) collective-permute-start(bf16[3,1024]{1,0:T(4,128)(2,1)S(1)} %get-tuple-element.31), channel_id=1, source_target_pairs={{0,9},{1,8},{2,11},{3,10},{4,13},{5,12},{6,15},{7,14},{8,1},{9,0},... | collective-permute-start | bytes 18440 | tf_op jit(solution)/shard_map/ppermute | solution.py:51
  7.1 4.9 %collective-permute-start.2 = (bf16[3,1024]{1,0:T(4,128)(2,1)S(1)}, bf16[3,1024]{1,0:T(4,128)(2,1)S(1)}, u32[]{:S(2)}, u32[]{:S(2)}) collective-permute-start(bf16[3,1024]{1,0:T(4,128)(2,1)S(1)} %get-tuple-element.32), channel_id=1, source_target_pairs={{0,13},{1,12},{2,15},{3,14},{4,9},{5,8},{6,11},{7,10},{8,5},{9,4},... | collective-permute-start | bytes 18440 | tf_op jit(solution)/shard_map/ppermute | solution.py:51
  12.0 6.5 %copy-start.15 = (f32[1,3,32]{2,0,1:T(1,128)S(1)}, f32[1,3,32]{2,0,1:T(1,128)}, u32[]{:S(2)}) copy-start(f32[1,3,32]{2,0,1:T(1,128)} %param.31) | copy-start | bytes 1156
  12.0 6.5 %copy-start = (f32[1,3,32,64,64]{4,3,2,1,0:T(8,128)S(1)}, f32[1,3,32,64,64]{4,3,2,1,0:T(8,128)}, u32[]{:S(2)}) copy-start(f32[1,3,32,64,64]{4,3,2,1,0:T(8,128)} %start.3) | copy-start | bytes 4718596
  12.1 6.5 %copy-start.7 = (bf16[1,6,2,1152]{3,2,1,0:T(2,128)(2,1)S(1)}, bf16[1,6,2,1152]{3,2,1,0:T(2,128)(2,1)}, u32[]{:S(2)}) copy-start(bf16[1,6,2,1152]{3,2,1,0:T(2,128)(2,1)} %refs_1_.1) | copy-start | bytes 82948
  12.1 6.5 %copy-start.10 = (bf16[4,2,1152]{2,1,0:T(2,128)(2,1)S(1)}, bf16[4,2,1152]{2,1,0:T(2,128)(2,1)}, u32[]{:S(2)}) copy-start(bf16[4,2,1152]{2,1,0:T(2,128)(2,1)} %taps.1) | copy-start | bytes 55300
  12.1 7.0 %copy-start.6 = (bf16[4096,32]{0,1:T(8,128)(2,1)S(1)}, bf16[4096,32]{0,1:T(8,128)(2,1)}, u32[]{:S(2)}) copy-start(bf16[4096,32]{0,1:T(8,128)(2,1)} %param.23) | copy-start | bytes 786436
  12.1 7.0 %copy-start.9 = (bf16[1,3,4096]{2,1,0:T(4,128)(2,1)S(1)}, bf16[1,3,4096]{2,1,0:T(4,128)(2,1)}, u32[]{:S(2)}) copy-start(bf16[1,3,4096]{2,1,0:T(4,128)(2,1)} %tokens.3) | copy-start | bytes 73732
  12.1 7.0 %copy-start.12 = (f32[32]{0:T(128)S(1)}, f32[32]{0:T(128)}, u32[]{:S(2)}) copy-start(f32[32]{0:T(128)} %param.24) | copy-start | bytes 388
  12.1 7.0 %copy-start.13 = (f32[32]{0:T(128)S(1)}, f32[32]{0:T(128)}, u32[]{:S(2)}) copy-start(f32[32]{0:T(128)} %param.25) | copy-start | bytes 388
  12.1 7.0 %copy-start.14 = (f32[32]{0:T(128)S(1)}, f32[32]{0:T(128)}, u32[]{:S(2)}) copy-start(f32[32]{0:T(128)} %param.26) | copy-start | bytes 388
  12.1 7.9 %copy-start.11 = (f32[2048]{0:T(1024)S(1)}, f32[2048]{0:T(1024)}, u32[]{:S(2)}) copy-start(f32[2048]{0:T(1024)} %param.32) | copy-start | bytes 24580
  13.5 6.5 %collective-permute-start.3 = (bf16[4,3328]{1,0:T(4,128)(2,1)S(1)}, bf16[4,3328]{1,0:T(4,128)(2,1)S(1)}, u32[]{:S(2)}, u32[]{:S(2)}) collective-permute-start(bf16[4,3328]{1,0:T(4,128)(2,1)S(1)} %get-tuple-element.34), channel_id=1, source_target_pairs={{0,4},{4,0},{8,12},{12,8},{1,5},{5,1},{9,13},{13,9},{2,6},{6,2},{1... | collective-permute-start | bytes 79880 | tf_op jit(solution)/shard_map/ppermute | solution.py:59
  13.5 6.4 %collective-permute-start.4 = (bf16[4,3328]{1,0:T(4,128)(2,1)S(1)}, bf16[4,3328]{1,0:T(4,128)(2,1)S(1)}, u32[]{:S(2)}, u32[]{:S(2)}) collective-permute-start(bf16[4,3328]{1,0:T(4,128)(2,1)S(1)} %get-tuple-element.35), channel_id=1, source_target_pairs={{0,8},{4,12},{8,0},{12,4},{1,9},{5,13},{9,1},{13,5},{2,10},{6,14},... | collective-permute-start | bytes 79880 | tf_op jit(solution)/shard_map/ppermute | solution.py:59
  13.9 6.1 %collective-permute-start.5 = (bf16[4,3328]{1,0:T(4,128)(2,1)S(1)}, bf16[4,3328]{1,0:T(4,128)(2,1)S(1)}, u32[]{:S(2)}, u32[]{:S(2)}) collective-permute-start(bf16[4,3328]{1,0:T(4,128)(2,1)S(1)} %get-tuple-element.36), channel_id=1, source_target_pairs={{0,12},{4,8},{8,4},{12,0},{1,13},{5,9},{9,5},{13,1},{2,14},{6,10},... | collective-permute-start | bytes 79880 | tf_op jit(solution)/shard_map/ppermute | solution.py:59
  18.6 10.1 %copy-start.1 = (bf16[2048,1024]{1,0:T(8,128)(2,1)S(1)}, bf16[2048,1024]{1,0:T(8,128)(2,1)}, u32[]{:S(2)}) copy-start(bf16[2048,1024]{1,0:T(8,128)(2,1)} %refs_4_.3) | copy-start | bytes 12582916
  20.5 6.2 %collective-permute-start.8 = (bf16[4,2048]{1,0:T(4,128)(2,1)S(1)}, bf16[4,2048]{1,0:T(4,128)(2,1)S(1)}, u32[]{:S(2)}, u32[]{:S(2)}) collective-permute-start(bf16[4,2048]{1,0:T(4,128)(2,1)S(1)} %get-tuple-element.43.refs_0_), channel_id=1, source_target_pairs={{0,12},{4,8},{8,4},{12,0},{1,13},{5,9},{9,5},{13,1},{2,14},{6,10},... | collective-permute-start | bytes 49160 | tf_op jit(solution)/shard_map/ppermute | solution.py:59
  24.1 4.6 %collective-permute-start.7 = (bf16[4,2048]{1,0:T(4,128)(2,1)S(1)}, bf16[4,2048]{1,0:T(4,128)(2,1)S(1)}, u32[]{:S(2)}, u32[]{:S(2)}) collective-permute-start(bf16[4,2048]{1,0:T(4,128)(2,1)S(1)} %get-tuple-element.43.refs_0_), channel_id=1, source_target_pairs={{0,8},{4,12},{8,0},{12,4},{1,9},{5,13},{9,1},{13,5},{2,10},{6,14},... | collective-permute-start | bytes 49160 | tf_op jit(solution)/shard_map/ppermute | solution.py:59
  24.1 4.6 %collective-permute-start.6 = (bf16[4,2048]{1,0:T(4,128)(2,1)S(1)}, bf16[4,2048]{1,0:T(4,128)(2,1)S(1)}, u32[]{:S(2)}, u32[]{:S(2)}) collective-permute-start(bf16[4,2048]{1,0:T(4,128)(2,1)S(1)} %get-tuple-element.43.refs_0_), channel_id=1, source_target_pairs={{0,4},{4,0},{8,12},{12,8},{1,5},{5,1},{9,13},{13,9},{2,6},{6,2},{1... | collective-permute-start | bytes 49160 | tf_op jit(solution)/shard_map/ppermute | solution.py:59
  29.4 3.2 %collective-permute-start.9 = (bf16[4,1024]{1,0:T(4,128)(2,1)S(1)}, bf16[4,1024]{1,0:T(4,128)(2,1)S(1)}, u32[]{:S(2)}, u32[]{:S(2)}) collective-permute-start(bf16[4,1024]{1,0:T(4,128)(2,1)S(1)} %get-tuple-element.48), channel_id=1, source_target_pairs={{0,1},{1,0},{2,3},{3,2},{4,5},{5,4},{6,7},{7,6},{8,9},{9,8},{10,11... | collective-permute-start | bytes 24584 | tf_op jit(solution)/shard_map/ppermute | solution.py:59
  29.5 3.7 %collective-permute-start.10 = (bf16[4,1024]{1,0:T(4,128)(2,1)S(1)}, bf16[4,1024]{1,0:T(4,128)(2,1)S(1)}, u32[]{:S(2)}, u32[]{:S(2)}) collective-permute-start(bf16[4,1024]{1,0:T(4,128)(2,1)S(1)} %get-tuple-element.49), channel_id=1, source_target_pairs={{0,2},{1,3},{2,0},{3,1},{4,6},{5,7},{6,4},{7,5},{8,10},{9,11},{10,... | collective-permute-start | bytes 24584 | tf_op jit(solution)/shard_map/ppermute | solution.py:59
  31.1 3.1 %collective-permute-start.11 = (bf16[4,1024]{1,0:T(4,128)(2,1)S(1)}, bf16[4,1024]{1,0:T(4,128)(2,1)S(1)}, u32[]{:S(2)}, u32[]{:S(2)}) collective-permute-start(bf16[4,1024]{1,0:T(4,128)(2,1)S(1)} %get-tuple-element.50), channel_id=1, source_target_pairs={{0,3},{1,2},{2,1},{3,0},{4,7},{5,6},{6,5},{7,4},{8,11},{9,10},{10,... | collective-permute-start | bytes 24584 | tf_op jit(solution)/shard_map/ppermute | solution.py:59

commit v5 on v4

--- a/solution.py
+++ b/solution.py
@@ -83,6 +83,10 @@
         copies.append(copy)
     for copy in copies:
         copy.wait()
+
+
+def hold_body(*refs):
+    pass
 
 
 def step_body(head_dim, accepted, tokens, scale, step_t, bias, rate, direct, extra, coef, small, norm, table):
@@ -123,7 +127,7 @@
         coef[part] = wide[part * ROWS : (part + 1) * ROWS]
 
 
-def state_body(accepted, states, history, taps, high, low, early, taps_wide):
+def state_body(accepted, states, history, taps, carry, early, taps_wide):
     count = accepted[0]
     heads, head_dim, size = states.shape[2:]
     groups = taps.shape[1]
@@ -156,8 +160,7 @@
         total = total + jnp.where(keep, pltpu.roll(context, ROWS - k, 0), 0.0) * taps_wide[k : k + 1, :]
     early[...] = jnp.where(keep, total, 0.0)
 
-    high[...] = jnp.zeros_like(high)
-    low[...] = jnp.zeros_like(low)
+    carry[...] = jnp.zeros_like(carry)
     pair = 128 // head_dim
     for g in range(groups):
         for block in range(per // pair):
@@ -165,8 +168,8 @@
             tile = states[0, count - 1, at : at + pair].reshape(pair * head_dim, size).T
             big, rest = split(tile)
             cols = slice(at * head_dim, (at + pair) * head_dim)
-            high[g * size : (g + 1) * size, cols] = big
-            low[g * size : (g + 1) * size, cols] = rest
+            carry[g * size : (g + 1) * size, cols] = big
+            carry[(groups + g) * size : (groups + g + 1) * size, cols] = rest
 
 
 def stack_rows(parts, lhs):
@@ -185,38 +188,46 @@
     inputs, inject, readout, gates, scale = refs[count : count + 5]
     own = refs[count + 5]
     outs = refs[count + 6 : count + 5 + count]
-    stage, rows = refs[-2:]
+    rows = refs[-1]
     depth = rows.shape[1]
     start = pl.multiple_of(lax.axis_index("kv") * depth, 128)
     stack_rows(slices, rows)
     lhs = (rows[...] * scale[:, pl.ds(start, depth)]).astype(BF16)
-    wide = stage.shape[1]
+    wide = own.shape[1]
     first = inputs.shape[1]
     both = inject.shape[1] + readout.shape[1]
     left = wide - first - both
     rest = gates.shape[1] - left
+    fourth = lax.broadcasted_iota(jnp.int32, (4, 1), 0) == 3
 
     result = jnp.dot(lhs, gates[...], preferred_element_type=F32)
-    stage[:, first + both :] = result[:, :left]
     extra = result[:, left:]
-    result = jnp.dot(lhs, inputs[...], preferred_element_type=F32)
-    stage[:, :first] = result
+
+    def store(at, values):
+        width = values.shape[1]
+        for j, out in enumerate((own, *outs)):
+            block = values[4 * j : 4 * j + 4]
+            for r in range(props):
+                low, high = max(at, r * rest), min(at + width, (r + 1) * rest)
+                if low < high:
+                    row = extra[4 * j + r : 4 * j + r + 1, low - r * rest : high - r * rest]
+                    part = block[:, low - at : high - at]
+                    out[:, low:high] = jnp.where(fourth, row, part).astype(out.dtype)
+            low = max(at, props * rest)
+            if low < at + width:
+                out[:, low : at + width] = block[:, low - at :].astype(out.dtype)
+
+    store(first + both, result[:, :left])
+    store(0, jnp.dot(lhs, inputs[...], preferred_element_type=F32))
     pair = jnp.concatenate([inject[...], readout[...]], axis=1)
-    stage[:, first : first + both] = jnp.dot(lhs, pair, preferred_element_type=F32)
-    for j in range(count):
-        for r in range(props):
-            at = 4 * j + r
-            stage[4 * j + 3 : 4 * j + 4, r * rest : (r + 1) * rest] = extra[at : at + 1]
-    own[...] = stage[0:4, :]
-    for j, out in enumerate(outs, 1):
-        out[...] = stage[4 * j : 4 * j + 4, :].astype(BF16)
+    store(first, jnp.dot(lhs, pair, preferred_element_type=F32))
 
 
 def mixer_body(props, groups, *refs):
     own, *rest = refs
-    count = len(rest) - 12
+    count = len(rest) - 11
     others = rest[:count]
-    norm, coef, early, taps, high, low, gain, gated, fresh, act, summed, norms = rest[count:]
+    norm, coef, early, taps, carry, gain, gated, fresh, act, summed, norms = rest[count:]
     inner = gain.shape[1]
     conv = early.shape[1]
     per = inner // groups
@@ -244,10 +255,16 @@
     b = value[:, inner : inner + both]
     c = value[:, inner + both :]
     c_high, c_low = split(c)
-    left = jnp.concatenate([c_high.astype(F32), c_low.astype(F32)], axis=0).astype(BF16)
-    carried = jnp.dot(left, high[...], preferred_element_type=F32)
+    c_high, c_low = c_high.astype(F32), c_low.astype(F32)
+    left = jnp.concatenate(
+        [
+            jnp.concatenate([c_high, c_high], axis=1),
+            jnp.concatenate([c_low, jnp.zeros_like(c_low)], axis=1),
+        ],
+        axis=0,
+    ).astype(BF16)
+    carried = jnp.dot(left, carry[...], preferred_element_type=F32)
     carried = carried[:ROWS] + carried[ROWS:]
-    carried = carried + jnp.dot(c_high, low[...], preferred_element_type=F32)
     lane = lax.broadcasted_iota(jnp.int32, (ROWS, both), 1)
     response = coef[0] * carried + coef[1 + props, 0:1, :] * x
     pieces = []
@@ -407,9 +424,16 @@
         [pltpu.VMEM((props, rows), BF16)] * count,
         [hbm(tokens)],
         [HBM_SPEC],
+        scratch=[pltpu.SemaphoreType.DMA((count,))],
+    )
+    slices = call(
+        hold_body,
+        [pltpu.VMEM((props, rows), BF16)] * count,
+        [vmem(v) for v in slices],
+        [VMEM_SPEC] * count,
         flops=1_000_000_000_000,
         moved=10_000_000_000,
-        scratch=[pltpu.SemaphoreType.DMA((count,))],
+        aliases={i: i for i in range(count)},
     )
     received = exchange_tokens(slices, count)
     matrices = [head_input_matrix, group_input_matrix, group_readout_matrix, output_gate_matrix]
@@ -437,11 +461,10 @@
         scratch=[pltpu.VMEM(((props + 2) * ROWS, heads), F32)],
     )
     states = vmem(per_proposal_states)
-    high, low, early, taps = call(
+    carry, early, taps = call(
         state_body,
         [
-            pltpu.VMEM((groups * size, inner), BF16),
-            pltpu.VMEM((groups * size, inner), BF16),
+            pltpu.VMEM((2 * groups * size, inner), BF16),
             pltpu.VMEM((ROWS, conv), F32),
             pltpu.VMEM((ROWS, conv), F32),
         ],
@@ -458,7 +481,7 @@
         + [vmem(scale)],
         [VMEM_SPEC] * (count + 5),
         flops=200_000_000,
-        scratch=[pltpu.VMEM((4 * count, packed), F32), pltpu.VMEM((4 * count, rows), F32)],
+        scratch=[pltpu.VMEM((4 * count, rows), F32)],
     )
     sums = exchange([None] + partials, "kv", count)
     gated, fresh, act = call(
@@ -468,9 +491,9 @@
             pltpu.VMEM((ROWS, conv), F32),
             pltpu.VMEM((ROWS, conv), F32),
         ],
-        [vmem(v) for v in [own] + sums + [norm, coef, early, taps, high, low]]
+        [vmem(v) for v in [own] + sums + [norm, coef, early, taps, carry]]
         + [vmem(group_norm_scale.reshape(1, inner))],
-        [VMEM_SPEC] * (count + 7),
+        [VMEM_SPEC] * (count + 6),
         flops=20_000_000,
         scratch=[pltpu.VMEM((ROWS, total), F32), pltpu.VMEM((ROWS, inner), F32)],
     )

time: 35 us -> 34.9 us (level)
    pallas_call x9 -> x10, Pallas kernels: 8.22 us -> 8.04 us  [call(): pl.pallas_call(body, out_shape=outs, in_specs=specs, out_specs=out_specs...]
where the time goes in v5:
time: 34.9 us; the launch traced here: 34.6 us
  starting transfers between devices  16.2 us (46%)
  waiting for transfers between devices  8.64 us (25%)
  Pallas kernels  8.04 us (23%)
  between operations  1.62 us (5%)
    ppermute x9, starting transfers between devices, exchange(): got.append(lax.ppermute(blocks[step], axis, pairs))  10.8 us
    pallas_call x10, Pallas kernels, call(): pl.pallas_call(body, out_shape=outs, in_specs=specs, out_specs=out_specs...  8.04 us
    ppermute x3, starting transfers between devices, exchange_tokens(): got.append(lax.ppermute(blocks[step], ('kv', 'tp'), pairs))  5.43 us
    ppermute x3, waiting for transfers between devices, exchange_tokens(): got.append(lax.ppermute(blocks[step], ('kv', 'tp'), pairs))  4.94 us
    ppermute x9, waiting for transfers between devices, exchange(): got.append(lax.ppermute(blocks[step], axis, pairs))  3.7 us
  transfers between devices with their start and end apart: 12, of which 5 were waited for; matrix products, arithmetic and copies ran while one was open for 0% of the time, Pallas kernels for 12%

profile of v5, /device:TPU:0, one launch (start us, length us, event | category | flops | bytes accessed | tf_op | source)
XLA Modules:
  0.0 34.6 jit_solution(7206859084803055938)
XLA Ops:
  0.6 0.8 %shard_map.184 = (bf16[3,1024]{1,0:T(4,128)(2,1)S(1)}, bf16[3,1024]{1,0:T(4,128)(2,1)S(1)}, bf16[3,1024]{1,0:T(4,128)(2,1)S(1)}, bf16[3,1024]{1,0:T(4,128)(2,1)S(1)}) custom-call(bf16[1,3,4096]{2,1,0:T(4,128)(2,1)} %tokens.3), custom_call_target="tpu_custom_call" | custom-call | tf_op jit(solution)/shard_map/pallas_call | solution.py:31
  1.4 0.0 copy-start.2
  1.4 0.0 copy-start.3
  1.5 0.0 copy-start.4
  1.5 0.0 copy-start.5
  1.5 0.0 copy-start.9
  1.5 2.6 %collective-permute-start = (bf16[3,1024]{1,0:T(4,128)(2,1)S(1)}, bf16[3,1024]{1,0:T(4,128)(2,1)S(1)}, u32[]{:S(2)}, u32[]{:S(2)}) collective-permute-start(bf16[3,1024]{1,0:T(4,128)(2,1)S(1)} %get-tuple-element.37), channel_id=1, source_target_pairs={{0,5},{1,4},{2,7},{3,6},{4,1},{5,0},{6,3},{7,2},{8,13},{9,12},{10,... | collective-permute-start | bytes 18440 | tf_op jit(solution)/shard_map/ppermute | solution.py:51
  4.1 2.9 %collective-permute-start.1 = (bf16[3,1024]{1,0:T(4,128)(2,1)S(1)}, bf16[3,1024]{1,0:T(4,128)(2,1)S(1)}, u32[]{:S(2)}, u32[]{:S(2)}) collective-permute-start(bf16[3,1024]{1,0:T(4,128)(2,1)S(1)} %get-tuple-element.38), channel_id=1, source_target_pairs={{0,9},{1,8},{2,11},{3,10},{4,13},{5,12},{6,15},{7,14},{8,1},{9,0},... | collective-permute-start | bytes 18440 | tf_op jit(solution)/shard_map/ppermute | solution.py:51
  6.9 0.0 collective-permute-start.2
  6.9 0.0 collective-permute-done.refs_1_
  6.9 1.4 %collective-permute-done.1.refs_2_ = bf16[3,1024]{1,0:T(4,128)(2,1)S(1)} collective-permute-done((bf16[3,1024]{1,0:T(4,128)(2,1)S(1)}, bf16[3,1024]{1,0:T(4,128)(2,1)S(1)}, u32[]{:S(2)}, u32[]{:S(2)}) %collective-permute-start.1) | collective-permute-done | bytes 6176 | tf_op jit(solution)/shard_map/ppermute | solution.py:51
  8.3 3.6 %collective-permute-done.2.refs_3_ = bf16[3,1024]{1,0:T(4,128)(2,1)S(1)} collective-permute-done((bf16[3,1024]{1,0:T(4,128)(2,1)S(1)}, bf16[3,1024]{1,0:T(4,128)(2,1)S(1)}, u32[]{:S(2)}, u32[]{:S(2)}) %collective-permute-start.2) | collective-permute-done | bytes 6176 | tf_op jit(solution)/shard_map/ppermute | solution.py:51
  11.9 0.0 copy-done.2
  11.9 0.0 copy-done.3
  11.9 0.0 copy-done.4
  11.9 0.0 copy-done.5
  11.9 0.0 copy-done.9
  11.9 0.0 copy-start.15
  11.9 0.0 copy-start
  11.9 0.0 copy-start.8
  11.9 0.0 copy-start.10
  12.0 0.0 copy-start.6
  12.0 0.0 copy-start.7
  12.0 0.0 copy-start.12
  12.0 0.0 copy-start.13
  12.0 0.0 copy-start.14
  12.0 0.0 copy-start.11
  12.0 1.3 %shard_map.186 = (f32[4,3328]{1,0:T(4,128)S(1)}, bf16[4,3328]{1,0:T(4,128)(2,1)S(1)}, bf16[4,3328]{1,0:T(4,128)(2,1)S(1)}, bf16[4,3328]{1,0:T(4,128)(2,1)S(1)}) custom-call(bf16[3,1024]{1,0:T(4,128)(2,1)S(1)} %get-tuple-element.36.refs_0_, bf16[3,1024]{1,0:T(4,128)(2,1)S(1)} %collective-permute-done.refs_1_, ...), custom_call_target="tpu_custom_call" | custom-call | flops 200000000 | tf_op jit(solution)/shard_map/pallas_call | solution.py:31
  13.3 0.0 collective-permute-start.3
  13.3 0.4 %collective-permute-start.4 = (bf16[4,3328]{1,0:T(4,128)(2,1)S(1)}, bf16[4,3328]{1,0:T(4,128)(2,1)S(1)}, u32[]{:S(2)}, u32[]{:S(2)}) collective-permute-start(bf16[4,3328]{1,0:T(4,128)(2,1)S(1)} %get-tuple-element.42), channel_id=1, source_target_pairs={{0,8},{4,12},{8,0},{12,4},{1,9},{5,13},{9,1},{13,5},{2,10},{6,14},... | collective-permute-start | bytes 79880 | tf_op jit(solution)/shard_map/ppermute | solution.py:59
  13.7 4.0 %collective-permute-start.5 = (bf16[4,3328]{1,0:T(4,128)(2,1)S(1)}, bf16[4,3328]{1,0:T(4,128)(2,1)S(1)}, u32[]{:S(2)}, u32[]{:S(2)}) collective-permute-start(bf16[4,3328]{1,0:T(4,128)(2,1)S(1)} %get-tuple-element.43), channel_id=1, source_target_pairs={{0,12},{4,8},{8,4},{12,0},{1,13},{5,9},{9,5},{13,1},{2,14},{6,10},... | collective-permute-start | bytes 79880 | tf_op jit(solution)/shard_map/ppermute | solution.py:59
  18.4 0.0 copy-done.15
  18.4 0.0 copy-done
  18.4 0.0 copy-done.8
  18.4 0.0 copy-done.10
  18.4 0.0 copy-start.1
  18.4 0.4 %shard_map.188 = (bf16[256,2048]{1,0:T(8,128)(2,1)S(1)}, f32[8,2304]{1,0:T(8,128)S(1)}, f32[8,2304]{1,0:T(8,128)S(1)}) custom-call(s32[1]{0:T(128)S(6)} %copy.33.accepted, f32[1,3,32,64,64]{4,3,2,1,0:T(8,128)S(1)} %copy-done, bf16[1,6,2,1152]{3,2,1,0:T(2,128)(2,1)S(1)} %copy-done.8, bf16[4,2,1152]{2,1,0:T(2,128)(2,1)S(1)} %copy-done.10), custom_call_target="tpu_custom_call" | custom-call | flops 20000000 | tf_op jit(solution)/shard_map/pallas_call | solution.py:31
  18.8 0.0 copy-done.6
  18.9 0.0 copy-done.7
  18.9 0.0 copy-done.12
  18.9 0.0 copy-done.13
  18.9 0.0 copy-done.14
  18.9 0.9 %shard_map.187 = (f32[5,8,2048]{2,1,0:T(8,128)S(1)}, f32[8,32]{1,0:T(8,128)S(1)}, f32[8,128]{1,0:T(8,128)S(1)}) custom-call(s32[1]{0:T(128)S(6)} %copy.33.accepted, bf16[1,3,4096]{2,1,0:T(4,128)(2,1)S(1)} %copy-done.7, f32[1,4096]{1,0:T(1,128)S(1)} %bitcast.11, bf16[32,4096]{1,0:T(8,128)(2,1)S(1)} %bitcast.9, f32[1,32]{1,0:T(1,128)S(1)} %bitcast.14, ...), custom_call_target="tpu_custom_call" | custom-call | flops 20000000 | tf_op jit(solution)/shard_map/pallas_call | solution.py:31
  19.8 0.0 collective-permute-done.3.refs_1_
  19.8 0.0 collective-permute-done.4.refs_2_
  19.8 0.0 collective-permute-done.5.refs_3_
  19.8 0.0 copy-done.11
  19.8 0.4 %shard_map.189 = (bf16[4,2048]{1,0:T(4,128)(2,1)S(1)}, f32[8,2304]{1,0:T(8,128)S(1)}, f32[8,2304]{1,0:T(8,128)S(1)}) custom-call(f32[4,3328]{1,0:T(4,128)S(1)} %get-tuple-element.40.refs_0_, bf16[4,3328]{1,0:T(4,128)(2,1)S(1)} %collective-permute-done.3.refs_1_, bf16[4,3328]{1,0:T(4,128)(2,1)S(1)} %collective-permute-done.4.refs_2_, ...), custom_call_target="tpu_custom_call" | custom-call | flops 20000000 | tf_op jit(solution)/shard_map/pallas_call | solution.py:31
  20.2 3.6 %collective-permute-start.8 = (bf16[4,2048]{1,0:T(4,128)(2,1)S(1)}, bf16[4,2048]{1,0:T(4,128)(2,1)S(1)}, u32[]{:S(2)}, u32[]{:S(2)}) collective-permute-start(bf16[4,2048]{1,0:T(4,128)(2,1)S(1)} %get-tuple-element.49.refs_0_), channel_id=1, source_target_pairs={{0,12},{4,8},{8,4},{12,0},{1,13},{5,9},{9,5},{13,1},{2,14},{6,10},... | collective-permute-start | bytes 49160 | tf_op jit(solution)/shard_map/ppermute | solution.py:59
  23.8 0.0 collective-permute-start.7
  23.9 0.8 %collective-permute-start.6 = (bf16[4,2048]{1,0:T(4,128)(2,1)S(1)}, bf16[4,2048]{1,0:T(4,128)(2,1)S(1)}, u32[]{:S(2)}, u32[]{:S(2)}) collective-permute-start(bf16[4,2048]{1,0:T(4,128)(2,1)S(1)} %get-tuple-element.49.refs_0_), channel_id=1, source_target_pairs={{0,4},{4,0},{8,12},{12,8},{1,5},{5,1},{9,13},{13,9},{2,6},{6,2},{1... | collective-permute-start | bytes 49160 | tf_op jit(solution)/shard_map/ppermute | solution.py:59
  24.7 1.8 %shard_map.190 = (f32[1,3,32,64,64]{4,3,2,1,0:T(8,128)}, f32[8,128]{1,0:T(8,128)S(1)}) custom-call(s32[1]{0:T(128)S(6)} %copy.33.accepted, f32[1,3,32,64,64]{4,3,2,1,0:T(8,128)S(1)} %copy-done, f32[8,32]{1,0:T(8,128)S(1)} %get-tuple-element.50.small, f32[8,2304]{1,0:T(8,128)S(1)} %get-tuple-element.51.act, f32[5,8,2048]{2,1,0:T(8,128)S(1)} %get-tuple-element.45.refs_5_.coef), custom_call_target="tpu_custom_call" | custom-call | flops 30000000 | tf_op jit(solution)/shard_map/pallas_call | solution.py:31
  26.5 0.0 collective-permute-done.8.refs_3_
  26.5 2.0 %collective-permute-done.7.refs_2_ = bf16[4,2048]{1,0:T(4,128)(2,1)S(1)} collective-permute-done((bf16[4,2048]{1,0:T(4,128)(2,1)S(1)}, bf16[4,2048]{1,0:T(4,128)(2,1)S(1)}, u32[]{:S(2)}, u32[]{:S(2)}) %collective-permute-start.7) | collective-permute-done | bytes 16416 | tf_op jit(solution)/shard_map/ppermute | solution.py:59
  28.5 0.0 collective-permute-done.6.refs_1_
  28.5 0.7 %shard_map.191 = (bf16[4,1024]{1,0:T(4,128)(2,1)S(1)}, bf16[4,1024]{1,0:T(4,128)(2,1)S(1)}, bf16[4,1024]{1,0:T(4,128)(2,1)S(1)}, bf16[4,1024]{1,0:T(4,128)(2,1)S(1)}) custom-call(bf16[4,2048]{1,0:T(4,128)(2,1)S(1)} %get-tuple-element.49.refs_0_, bf16[4,2048]{1,0:T(4,128)(2,1)S(1)} %collective-permute-done.6.refs_1_, ...), custom_call_target="tpu_custom_call" | custom-call | flops 100000000 | tf_op jit(solution)/shard_map/pallas_call | solution.py:31
  29.2 0.1 collective-permute-start.9
  29.3 1.7 %collective-permute-start.10 = (bf16[4,1024]{1,0:T(4,128)(2,1)S(1)}, bf16[4,1024]{1,0:T(4,128)(2,1)S(1)}, u32[]{:S(2)}, u32[]{:S(2)}) collective-permute-start(bf16[4,1024]{1,0:T(4,128)(2,1)S(1)} %get-tuple-element.55), channel_id=1, source_target_pairs={{0,2},{1,3},{2,0},{3,1},{4,6},{5,7},{6,4},{7,5},{8,10},{9,11},{10,... | collective-permute-start | bytes 24584 | tf_op jit(solution)/shard_map/ppermute | solution.py:59
  30.9 0.2 collective-permute-start.11
  31.1 1.2 %shard_map.193 = (f32[1,3,32,64,64]{4,3,2,1,0:T(8,128)}, bf16[1,6,2,1152]{3,2,1,0:T(2,128)(2,1)}) custom-call(s32[1]{0:T(128)S(6)} %copy.33.accepted, f32[1,3,32,64,64]{4,3,2,1,0:T(8,128)S(1)} %copy-done, f32[8,32]{1,0:T(8,128)S(1)} %get-tuple-element.50.small, f32[8,2304]{1,0:T(8,128)S(1)} %get-tuple-element.51.act, ...), custom_call_target="tpu_custom_call", output_to_operand_aliasing={{0}: (7, {})} | custom-call | flops 30000000 | tf_op jit(solution)/shard_map/pallas_call | solution.py:31
  32.3 0.0 collective-permute-done.9.refs_1_
  32.3 0.6 %collective-permute-done.10.refs_2_ = bf16[4,1024]{1,0:T(4,128)(2,1)S(1)} collective-permute-done((bf16[4,1024]{1,0:T(4,128)(2,1)S(1)}, bf16[4,1024]{1,0:T(4,128)(2,1)S(1)}, u32[]{:S(2)}, u32[]{:S(2)}) %collective-permute-start.10) | collective-permute-done | bytes 8224 | tf_op jit(solution)/shard_map/ppermute | solution.py:59
  33.0 1.0 %collective-permute-done.11.refs_3_ = bf16[4,1024]{1,0:T(4,128)(2,1)S(1)} collective-permute-done((bf16[4,1024]{1,0:T(4,128)(2,1)S(1)}, bf16[4,1024]{1,0:T(4,128)(2,1)S(1)}, u32[]{:S(2)}, u32[]{:S(2)}) %collective-permute-start.11) | collective-permute-done | bytes 8224 | tf_op jit(solution)/shard_map/ppermute | solution.py:59
  34.0 0.6 %shard_map.192 = bf16[1,3,1024]{2,1,0:T(4,128)(2,1)} custom-call(bf16[4,1024]{1,0:T(4,128)(2,1)S(1)} %get-tuple-element.53.refs_0_, bf16[4,1024]{1,0:T(4,128)(2,1)S(1)} %collective-permute-done.9.refs_1_, bf16[4,1024]{1,0:T(4,128)(2,1)S(1)} %collective-permute-done.10.refs_2_, bf16[4,1024]{1,0:T(4,128)(2,1)S(1)} %collective-permute-done.11.refs_3_), custom_call_target="tpu_custom_call" | custom-call | tf_op jit(solution)/shard_map/pallas_call | solution.py:31
  (3 shorter events, 0.0 us)
Async XLA Ops:
  1.4 10.4 %copy-start.2 = (bf16[1024,2048]{1,0:T(8,128)(2,1)S(1)}, bf16[1024,2048]{1,0:T(8,128)(2,1)}, u32[]{:S(2)}) copy-start(bf16[1024,2048]{1,0:T(8,128)(2,1)} %refs_4_.2) | copy-start | bytes 12582916
  1.4 10.4 %copy-start.3 = (bf16[1024,2048]{1,0:T(8,128)(2,1)S(1)}, bf16[1024,2048]{1,0:T(8,128)(2,1)}, u32[]{:S(2)}) copy-start(bf16[1024,2048]{1,0:T(8,128)(2,1)} %refs_7_.1) | copy-start | bytes 12582916
  1.5 10.4 %copy-start.4 = (bf16[1024,128]{1,0:T(8,128)(2,1)S(1)}, bf16[1024,128]{1,0:T(8,128)(2,1)}, u32[]{:S(2)}) copy-start(bf16[1024,128]{1,0:T(8,128)(2,1)} %refs_5_.1) | copy-start | bytes 786436
  1.5 10.4 %copy-start.5 = (bf16[1024,128]{1,0:T(8,128)(2,1)S(1)}, bf16[1024,128]{1,0:T(8,128)(2,1)}, u32[]{:S(2)}) copy-start(bf16[1024,128]{1,0:T(8,128)(2,1)} %refs_6_.1) | copy-start | bytes 786436
  1.5 10.4 %copy-start.9 = (f32[4096]{0:T(1024)S(1)}, f32[4096]{0:T(1024)}, u32[]{:S(2)}) copy-start(f32[4096]{0:T(1024)} %param.18) | copy-start | bytes 49156
  1.5 5.4 %collective-permute-start = (bf16[3,1024]{1,0:T(4,128)(2,1)S(1)}, bf16[3,1024]{1,0:T(4,128)(2,1)S(1)}, u32[]{:S(2)}, u32[]{:S(2)}) collective-permute-start(bf16[3,1024]{1,0:T(4,128)(2,1)S(1)} %get-tuple-element.37), channel_id=1, source_target_pairs={{0,5},{1,4},{2,7},{3,6},{4,1},{5,0},{6,3},{7,2},{8,13},{9,12},{10,... | collective-permute-start | bytes 18440 | tf_op jit(solution)/shard_map/ppermute | solution.py:51
  4.1 4.3 %collective-permute-start.1 = (bf16[3,1024]{1,0:T(4,128)(2,1)S(1)}, bf16[3,1024]{1,0:T(4,128)(2,1)S(1)}, u32[]{:S(2)}, u32[]{:S(2)}) collective-permute-start(bf16[3,1024]{1,0:T(4,128)(2,1)S(1)} %get-tuple-element.38), channel_id=1, source_target_pairs={{0,9},{1,8},{2,11},{3,10},{4,13},{5,12},{6,15},{7,14},{8,1},{9,0},... | collective-permute-start | bytes 18440 | tf_op jit(solution)/shard_map/ppermute | solution.py:51
  6.9 4.9 %collective-permute-start.2 = (bf16[3,1024]{1,0:T(4,128)(2,1)S(1)}, bf16[3,1024]{1,0:T(4,128)(2,1)S(1)}, u32[]{:S(2)}, u32[]{:S(2)}) collective-permute-start(bf16[3,1024]{1,0:T(4,128)(2,1)S(1)} %get-tuple-element.39), channel_id=1, source_target_pairs={{0,13},{1,12},{2,15},{3,14},{4,9},{5,8},{6,11},{7,10},{8,5},{9,4},... | collective-permute-start | bytes 18440 | tf_op jit(solution)/shard_map/ppermute | solution.py:51
  11.9 6.5 %copy-start.15 = (f32[1,3,32]{2,0,1:T(1,128)S(1)}, f32[1,3,32]{2,0,1:T(1,128)}, u32[]{:S(2)}) copy-start(f32[1,3,32]{2,0,1:T(1,128)} %param.31) | copy-start | bytes 1156
  11.9 6.5 %copy-start = (f32[1,3,32,64,64]{4,3,2,1,0:T(8,128)S(1)}, f32[1,3,32,64,64]{4,3,2,1,0:T(8,128)}, u32[]{:S(2)}) copy-start(f32[1,3,32,64,64]{4,3,2,1,0:T(8,128)} %start.3) | copy-start | bytes 4718596
  11.9 6.5 %copy-start.8 = (bf16[1,6,2,1152]{3,2,1,0:T(2,128)(2,1)S(1)}, bf16[1,6,2,1152]{3,2,1,0:T(2,128)(2,1)}, u32[]{:S(2)}) copy-start(bf16[1,6,2,1152]{3,2,1,0:T(2,128)(2,1)} %refs_1_.1) | copy-start | bytes 82948
  11.9 6.5 %copy-start.10 = (bf16[4,2,1152]{2,1,0:T(2,128)(2,1)S(1)}, bf16[4,2,1152]{2,1,0:T(2,128)(2,1)}, u32[]{:S(2)}) copy-start(bf16[4,2,1152]{2,1,0:T(2,128)(2,1)} %taps.1) | copy-start | bytes 55300
  12.0 6.9 %copy-start.6 = (bf16[4096,32]{0,1:T(8,128)(2,1)S(1)}, bf16[4096,32]{0,1:T(8,128)(2,1)}, u32[]{:S(2)}) copy-start(bf16[4096,32]{0,1:T(8,128)(2,1)} %param.23) | copy-start | bytes 786436
  12.0 6.9 %copy-start.7 = (bf16[1,3,4096]{2,1,0:T(4,128)(2,1)S(1)}, bf16[1,3,4096]{2,1,0:T(4,128)(2,1)}, u32[]{:S(2)}) copy-start(bf16[1,3,4096]{2,1,0:T(4,128)(2,1)} %tokens.3) | copy-start | bytes 73732
  12.0 6.9 %copy-start.12 = (f32[32]{0:T(128)S(1)}, f32[32]{0:T(128)}, u32[]{:S(2)}) copy-start(f32[32]{0:T(128)} %param.24) | copy-start | bytes 388
  12.0 6.9 %copy-start.13 = (f32[32]{0:T(128)S(1)}, f32[32]{0:T(128)}, u32[]{:S(2)}) copy-start(f32[32]{0:T(128)} %param.25) | copy-start | bytes 388
  12.0 6.9 %copy-start.14 = (f32[32]{0:T(128)S(1)}, f32[32]{0:T(128)}, u32[]{:S(2)}) copy-start(f32[32]{0:T(128)} %param.26) | copy-start | bytes 388
  12.0 7.8 %copy-start.11 = (f32[2048]{0:T(1024)S(1)}, f32[2048]{0:T(1024)}, u32[]{:S(2)}) copy-start(f32[2048]{0:T(1024)} %param.32) | copy-start | bytes 24580
  13.3 6.4 %collective-permute-start.3 = (bf16[4,3328]{1,0:T(4,128)(2,1)S(1)}, bf16[4,3328]{1,0:T(4,128)(2,1)S(1)}, u32[]{:S(2)}, u32[]{:S(2)}) collective-permute-start(bf16[4,3328]{1,0:T(4,128)(2,1)S(1)} %get-tuple-element.41), channel_id=1, source_target_pairs={{0,4},{4,0},{8,12},{12,8},{1,5},{5,1},{9,13},{13,9},{2,6},{6,2},{1... | collective-permute-start | bytes 79880 | tf_op jit(solution)/shard_map/ppermute | solution.py:59
  13.3 6.4 %collective-permute-start.4 = (bf16[4,3328]{1,0:T(4,128)(2,1)S(1)}, bf16[4,3328]{1,0:T(4,128)(2,1)S(1)}, u32[]{:S(2)}, u32[]{:S(2)}) collective-permute-start(bf16[4,3328]{1,0:T(4,128)(2,1)S(1)} %get-tuple-element.42), channel_id=1, source_target_pairs={{0,8},{4,12},{8,0},{12,4},{1,9},{5,13},{9,1},{13,5},{2,10},{6,14},... | collective-permute-start | bytes 79880 | tf_op jit(solution)/shard_map/ppermute | solution.py:59
  13.7 6.1 %collective-permute-start.5 = (bf16[4,3328]{1,0:T(4,128)(2,1)S(1)}, bf16[4,3328]{1,0:T(4,128)(2,1)S(1)}, u32[]{:S(2)}, u32[]{:S(2)}) collective-permute-start(bf16[4,3328]{1,0:T(4,128)(2,1)S(1)} %get-tuple-element.43), channel_id=1, source_target_pairs={{0,12},{4,8},{8,4},{12,0},{1,13},{5,9},{9,5},{13,1},{2,14},{6,10},... | collective-permute-start | bytes 79880 | tf_op jit(solution)/shard_map/ppermute | solution.py:59
  18.4 10.1 %copy-start.1 = (bf16[2048,1024]{1,0:T(8,128)(2,1)S(1)}, bf16[2048,1024]{1,0:T(8,128)(2,1)}, u32[]{:S(2)}) copy-start(bf16[2048,1024]{1,0:T(8,128)(2,1)} %refs_4_.3) | copy-start | bytes 12582916
  20.2 6.2 %collective-permute-start.8 = (bf16[4,2048]{1,0:T(4,128)(2,1)S(1)}, bf16[4,2048]{1,0:T(4,128)(2,1)S(1)}, u32[]{:S(2)}, u32[]{:S(2)}) collective-permute-start(bf16[4,2048]{1,0:T(4,128)(2,1)S(1)} %get-tuple-element.49.refs_0_), channel_id=1, source_target_pairs={{0,12},{4,8},{8,4},{12,0},{1,13},{5,9},{9,5},{13,1},{2,14},{6,10},... | collective-permute-start | bytes 49160 | tf_op jit(solution)/shard_map/ppermute | solution.py:59
  23.8 4.6 %collective-permute-start.7 = (bf16[4,2048]{1,0:T(4,128)(2,1)S(1)}, bf16[4,2048]{1,0:T(4,128)(2,1)S(1)}, u32[]{:S(2)}, u32[]{:S(2)}) collective-permute-start(bf16[4,2048]{1,0:T(4,128)(2,1)S(1)} %get-tuple-element.49.refs_0_), channel_id=1, source_target_pairs={{0,8},{4,12},{8,0},{12,4},{1,9},{5,13},{9,1},{13,5},{2,10},{6,14},... | collective-permute-start | bytes 49160 | tf_op jit(solution)/shard_map/ppermute | solution.py:59
  23.9 4.6 %collective-permute-start.6 = (bf16[4,2048]{1,0:T(4,128)(2,1)S(1)}, bf16[4,2048]{1,0:T(4,128)(2,1)S(1)}, u32[]{:S(2)}, u32[]{:S(2)}) collective-permute-start(bf16[4,2048]{1,0:T(4,128)(2,1)S(1)} %get-tuple-element.49.refs_0_), channel_id=1, source_target_pairs={{0,4},{4,0},{8,12},{12,8},{1,5},{5,1},{9,13},{13,9},{2,6},{6,2},{1... | collective-permute-start | bytes 49160 | tf_op jit(solution)/shard_map/ppermute | solution.py:59
  29.2 3.2 %collective-permute-start.9 = (bf16[4,1024]{1,0:T(4,128)(2,1)S(1)}, bf16[4,1024]{1,0:T(4,128)(2,1)S(1)}, u32[]{:S(2)}, u32[]{:S(2)}) collective-permute-start(bf16[4,1024]{1,0:T(4,128)(2,1)S(1)} %get-tuple-element.54), channel_id=1, source_target_pairs={{0,1},{1,0},{2,3},{3,2},{4,5},{5,4},{6,7},{7,6},{8,9},{9,8},{10,11... | collective-permute-start | bytes 24584 | tf_op jit(solution)/shard_map/ppermute | solution.py:59
  29.3 3.7 %collective-permute-start.10 = (bf16[4,1024]{1,0:T(4,128)(2,1)S(1)}, bf16[4,1024]{1,0:T(4,128)(2,1)S(1)}, u32[]{:S(2)}, u32[]{:S(2)}) collective-permute-start(bf16[4,1024]{1,0:T(4,128)(2,1)S(1)} %get-tuple-element.55), channel_id=1, source_target_pairs={{0,2},{1,3},{2,0},{3,1},{4,6},{5,7},{6,4},{7,5},{8,10},{9,11},{10,... | collective-permute-start | bytes 24584 | tf_op jit(solution)/shard_map/ppermute | solution.py:59
  30.9 3.1 %collective-permute-start.11 = (bf16[4,1024]{1,0:T(4,128)(2,1)S(1)}, bf16[4,1024]{1,0:T(4,128)(2,1)S(1)}, u32[]{:S(2)}, u32[]{:S(2)}) collective-permute-start(bf16[4,1024]{1,0:T(4,128)(2,1)S(1)} %get-tuple-element.56), channel_id=1, source_target_pairs={{0,3},{1,2},{2,1},{3,0},{4,7},{5,6},{6,5},{7,4},{8,11},{9,10},{10,... | collective-permute-start | bytes 24584 | tf_op jit(solution)/shard_map/ppermute | solution.py:59

commit v6 on v5

--- a/solution.py
+++ b/solution.py
@@ -49,6 +49,14 @@
             for j in range(count)
         ]
         got.append(lax.ppermute(blocks[step], ("kv", "tp"), pairs))
+    return got
+
+
+def exchange_round(block, axis, count):
+    got = []
+    for step in range(1, count):
+        pairs = [(i, (i + step) % count) for i in range(count)]
+        got.append(lax.ppermute(block, axis, pairs))
     return got
 
 
@@ -223,7 +231,7 @@
     store(first, jnp.dot(lhs, pair, preferred_element_type=F32))
 
 
-def mixer_body(props, groups, *refs):
+def mixer_body(props, groups, tap_count, *refs):
     own, *rest = refs
     count = len(rest) - 11
     others = rest[:count]
@@ -245,7 +253,6 @@
     summed[...] = (summed[...] * norm[:, 0:1]).astype(BF16).astype(F32)
     rows = summed[:, :conv]
     fresh[...] = rows
-    tap_count = 4
     value = early[...] + rows * taps[tap_count - 1 : tap_count, :]
     for k in range(1, props):
         value = value + pltpu.roll(rows * taps[tap_count - 1 - k : tap_count - k, :], k, 0)
@@ -372,12 +379,13 @@
     weight = refs[count]
     outs = refs[count + 2 : count + 2 + count]
     result, lhs = refs[-2:]
-    which = lax.bitwise_xor(lax.axis_index("kv"), lax.axis_index("tp"))
+    me, part = lax.axis_index("kv"), lax.axis_index("tp")
     product = jnp.dot(stack_rows(parts, lhs), weight[...], preferred_element_type=F32)
     for j in range(count):
         result[j, 0:4] = product[4 * j : 4 * j + 4]
     for step in range(count):
-        outs[step][...] = result[lax.bitwise_xor(which, step), 0:4].astype(BF16)
+        places = lax.rem(me - lax.bitwise_xor(part, step) + count, count)
+        outs[step][...] = result[places, 0:4].astype(BF16)
 
 
 def final_body(*refs):
@@ -485,7 +493,7 @@
     )
     sums = exchange([None] + partials, "kv", count)
     gated, fresh, act = call(
-        functools.partial(mixer_body, props, groups),
+        functools.partial(mixer_body, props, groups, convolution_tap_weight.shape[0]),
         [
             pltpu.VMEM((4, inner), BF16),
             pltpu.VMEM((ROWS, conv), F32),
@@ -497,11 +505,11 @@
         flops=20_000_000,
         scratch=[pltpu.VMEM((ROWS, total), F32), pltpu.VMEM((ROWS, inner), F32)],
     )
-    gathered = exchange([gated] * count, "kv", count)
+    gathered = exchange_round(gated, "kv", count)
     per = heads // groups
     half = per // 2
     pieces = [(g, at, at + half) for g in range(groups) for at in (0, half)]
-    first = 3 * len(pieces) // 4
+    first = len(pieces) // 4
     all_states = jax.ShapeDtypeStruct((1, props, heads, head_dim, size), F32)
 
     def scratch(number, *more):

time: 34.9 us -> 35.7 us (1.023)
  waiting for transfers between devices: 8.64 us -> 9.64 us
    ppermute x9 -> x6, starting transfers between devices: 10.8 us -> 6.31 us  [exchange(): got.append(lax.ppermute(blocks[step], axis, pairs))]
    ppermute x0 -> x3, starting transfers between devices: none -> 4.23 us  [exchange_round(): got.append(lax.ppermute(block, axis, pairs))]
    ppermute x0 -> x3, waiting for transfers between devices: none -> 3.67 us  [exchange_round(): got.append(lax.ppermute(block, axis, pairs))]
    ppermute x9 -> x6, waiting for transfers between devices: 3.7 us -> 1.02 us  [exchange(): got.append(lax.ppermute(blocks[step], axis, pairs))]
where the time goes in v6:
time: 35.7 us; the launch traced here: 35.4 us
  starting transfers between devices  16 us (45%)
  waiting for transfers between devices  9.64 us (27%)
  Pallas kernels  8.05 us (23%)
  between operations  1.62 us (5%)
    pallas_call x10, Pallas kernels, call(): pl.pallas_call(body, out_shape=outs, in_specs=specs, out_specs=out_specs...  8.05 us
    ppermute x6, starting transfers between devices, exchange(): got.append(lax.ppermute(blocks[step], axis, pairs))  6.31 us
    ppermute x3, starting transfers between devices, exchange_tokens(): got.append(lax.ppermute(blocks[step], ('kv', 'tp'), pairs))  5.43 us
    ppermute x3, waiting for transfers between devices, exchange_tokens(): got.append(lax.ppermute(blocks[step], ('kv', 'tp'), pairs))  4.94 us
    ppermute x3, starting transfers between devices, exchange_round(): got.append(lax.ppermute(block, axis, pairs))  4.23 us
    ppermute x3, waiting for transfers between devices, exchange_round(): got.append(lax.ppermute(block, axis, pairs))  3.67 us
    ppermute x6, waiting for transfers between devices, exchange(): got.append(lax.ppermute(blocks[step], axis, pairs))  1.02 us
  transfers between devices with their start and end apart: 12, of which 5 were waited for; matrix products, arithmetic and copies ran while one was open for 0% of the time, Pallas kernels for 12%

profile of v6, /device:TPU:0, one launch (start us, length us, event | category | flops | bytes accessed | tf_op | source)
XLA Modules:
  0.0 35.4 jit_solution(72505649177262083)
XLA Ops:
  0.6 0.8 %shard_map.184 = (bf16[3,1024]{1,0:T(4,128)(2,1)S(1)}, bf16[3,1024]{1,0:T(4,128)(2,1)S(1)}, bf16[3,1024]{1,0:T(4,128)(2,1)S(1)}, bf16[3,1024]{1,0:T(4,128)(2,1)S(1)}) custom-call(bf16[1,3,4096]{2,1,0:T(4,128)(2,1)} %tokens.3), custom_call_target="tpu_custom_call" | custom-call | tf_op jit(solution)/shard_map/pallas_call | solution.py:31
  1.4 0.0 copy-start.2
  1.4 0.0 copy-start.3
  1.5 0.0 copy-start.4
  1.5 0.0 copy-start.5
  1.5 0.0 copy-start.9
  1.5 2.6 %collective-permute-start = (bf16[3,1024]{1,0:T(4,128)(2,1)S(1)}, bf16[3,1024]{1,0:T(4,128)(2,1)S(1)}, u32[]{:S(2)}, u32[]{:S(2)}) collective-permute-start(bf16[3,1024]{1,0:T(4,128)(2,1)S(1)} %get-tuple-element.37), channel_id=1, source_target_pairs={{0,5},{1,4},{2,7},{3,6},{4,1},{5,0},{6,3},{7,2},{8,13},{9,12},{10,... | collective-permute-start | bytes 18440 | tf_op jit(solution)/shard_map/ppermute | solution.py:51
  4.1 2.9 %collective-permute-start.1 = (bf16[3,1024]{1,0:T(4,128)(2,1)S(1)}, bf16[3,1024]{1,0:T(4,128)(2,1)S(1)}, u32[]{:S(2)}, u32[]{:S(2)}) collective-permute-start(bf16[3,1024]{1,0:T(4,128)(2,1)S(1)} %get-tuple-element.38), channel_id=1, source_target_pairs={{0,9},{1,8},{2,11},{3,10},{4,13},{5,12},{6,15},{7,14},{8,1},{9,0},... | collective-permute-start | bytes 18440 | tf_op jit(solution)/shard_map/ppermute | solution.py:51
  6.9 0.0 collective-permute-start.2
  6.9 0.0 collective-permute-done.refs_1_
  6.9 1.4 %collective-permute-done.1.refs_2_ = bf16[3,1024]{1,0:T(4,128)(2,1)S(1)} collective-permute-done((bf16[3,1024]{1,0:T(4,128)(2,1)S(1)}, bf16[3,1024]{1,0:T(4,128)(2,1)S(1)}, u32[]{:S(2)}, u32[]{:S(2)}) %collective-permute-start.1) | collective-permute-done | bytes 6176 | tf_op jit(solution)/shard_map/ppermute | solution.py:51
  8.3 3.6 %collective-permute-done.2.refs_3_ = bf16[3,1024]{1,0:T(4,128)(2,1)S(1)} collective-permute-done((bf16[3,1024]{1,0:T(4,128)(2,1)S(1)}, bf16[3,1024]{1,0:T(4,128)(2,1)S(1)}, u32[]{:S(2)}, u32[]{:S(2)}) %collective-permute-start.2) | collective-permute-done | bytes 6176 | tf_op jit(solution)/shard_map/ppermute | solution.py:51
  11.9 0.0 copy-done.2
  11.9 0.0 copy-done.3
  11.9 0.0 copy-done.4
  11.9 0.0 copy-done.5
  11.9 0.0 copy-done.9
  11.9 0.0 copy-start.15
  11.9 0.0 copy-start
  11.9 0.0 copy-start.8
  11.9 0.0 copy-start.10
  12.0 0.0 copy-start.6
  12.0 0.0 copy-start.7
  12.0 0.0 copy-start.12
  12.0 0.0 copy-start.13
  12.0 0.0 copy-start.14
  12.0 0.0 copy-start.11
  12.0 1.3 %shard_map.186 = (f32[4,3328]{1,0:T(4,128)S(1)}, bf16[4,3328]{1,0:T(4,128)(2,1)S(1)}, bf16[4,3328]{1,0:T(4,128)(2,1)S(1)}, bf16[4,3328]{1,0:T(4,128)(2,1)S(1)}) custom-call(bf16[3,1024]{1,0:T(4,128)(2,1)S(1)} %get-tuple-element.36.refs_0_, bf16[3,1024]{1,0:T(4,128)(2,1)S(1)} %collective-permute-done.refs_1_, ...), custom_call_target="tpu_custom_call" | custom-call | flops 200000000 | tf_op jit(solution)/shard_map/pallas_call | solution.py:31
  13.3 0.0 collective-permute-start.3
  13.3 0.4 collective-permute-start.4
  13.7 4.0 %collective-permute-start.5 = (bf16[4,3328]{1,0:T(4,128)(2,1)S(1)}, bf16[4,3328]{1,0:T(4,128)(2,1)S(1)}, u32[]{:S(2)}, u32[]{:S(2)}) collective-permute-start(bf16[4,3328]{1,0:T(4,128)(2,1)S(1)} %get-tuple-element.43), channel_id=1, source_target_pairs={{0,12},{4,8},{8,4},{12,0},{1,13},{5,9},{9,5},{13,1},{2,14},{6,10},... | collective-permute-start | bytes 79880 | tf_op jit(solution)/shard_map/ppermute | solution.py:67
  18.4 0.0 copy-done.15
  18.4 0.0 copy-done
  18.4 0.0 copy-done.8
  18.4 0.0 copy-start.1
  18.4 0.4 %shard_map.188 = (bf16[256,2048]{1,0:T(8,128)(2,1)S(1)}, f32[8,2304]{1,0:T(8,128)S(1)}, f32[8,2304]{1,0:T(8,128)S(1)}) custom-call(s32[1]{0:T(128)S(6)} %copy.33.accepted, f32[1,3,32,64,64]{4,3,2,1,0:T(8,128)S(1)} %copy-done, bf16[1,6,2,1152]{3,2,1,0:T(2,128)(2,1)S(1)} %copy-done.8, bf16[4,2,1152]{2,1,0:T(2,128)(2,1)S(1)} %copy-done.10), custom_call_target="tpu_custom_call" | custom-call | flops 20000000 | tf_op jit(solution)/shard_map/pallas_call | solution.py:31
  18.8 0.0 copy-done.6
  18.9 0.0 copy-done.7
  18.9 0.0 copy-done.12
  18.9 0.0 copy-done.13
  18.9 0.0 copy-done.14
  18.9 0.9 %shard_map.187 = (f32[5,8,2048]{2,1,0:T(8,128)S(1)}, f32[8,32]{1,0:T(8,128)S(1)}, f32[8,128]{1,0:T(8,128)S(1)}) custom-call(s32[1]{0:T(128)S(6)} %copy.33.accepted, bf16[1,3,4096]{2,1,0:T(4,128)(2,1)S(1)} %copy-done.7, f32[1,4096]{1,0:T(1,128)S(1)} %bitcast.11, bf16[32,4096]{1,0:T(8,128)(2,1)S(1)} %bitcast.9, f32[1,32]{1,0:T(1,128)S(1)} %bitcast.14, ...), custom_call_target="tpu_custom_call" | custom-call | flops 20000000 | tf_op jit(solution)/shard_map/pallas_call | solution.py:31
  19.8 0.0 collective-permute-done.3.refs_1_
  19.8 0.0 collective-permute-done.4.refs_2_
  19.8 0.0 collective-permute-done.5.refs_3_
  19.8 0.0 copy-done.11
  19.8 0.4 %shard_map.189 = (bf16[4,2048]{1,0:T(4,128)(2,1)S(1)}, f32[8,2304]{1,0:T(8,128)S(1)}, f32[8,2304]{1,0:T(8,128)S(1)}) custom-call(f32[4,3328]{1,0:T(4,128)S(1)} %get-tuple-element.40.refs_0_, bf16[4,3328]{1,0:T(4,128)(2,1)S(1)} %collective-permute-done.3.refs_1_, bf16[4,3328]{1,0:T(4,128)(2,1)S(1)} %collective-permute-done.4.refs_2_, ...), custom_call_target="tpu_custom_call" | custom-call | flops 20000000 | tf_op jit(solution)/shard_map/pallas_call | solution.py:31
  20.2 3.6 %collective-permute-start.8 = (bf16[4,2048]{1,0:T(4,128)(2,1)S(1)}, bf16[4,2048]{1,0:T(4,128)(2,1)S(1)}, u32[]{:S(2)}, u32[]{:S(2)}) collective-permute-start(bf16[4,2048]{1,0:T(4,128)(2,1)S(1)} %get-tuple-element.49.refs_0_), channel_id=1, source_target_pairs={{0,12},{4,0},{8,4},{12,8},{1,13},{5,1},{9,5},{13,9},{2,14},{6,2},{... | collective-permute-start | bytes 49160 | tf_op jit(solution)/shard_map/ppermute | solution.py:59
  23.8 0.0 collective-permute-start.7
  23.8 0.6 %collective-permute-start.6 = (bf16[4,2048]{1,0:T(4,128)(2,1)S(1)}, bf16[4,2048]{1,0:T(4,128)(2,1)S(1)}, u32[]{:S(2)}, u32[]{:S(2)}) collective-permute-start(bf16[4,2048]{1,0:T(4,128)(2,1)S(1)} %get-tuple-element.49.refs_0_), channel_id=1, source_target_pairs={{0,4},{4,8},{8,12},{12,0},{1,5},{5,9},{9,13},{13,1},{2,6},{6,10},{... | collective-permute-start | bytes 49160 | tf_op jit(solution)/shard_map/ppermute | solution.py:59
  24.5 1.2 %shard_map.190 = (f32[1,3,32,64,64]{4,3,2,1,0:T(8,128)}, f32[8,128]{1,0:T(8,128)S(1)}) custom-call(s32[1]{0:T(128)S(6)} %copy.33.accepted, f32[1,3,32,64,64]{4,3,2,1,0:T(8,128)S(1)} %copy-done, f32[8,32]{1,0:T(8,128)S(1)} %get-tuple-element.50.small, f32[8,2304]{1,0:T(8,128)S(1)} %get-tuple-element.51.act, f32[5,8,2048]{2,1,0:T(8,128)S(1)} %get-tuple-element.45.refs_5_.coef), custom_call_target="tpu_custom_call" | custom-call | flops 30000000 | tf_op jit(solution)/shard_map/pallas_call | solution.py:31
  25.7 0.0 collective-permute-done.8.refs_3_
  25.7 2.8 %collective-permute-done.7.refs_2_ = bf16[4,2048]{1,0:T(4,128)(2,1)S(1)} collective-permute-done((bf16[4,2048]{1,0:T(4,128)(2,1)S(1)}, bf16[4,2048]{1,0:T(4,128)(2,1)S(1)}, u32[]{:S(2)}, u32[]{:S(2)}) %collective-permute-start.7) | collective-permute-done | bytes 16416 | tf_op jit(solution)/shard_map/ppermute | solution.py:59
  28.5 0.9 %collective-permute-done.6.refs_1_ = bf16[4,2048]{1,0:T(4,128)(2,1)S(1)} collective-permute-done((bf16[4,2048]{1,0:T(4,128)(2,1)S(1)}, bf16[4,2048]{1,0:T(4,128)(2,1)S(1)}, u32[]{:S(2)}, u32[]{:S(2)}) %collective-permute-start.6) | collective-permute-done | bytes 16416 | tf_op jit(solution)/shard_map/ppermute | solution.py:59
  29.4 0.0 copy-done.1
  29.4 0.7 %shard_map.191 = (bf16[4,1024]{1,0:T(4,128)(2,1)S(1)}, bf16[4,1024]{1,0:T(4,128)(2,1)S(1)}, bf16[4,1024]{1,0:T(4,128)(2,1)S(1)}, bf16[4,1024]{1,0:T(4,128)(2,1)S(1)}) custom-call(bf16[4,2048]{1,0:T(4,128)(2,1)S(1)} %get-tuple-element.49.refs_0_, bf16[4,2048]{1,0:T(4,128)(2,1)S(1)} %collective-permute-done.6.refs_1_, ...), custom_call_target="tpu_custom_call" | custom-call | flops 100000000 | tf_op jit(solution)/shard_map/pallas_call | solution.py:31
  30.1 0.1 collective-permute-start.9
  30.1 1.6 %collective-permute-start.10 = (bf16[4,1024]{1,0:T(4,128)(2,1)S(1)}, bf16[4,1024]{1,0:T(4,128)(2,1)S(1)}, u32[]{:S(2)}, u32[]{:S(2)}) collective-permute-start(bf16[4,1024]{1,0:T(4,128)(2,1)S(1)} %get-tuple-element.55), channel_id=1, source_target_pairs={{0,2},{1,3},{2,0},{3,1},{4,6},{5,7},{6,4},{7,5},{8,10},{9,11},{10,... | collective-permute-start | bytes 24584 | tf_op jit(solution)/shard_map/ppermute | solution.py:67
  31.7 0.3 collective-permute-start.11
  32.0 1.8 %shard_map.193 = (f32[1,3,32,64,64]{4,3,2,1,0:T(8,128)}, bf16[1,6,2,1152]{3,2,1,0:T(2,128)(2,1)}) custom-call(s32[1]{0:T(128)S(6)} %copy.33.accepted, f32[1,3,32,64,64]{4,3,2,1,0:T(8,128)S(1)} %copy-done, f32[8,32]{1,0:T(8,128)S(1)} %get-tuple-element.50.small, f32[8,2304]{1,0:T(8,128)S(1)} %get-tuple-element.51.act, ...), custom_call_target="tpu_custom_call", output_to_operand_aliasing={{0}: (7, {})} | custom-call | flops 30000000 | tf_op jit(solution)/shard_map/pallas_call | solution.py:31
  33.8 0.0 collective-permute-done.9.refs_1_
  33.8 0.0 collective-permute-done.10.refs_2_
  33.9 0.9 %collective-permute-done.11.refs_3_ = bf16[4,1024]{1,0:T(4,128)(2,1)S(1)} collective-permute-done((bf16[4,1024]{1,0:T(4,128)(2,1)S(1)}, bf16[4,1024]{1,0:T(4,128)(2,1)S(1)}, u32[]{:S(2)}, u32[]{:S(2)}) %collective-permute-start.11) | collective-permute-done | bytes 8224 | tf_op jit(solution)/shard_map/ppermute | solution.py:67
  34.8 0.6 %shard_map.192 = bf16[1,3,1024]{2,1,0:T(4,128)(2,1)} custom-call(bf16[4,1024]{1,0:T(4,128)(2,1)S(1)} %get-tuple-element.53.refs_0_, bf16[4,1024]{1,0:T(4,128)(2,1)S(1)} %collective-permute-done.9.refs_1_, bf16[4,1024]{1,0:T(4,128)(2,1)S(1)} %collective-permute-done.10.refs_2_, bf16[4,1024]{1,0:T(4,128)(2,1)S(1)} %collective-permute-done.11.refs_3_), custom_call_target="tpu_custom_call" | custom-call | tf_op jit(solution)/shard_map/pallas_call | solution.py:31
  (3 shorter events, 0.0 us)
Async XLA Ops:
  1.4 10.4 %copy-start.2 = (bf16[1024,2048]{1,0:T(8,128)(2,1)S(1)}, bf16[1024,2048]{1,0:T(8,128)(2,1)}, u32[]{:S(2)}) copy-start(bf16[1024,2048]{1,0:T(8,128)(2,1)} %refs_4_.2) | copy-start | bytes 12582916
  1.4 10.4 %copy-start.3 = (bf16[1024,2048]{1,0:T(8,128)(2,1)S(1)}, bf16[1024,2048]{1,0:T(8,128)(2,1)}, u32[]{:S(2)}) copy-start(bf16[1024,2048]{1,0:T(8,128)(2,1)} %refs_7_.1) | copy-start | bytes 12582916
  1.5 10.4 %copy-start.4 = (bf16[1024,128]{1,0:T(8,128)(2,1)S(1)}, bf16[1024,128]{1,0:T(8,128)(2,1)}, u32[]{:S(2)}) copy-start(bf16[1024,128]{1,0:T(8,128)(2,1)} %refs_5_.1) | copy-start | bytes 786436
  1.5 10.4 %copy-start.5 = (bf16[1024,128]{1,0:T(8,128)(2,1)S(1)}, bf16[1024,128]{1,0:T(8,128)(2,1)}, u32[]{:S(2)}) copy-start(bf16[1024,128]{1,0:T(8,128)(2,1)} %refs_6_.1) | copy-start | bytes 786436
  1.5 10.4 %copy-start.9 = (f32[4096]{0:T(1024)S(1)}, f32[4096]{0:T(1024)}, u32[]{:S(2)}) copy-start(f32[4096]{0:T(1024)} %param.18) | copy-start | bytes 49156
  1.5 5.4 %collective-permute-start = (bf16[3,1024]{1,0:T(4,128)(2,1)S(1)}, bf16[3,1024]{1,0:T(4,128)(2,1)S(1)}, u32[]{:S(2)}, u32[]{:S(2)}) collective-permute-start(bf16[3,1024]{1,0:T(4,128)(2,1)S(1)} %get-tuple-element.37), channel_id=1, source_target_pairs={{0,5},{1,4},{2,7},{3,6},{4,1},{5,0},{6,3},{7,2},{8,13},{9,12},{10,... | collective-permute-start | bytes 18440 | tf_op jit(solution)/shard_map/ppermute | solution.py:51
  4.1 4.3 %collective-permute-start.1 = (bf16[3,1024]{1,0:T(4,128)(2,1)S(1)}, bf16[3,1024]{1,0:T(4,128)(2,1)S(1)}, u32[]{:S(2)}, u32[]{:S(2)}) collective-permute-start(bf16[3,1024]{1,0:T(4,128)(2,1)S(1)} %get-tuple-element.38), channel_id=1, source_target_pairs={{0,9},{1,8},{2,11},{3,10},{4,13},{5,12},{6,15},{7,14},{8,1},{9,0},... | collective-permute-start | bytes 18440 | tf_op jit(solution)/shard_map/ppermute | solution.py:51
  6.9 4.9 %collective-permute-start.2 = (bf16[3,1024]{1,0:T(4,128)(2,1)S(1)}, bf16[3,1024]{1,0:T(4,128)(2,1)S(1)}, u32[]{:S(2)}, u32[]{:S(2)}) collective-permute-start(bf16[3,1024]{1,0:T(4,128)(2,1)S(1)} %get-tuple-element.39), channel_id=1, source_target_pairs={{0,13},{1,12},{2,15},{3,14},{4,9},{5,8},{6,11},{7,10},{8,5},{9,4},... | collective-permute-start | bytes 18440 | tf_op jit(solution)/shard_map/ppermute | solution.py:51
  11.9 6.5 %copy-start.15 = (f32[1,3,32]{2,0,1:T(1,128)S(1)}, f32[1,3,32]{2,0,1:T(1,128)}, u32[]{:S(2)}) copy-start(f32[1,3,32]{2,0,1:T(1,128)} %param.31) | copy-start | bytes 1156
  11.9 6.5 %copy-start = (f32[1,3,32,64,64]{4,3,2,1,0:T(8,128)S(1)}, f32[1,3,32,64,64]{4,3,2,1,0:T(8,128)}, u32[]{:S(2)}) copy-start(f32[1,3,32,64,64]{4,3,2,1,0:T(8,128)} %start.3) | copy-start | bytes 4718596
  11.9 6.5 %copy-start.8 = (bf16[1,6,2,1152]{3,2,1,0:T(2,128)(2,1)S(1)}, bf16[1,6,2,1152]{3,2,1,0:T(2,128)(2,1)}, u32[]{:S(2)}) copy-start(bf16[1,6,2,1152]{3,2,1,0:T(2,128)(2,1)} %refs_1_.1) | copy-start | bytes 82948
  11.9 6.5 %copy-start.10 = (bf16[4,2,1152]{2,1,0:T(2,128)(2,1)S(1)}, bf16[4,2,1152]{2,1,0:T(2,128)(2,1)}, u32[]{:S(2)}) copy-start(bf16[4,2,1152]{2,1,0:T(2,128)(2,1)} %taps.1) | copy-start | bytes 55300
  12.0 6.9 %copy-start.6 = (bf16[4096,32]{0,1:T(8,128)(2,1)S(1)}, bf16[4096,32]{0,1:T(8,128)(2,1)}, u32[]{:S(2)}) copy-start(bf16[4096,32]{0,1:T(8,128)(2,1)} %param.23) | copy-start | bytes 786436
  12.0 6.9 %copy-start.7 = (bf16[1,3,4096]{2,1,0:T(4,128)(2,1)S(1)}, bf16[1,3,4096]{2,1,0:T(4,128)(2,1)}, u32[]{:S(2)}) copy-start(bf16[1,3,4096]{2,1,0:T(4,128)(2,1)} %tokens.3) | copy-start | bytes 73732
  12.0 6.9 %copy-start.12 = (f32[32]{0:T(128)S(1)}, f32[32]{0:T(128)}, u32[]{:S(2)}) copy-start(f32[32]{0:T(128)} %param.24) | copy-start | bytes 388
  12.0 6.9 %copy-start.13 = (f32[32]{0:T(128)S(1)}, f32[32]{0:T(128)}, u32[]{:S(2)}) copy-start(f32[32]{0:T(128)} %param.25) | copy-start | bytes 388
  12.0 6.9 %copy-start.14 = (f32[32]{0:T(128)S(1)}, f32[32]{0:T(128)}, u32[]{:S(2)}) copy-start(f32[32]{0:T(128)} %param.26) | copy-start | bytes 388
  12.0 7.8 %copy-start.11 = (f32[2048]{0:T(1024)S(1)}, f32[2048]{0:T(1024)}, u32[]{:S(2)}) copy-start(f32[2048]{0:T(1024)} %param.32) | copy-start | bytes 24580
  13.3 6.4 %collective-permute-start.3 = (bf16[4,3328]{1,0:T(4,128)(2,1)S(1)}, bf16[4,3328]{1,0:T(4,128)(2,1)S(1)}, u32[]{:S(2)}, u32[]{:S(2)}) collective-permute-start(bf16[4,3328]{1,0:T(4,128)(2,1)S(1)} %get-tuple-element.41), channel_id=1, source_target_pairs={{0,4},{4,0},{8,12},{12,8},{1,5},{5,1},{9,13},{13,9},{2,6},{6,2},{1... | collective-permute-start | bytes 79880 | tf_op jit(solution)/shard_map/ppermute | solution.py:67
  13.3 6.4 %collective-permute-start.4 = (bf16[4,3328]{1,0:T(4,128)(2,1)S(1)}, bf16[4,3328]{1,0:T(4,128)(2,1)S(1)}, u32[]{:S(2)}, u32[]{:S(2)}) collective-permute-start(bf16[4,3328]{1,0:T(4,128)(2,1)S(1)} %get-tuple-element.42), channel_id=1, source_target_pairs={{0,8},{4,12},{8,0},{12,4},{1,9},{5,13},{9,1},{13,5},{2,10},{6,14},... | collective-permute-start | bytes 79880 | tf_op jit(solution)/shard_map/ppermute | solution.py:67
  13.7 6.1 %collective-permute-start.5 = (bf16[4,3328]{1,0:T(4,128)(2,1)S(1)}, bf16[4,3328]{1,0:T(4,128)(2,1)S(1)}, u32[]{:S(2)}, u32[]{:S(2)}) collective-permute-start(bf16[4,3328]{1,0:T(4,128)(2,1)S(1)} %get-tuple-element.43), channel_id=1, source_target_pairs={{0,12},{4,8},{8,4},{12,0},{1,13},{5,9},{9,5},{13,1},{2,14},{6,10},... | collective-permute-start | bytes 79880 | tf_op jit(solution)/shard_map/ppermute | solution.py:67
  18.4 11.0 %copy-start.1 = (bf16[2048,1024]{1,0:T(8,128)(2,1)S(1)}, bf16[2048,1024]{1,0:T(8,128)(2,1)}, u32[]{:S(2)}) copy-start(bf16[2048,1024]{1,0:T(8,128)(2,1)} %refs_4_.3) | copy-start | bytes 12582916
  20.2 5.5 %collective-permute-start.8 = (bf16[4,2048]{1,0:T(4,128)(2,1)S(1)}, bf16[4,2048]{1,0:T(4,128)(2,1)S(1)}, u32[]{:S(2)}, u32[]{:S(2)}) collective-permute-start(bf16[4,2048]{1,0:T(4,128)(2,1)S(1)} %get-tuple-element.49.refs_0_), channel_id=1, source_target_pairs={{0,12},{4,0},{8,4},{12,8},{1,13},{5,1},{9,5},{13,9},{2,14},{6,2},{... | collective-permute-start | bytes 49160 | tf_op jit(solution)/shard_map/ppermute | solution.py:59
  23.8 4.6 %collective-permute-start.7 = (bf16[4,2048]{1,0:T(4,128)(2,1)S(1)}, bf16[4,2048]{1,0:T(4,128)(2,1)S(1)}, u32[]{:S(2)}, u32[]{:S(2)}) collective-permute-start(bf16[4,2048]{1,0:T(4,128)(2,1)S(1)} %get-tuple-element.49.refs_0_), channel_id=1, source_target_pairs={{0,8},{4,12},{8,0},{12,4},{1,9},{5,13},{9,1},{13,5},{2,10},{6,14},... | collective-permute-start | bytes 49160 | tf_op jit(solution)/shard_map/ppermute | solution.py:59
  23.8 5.5 %collective-permute-start.6 = (bf16[4,2048]{1,0:T(4,128)(2,1)S(1)}, bf16[4,2048]{1,0:T(4,128)(2,1)S(1)}, u32[]{:S(2)}, u32[]{:S(2)}) collective-permute-start(bf16[4,2048]{1,0:T(4,128)(2,1)S(1)} %get-tuple-element.49.refs_0_), channel_id=1, source_target_pairs={{0,4},{4,8},{8,12},{12,0},{1,5},{5,9},{9,13},{13,1},{2,6},{6,10},{... | collective-permute-start | bytes 49160 | tf_op jit(solution)/shard_map/ppermute | solution.py:59
  30.1 3.7 %collective-permute-start.9 = (bf16[4,1024]{1,0:T(4,128)(2,1)S(1)}, bf16[4,1024]{1,0:T(4,128)(2,1)S(1)}, u32[]{:S(2)}, u32[]{:S(2)}) collective-permute-start(bf16[4,1024]{1,0:T(4,128)(2,1)S(1)} %get-tuple-element.54), channel_id=1, source_target_pairs={{0,1},{1,0},{2,3},{3,2},{4,5},{5,4},{6,7},{7,6},{8,9},{9,8},{10,11... | collective-permute-start | bytes 24584 | tf_op jit(solution)/shard_map/ppermute | solution.py:67
  30.1 3.7 %collective-permute-start.10 = (bf16[4,1024]{1,0:T(4,128)(2,1)S(1)}, bf16[4,1024]{1,0:T(4,128)(2,1)S(1)}, u32[]{:S(2)}, u32[]{:S(2)}) collective-permute-start(bf16[4,1024]{1,0:T(4,128)(2,1)S(1)} %get-tuple-element.55), channel_id=1, source_target_pairs={{0,2},{1,3},{2,0},{3,1},{4,6},{5,7},{6,4},{7,5},{8,10},{9,11},{10,... | collective-permute-start | bytes 24584 | tf_op jit(solution)/shard_map/ppermute | solution.py:67
  31.7 3.1 %collective-permute-start.11 = (bf16[4,1024]{1,0:T(4,128)(2,1)S(1)}, bf16[4,1024]{1,0:T(4,128)(2,1)S(1)}, u32[]{:S(2)}, u32[]{:S(2)}) collective-permute-start(bf16[4,1024]{1,0:T(4,128)(2,1)S(1)} %get-tuple-element.56), channel_id=1, source_target_pairs={{0,3},{1,2},{2,1},{3,0},{4,7},{5,6},{6,5},{7,4},{8,11},{9,10},{10,... | collective-permute-start | bytes 24584 | tf_op jit(solution)/shard_map/ppermute | solution.py:67

commit v7 on v6

--- a/solution.py
+++ b/solution.py
@@ -295,7 +295,11 @@
         mean = jnp.sum(part * part, axis=1, keepdims=True) * (1.0 / per)
         pieces.append(part * lax.rsqrt(mean + epsilon) * gain[:, at])
     norms[...] = jnp.concatenate(pieces, axis=1)
-    gated[...] = norms[0:4].astype(BF16)
+    wide = gated.shape[1]
+    rest = inner - wide
+    for r in range(props):
+        norms[3:4, r * rest : (r + 1) * rest] = norms[r : r + 1, wide:]
+    gated[...] = norms[0:4, :wide].astype(BF16)
 
 
 def states_body(props, groups, pieces, accepted, start, small, act, coef, *refs):
@@ -374,13 +378,22 @@
         copy.wait()
 
 
-def output_body(count, *refs):
+def output_body(count, props, *refs):
     parts = refs[:count]
     weight = refs[count]
     outs = refs[count + 2 : count + 2 + count]
     result, lhs = refs[-2:]
     me, part = lax.axis_index("kv"), lax.axis_index("tp")
-    product = jnp.dot(stack_rows(parts, lhs), weight[...], preferred_element_type=F32)
+    wide = parts[0].shape[1]
+    rest = lhs.shape[1] - wide
+    lhs[...] = jnp.zeros_like(lhs)
+    for j, block in enumerate(parts):
+        rows = block[...].astype(F32)
+        lhs[4 * j : 4 * j + props, :wide] = rows[0:props]
+        for r in range(props):
+            at = 4 * j + r
+            lhs[at : at + 1, wide:] = rows[3:4, r * rest : (r + 1) * rest]
+    product = jnp.dot(lhs[...].astype(BF16), weight[...], preferred_element_type=F32)
     for j in range(count):
         result[j, 0:4] = product[4 * j : 4 * j + 4]
     for step in range(count):
@@ -495,7 +508,7 @@
     gated, fresh, act = call(
         functools.partial(mixer_body, props, groups, convolution_tap_weight.shape[0]),
         [
-            pltpu.VMEM((4, inner), BF16),
+            pltpu.VMEM((4, packed_width(props, inner)), BF16),
             pltpu.VMEM((ROWS, conv), F32),
             pltpu.VMEM((ROWS, conv), F32),
         ],
@@ -540,7 +553,7 @@
         aliases={7: 0},
     )
     blocks = call(
-        functools.partial(output_body, count),
+        functools.partial(output_body, count, props),
         [pltpu.VMEM((4, out_cols), BF16)] * count,
         [vmem(v) for v in [gated] + gathered + [output_projection_matrix, flag]],
         [VMEM_SPEC] * (count + 2),

time: 35.7 us -> 35.6 us (level)
  no operation moved by 1% of the time
where the time goes in v7:
time: 35.6 us; the launch traced here: 35.3 us
  starting transfers between devices  16 us (45%)
  waiting for transfers between devices  9.6 us (27%)
  Pallas kernels  8.06 us (23%)
  between operations  1.62 us (5%)
    pallas_call x10, Pallas kernels, call(): pl.pallas_call(body, out_shape=outs, in_specs=specs, out_specs=out_specs...  8.06 us
    ppermute x6, starting transfers between devices, exchange(): got.append(lax.ppermute(blocks[step], axis, pairs))  6.31 us
    ppermute x3, starting transfers between devices, exchange_tokens(): got.append(lax.ppermute(blocks[step], ('kv', 'tp'), pairs))  5.43 us
    ppermute x3, waiting for transfers between devices, exchange_tokens(): got.append(lax.ppermute(blocks[step], ('kv', 'tp'), pairs))  4.94 us
    ppermute x3, starting transfers between devices, exchange_round(): got.append(lax.ppermute(block, axis, pairs))  4.23 us
    ppermute x3, waiting for transfers between devices, exchange_round(): got.append(lax.ppermute(block, axis, pairs))  3.63 us
    ppermute x6, waiting for transfers between devices, exchange(): got.append(lax.ppermute(blocks[step], axis, pairs))  1.02 us
  transfers between devices with their start and end apart: 12, of which 5 were waited for; matrix products, arithmetic and copies ran while one was open for 0% of the time, Pallas kernels for 12%

profile of v7, /device:TPU:0, one launch (start us, length us, event | category | flops | bytes accessed | tf_op | source)
XLA Modules:
  0.0 35.3 jit_solution(7315231071775716397)
XLA Ops:
  0.6 0.8 %shard_map.184 = (bf16[3,1024]{1,0:T(4,128)(2,1)S(1)}, bf16[3,1024]{1,0:T(4,128)(2,1)S(1)}, bf16[3,1024]{1,0:T(4,128)(2,1)S(1)}, bf16[3,1024]{1,0:T(4,128)(2,1)S(1)}) custom-call(bf16[1,3,4096]{2,1,0:T(4,128)(2,1)} %tokens.3), custom_call_target="tpu_custom_call" | custom-call | tf_op jit(solution)/shard_map/pallas_call | solution.py:31
  1.4 0.0 copy-start.2
  1.4 0.0 copy-start.3
  1.5 0.0 copy-start.4
  1.5 0.0 copy-start.5
  1.5 0.0 copy-start.9
  1.5 2.6 %collective-permute-start = (bf16[3,1024]{1,0:T(4,128)(2,1)S(1)}, bf16[3,1024]{1,0:T(4,128)(2,1)S(1)}, u32[]{:S(2)}, u32[]{:S(2)}) collective-permute-start(bf16[3,1024]{1,0:T(4,128)(2,1)S(1)} %get-tuple-element.37), channel_id=1, source_target_pairs={{0,5},{1,4},{2,7},{3,6},{4,1},{5,0},{6,3},{7,2},{8,13},{9,12},{10,... | collective-permute-start | bytes 18440 | tf_op jit(solution)/shard_map/ppermute | solution.py:51
  4.1 2.9 %collective-permute-start.1 = (bf16[3,1024]{1,0:T(4,128)(2,1)S(1)}, bf16[3,1024]{1,0:T(4,128)(2,1)S(1)}, u32[]{:S(2)}, u32[]{:S(2)}) collective-permute-start(bf16[3,1024]{1,0:T(4,128)(2,1)S(1)} %get-tuple-element.38), channel_id=1, source_target_pairs={{0,9},{1,8},{2,11},{3,10},{4,13},{5,12},{6,15},{7,14},{8,1},{9,0},... | collective-permute-start | bytes 18440 | tf_op jit(solution)/shard_map/ppermute | solution.py:51
  6.9 0.0 collective-permute-start.2
  6.9 0.0 collective-permute-done.refs_1_
  6.9 1.4 %collective-permute-done.1.refs_2_ = bf16[3,1024]{1,0:T(4,128)(2,1)S(1)} collective-permute-done((bf16[3,1024]{1,0:T(4,128)(2,1)S(1)}, bf16[3,1024]{1,0:T(4,128)(2,1)S(1)}, u32[]{:S(2)}, u32[]{:S(2)}) %collective-permute-start.1) | collective-permute-done | bytes 6176 | tf_op jit(solution)/shard_map/ppermute | solution.py:51
  8.3 3.6 %collective-permute-done.2.refs_3_ = bf16[3,1024]{1,0:T(4,128)(2,1)S(1)} collective-permute-done((bf16[3,1024]{1,0:T(4,128)(2,1)S(1)}, bf16[3,1024]{1,0:T(4,128)(2,1)S(1)}, u32[]{:S(2)}, u32[]{:S(2)}) %collective-permute-start.2) | collective-permute-done | bytes 6176 | tf_op jit(solution)/shard_map/ppermute | solution.py:51
  11.9 0.0 copy-done.2
  11.9 0.0 copy-done.3
  11.9 0.0 copy-done.4
  11.9 0.0 copy-done.5
  11.9 0.0 copy-done.9
  11.9 0.0 copy-start.15
  11.9 0.0 copy-start
  11.9 0.0 copy-start.8
  11.9 0.0 copy-start.10
  12.0 0.0 copy-start.6
  12.0 0.0 copy-start.7
  12.0 0.0 copy-start.12
  12.0 0.0 copy-start.13
  12.0 0.0 copy-start.14
  12.0 0.0 copy-start.11
  12.0 1.3 %shard_map.186 = (f32[4,3328]{1,0:T(4,128)S(1)}, bf16[4,3328]{1,0:T(4,128)(2,1)S(1)}, bf16[4,3328]{1,0:T(4,128)(2,1)S(1)}, bf16[4,3328]{1,0:T(4,128)(2,1)S(1)}) custom-call(bf16[3,1024]{1,0:T(4,128)(2,1)S(1)} %get-tuple-element.36.refs_0_, bf16[3,1024]{1,0:T(4,128)(2,1)S(1)} %collective-permute-done.refs_1_, ...), custom_call_target="tpu_custom_call" | custom-call | flops 200000000 | tf_op jit(solution)/shard_map/pallas_call | solution.py:31
  13.3 0.0 collective-permute-start.3
  13.3 0.4 collective-permute-start.4
  13.7 4.0 %collective-permute-start.5 = (bf16[4,3328]{1,0:T(4,128)(2,1)S(1)}, bf16[4,3328]{1,0:T(4,128)(2,1)S(1)}, u32[]{:S(2)}, u32[]{:S(2)}) collective-permute-start(bf16[4,3328]{1,0:T(4,128)(2,1)S(1)} %get-tuple-element.43), channel_id=1, source_target_pairs={{0,12},{4,8},{8,4},{12,0},{1,13},{5,9},{9,5},{13,1},{2,14},{6,10},... | collective-permute-start | bytes 79880 | tf_op jit(solution)/shard_map/ppermute | solution.py:67
  18.4 0.0 copy-done.15
  18.4 0.0 copy-done
  18.4 0.0 copy-done.8
  18.4 0.0 copy-done.10
  18.4 0.0 copy-start.1
  18.4 0.4 %shard_map.188 = (bf16[256,2048]{1,0:T(8,128)(2,1)S(1)}, f32[8,2304]{1,0:T(8,128)S(1)}, f32[8,2304]{1,0:T(8,128)S(1)}) custom-call(s32[1]{0:T(128)S(6)} %copy.33.accepted, f32[1,3,32,64,64]{4,3,2,1,0:T(8,128)S(1)} %copy-done, bf16[1,6,2,1152]{3,2,1,0:T(2,128)(2,1)S(1)} %copy-done.8, bf16[4,2,1152]{2,1,0:T(2,128)(2,1)S(1)} %copy-done.10), custom_call_target="tpu_custom_call" | custom-call | flops 20000000 | tf_op jit(solution)/shard_map/pallas_call | solution.py:31
  18.8 0.0 copy-done.6
  18.9 0.0 copy-done.7
  18.9 0.0 copy-done.12
  18.9 0.0 copy-done.13
  18.9 0.0 copy-done.14
  18.9 0.9 %shard_map.187 = (f32[5,8,2048]{2,1,0:T(8,128)S(1)}, f32[8,32]{1,0:T(8,128)S(1)}, f32[8,128]{1,0:T(8,128)S(1)}) custom-call(s32[1]{0:T(128)S(6)} %copy.33.accepted, bf16[1,3,4096]{2,1,0:T(4,128)(2,1)S(1)} %copy-done.7, f32[1,4096]{1,0:T(1,128)S(1)} %bitcast.11, bf16[32,4096]{1,0:T(8,128)(2,1)S(1)} %bitcast.9, f32[1,32]{1,0:T(1,128)S(1)} %bitcast.14, ...), custom_call_target="tpu_custom_call" | custom-call | flops 20000000 | tf_op jit(solution)/shard_map/pallas_call | solution.py:31
  19.8 0.0 collective-permute-done.3.refs_1_
  19.8 0.0 collective-permute-done.4.refs_2_
  19.8 0.0 collective-permute-done.5.refs_3_
  19.8 0.0 copy-done.11
  19.8 0.4 %shard_map.189 = (bf16[4,1536]{1,0:T(4,128)(2,1)S(1)}, f32[8,2304]{1,0:T(8,128)S(1)}, f32[8,2304]{1,0:T(8,128)S(1)}) custom-call(f32[4,3328]{1,0:T(4,128)S(1)} %get-tuple-element.40.refs_0_, bf16[4,3328]{1,0:T(4,128)(2,1)S(1)} %collective-permute-done.3.refs_1_, bf16[4,3328]{1,0:T(4,128)(2,1)S(1)} %collective-permute-done.4.refs_2_, ...), custom_call_target="tpu_custom_call" | custom-call | flops 20000000 | tf_op jit(solution)/shard_map/pallas_call | solution.py:31
  20.3 3.6 %collective-permute-start.8 = (bf16[4,1536]{1,0:T(4,128)(2,1)S(1)}, bf16[4,1536]{1,0:T(4,128)(2,1)S(1)}, u32[]{:S(2)}, u32[]{:S(2)}) collective-permute-start(bf16[4,1536]{1,0:T(4,128)(2,1)S(1)} %get-tuple-element.49.refs_0_), channel_id=1, source_target_pairs={{0,12},{4,0},{8,4},{12,8},{1,13},{5,1},{9,5},{13,9},{2,14},{6,2},{... | collective-permute-start | bytes 36872 | tf_op jit(solution)/shard_map/ppermute | solution.py:59
  23.8 0.0 collective-permute-start.7
  23.8 0.6 %collective-permute-start.6 = (bf16[4,1536]{1,0:T(4,128)(2,1)S(1)}, bf16[4,1536]{1,0:T(4,128)(2,1)S(1)}, u32[]{:S(2)}, u32[]{:S(2)}) collective-permute-start(bf16[4,1536]{1,0:T(4,128)(2,1)S(1)} %get-tuple-element.49.refs_0_), channel_id=1, source_target_pairs={{0,4},{4,8},{8,12},{12,0},{1,5},{5,9},{9,13},{13,1},{2,6},{6,10},{... | collective-permute-start | bytes 36872 | tf_op jit(solution)/shard_map/ppermute | solution.py:59
  24.5 1.2 %shard_map.190 = (f32[1,3,32,64,64]{4,3,2,1,0:T(8,128)}, f32[8,128]{1,0:T(8,128)S(1)}) custom-call(s32[1]{0:T(128)S(6)} %copy.33.accepted, f32[1,3,32,64,64]{4,3,2,1,0:T(8,128)S(1)} %copy-done, f32[8,32]{1,0:T(8,128)S(1)} %get-tuple-element.50.small, f32[8,2304]{1,0:T(8,128)S(1)} %get-tuple-element.51.act, f32[5,8,2048]{2,1,0:T(8,128)S(1)} %get-tuple-element.45.refs_5_.coef), custom_call_target="tpu_custom_call" | custom-call | flops 30000000 | tf_op jit(solution)/shard_map/pallas_call | solution.py:31
  25.7 0.0 collective-permute-done.8.refs_3_
  25.7 2.7 %collective-permute-done.7.refs_2_ = bf16[4,1536]{1,0:T(4,128)(2,1)S(1)} collective-permute-done((bf16[4,1536]{1,0:T(4,128)(2,1)S(1)}, bf16[4,1536]{1,0:T(4,128)(2,1)S(1)}, u32[]{:S(2)}, u32[]{:S(2)}) %collective-permute-start.7) | collective-permute-done | bytes 12320 | tf_op jit(solution)/shard_map/ppermute | solution.py:59
  28.4 0.9 %collective-permute-done.6.refs_1_ = bf16[4,1536]{1,0:T(4,128)(2,1)S(1)} collective-permute-done((bf16[4,1536]{1,0:T(4,128)(2,1)S(1)}, bf16[4,1536]{1,0:T(4,128)(2,1)S(1)}, u32[]{:S(2)}, u32[]{:S(2)}) %collective-permute-start.6) | collective-permute-done | bytes 12320 | tf_op jit(solution)/shard_map/ppermute | solution.py:59
  29.3 0.7 %shard_map.191 = (bf16[4,1024]{1,0:T(4,128)(2,1)S(1)}, bf16[4,1024]{1,0:T(4,128)(2,1)S(1)}, bf16[4,1024]{1,0:T(4,128)(2,1)S(1)}, bf16[4,1024]{1,0:T(4,128)(2,1)S(1)}) custom-call(bf16[4,1536]{1,0:T(4,128)(2,1)S(1)} %get-tuple-element.49.refs_0_, bf16[4,1536]{1,0:T(4,128)(2,1)S(1)} %collective-permute-done.6.refs_1_, ...), custom_call_target="tpu_custom_call" | custom-call | flops 100000000 | tf_op jit(solution)/shard_map/pallas_call | solution.py:31
  30.0 0.1 collective-permute-start.9
  30.1 1.6 %collective-permute-start.10 = (bf16[4,1024]{1,0:T(4,128)(2,1)S(1)}, bf16[4,1024]{1,0:T(4,128)(2,1)S(1)}, u32[]{:S(2)}, u32[]{:S(2)}) collective-permute-start(bf16[4,1024]{1,0:T(4,128)(2,1)S(1)} %get-tuple-element.55), channel_id=1, source_target_pairs={{0,2},{1,3},{2,0},{3,1},{4,6},{5,7},{6,4},{7,5},{8,10},{9,11},{10,... | collective-permute-start | bytes 24584 | tf_op jit(solution)/shard_map/ppermute | solution.py:67
  31.7 0.3 collective-permute-start.11
  32.0 1.8 %shard_map.193 = (f32[1,3,32,64,64]{4,3,2,1,0:T(8,128)}, bf16[1,6,2,1152]{3,2,1,0:T(2,128)(2,1)}) custom-call(s32[1]{0:T(128)S(6)} %copy.33.accepted, f32[1,3,32,64,64]{4,3,2,1,0:T(8,128)S(1)} %copy-done, f32[8,32]{1,0:T(8,128)S(1)} %get-tuple-element.50.small, f32[8,2304]{1,0:T(8,128)S(1)} %get-tuple-element.51.act, ...), custom_call_target="tpu_custom_call", output_to_operand_aliasing={{0}: (7, {})} | custom-call | flops 30000000 | tf_op jit(solution)/shard_map/pallas_call | solution.py:31
  33.8 0.0 collective-permute-done.9.refs_1_
  33.8 0.0 collective-permute-done.10.refs_2_
  33.8 0.9 %collective-permute-done.11.refs_3_ = bf16[4,1024]{1,0:T(4,128)(2,1)S(1)} collective-permute-done((bf16[4,1024]{1,0:T(4,128)(2,1)S(1)}, bf16[4,1024]{1,0:T(4,128)(2,1)S(1)}, u32[]{:S(2)}, u32[]{:S(2)}) %collective-permute-start.11) | collective-permute-done | bytes 8224 | tf_op jit(solution)/shard_map/ppermute | solution.py:67
  34.7 0.6 %shard_map.192 = bf16[1,3,1024]{2,1,0:T(4,128)(2,1)} custom-call(bf16[4,1024]{1,0:T(4,128)(2,1)S(1)} %get-tuple-element.53.refs_0_, bf16[4,1024]{1,0:T(4,128)(2,1)S(1)} %collective-permute-done.9.refs_1_, bf16[4,1024]{1,0:T(4,128)(2,1)S(1)} %collective-permute-done.10.refs_2_, bf16[4,1024]{1,0:T(4,128)(2,1)S(1)} %collective-permute-done.11.refs_3_), custom_call_target="tpu_custom_call" | custom-call | tf_op jit(solution)/shard_map/pallas_call | solution.py:31
  (3 shorter events, 0.0 us)
Async XLA Ops:
  1.4 10.4 %copy-start.2 = (bf16[1024,2048]{1,0:T(8,128)(2,1)S(1)}, bf16[1024,2048]{1,0:T(8,128)(2,1)}, u32[]{:S(2)}) copy-start(bf16[1024,2048]{1,0:T(8,128)(2,1)} %refs_4_.2) | copy-start | bytes 12582916
  1.4 10.4 %copy-start.3 = (bf16[1024,2048]{1,0:T(8,128)(2,1)S(1)}, bf16[1024,2048]{1,0:T(8,128)(2,1)}, u32[]{:S(2)}) copy-start(bf16[1024,2048]{1,0:T(8,128)(2,1)} %refs_7_.1) | copy-start | bytes 12582916
  1.5 10.4 %copy-start.4 = (bf16[1024,128]{1,0:T(8,128)(2,1)S(1)}, bf16[1024,128]{1,0:T(8,128)(2,1)}, u32[]{:S(2)}) copy-start(bf16[1024,128]{1,0:T(8,128)(2,1)} %refs_5_.1) | copy-start | bytes 786436
  1.5 10.4 %copy-start.5 = (bf16[1024,128]{1,0:T(8,128)(2,1)S(1)}, bf16[1024,128]{1,0:T(8,128)(2,1)}, u32[]{:S(2)}) copy-start(bf16[1024,128]{1,0:T(8,128)(2,1)} %refs_6_.1) | copy-start | bytes 786436
  1.5 10.4 %copy-start.9 = (f32[4096]{0:T(1024)S(1)}, f32[4096]{0:T(1024)}, u32[]{:S(2)}) copy-start(f32[4096]{0:T(1024)} %param.18) | copy-start | bytes 49156
  1.5 5.4 %collective-permute-start = (bf16[3,1024]{1,0:T(4,128)(2,1)S(1)}, bf16[3,1024]{1,0:T(4,128)(2,1)S(1)}, u32[]{:S(2)}, u32[]{:S(2)}) collective-permute-start(bf16[3,1024]{1,0:T(4,128)(2,1)S(1)} %get-tuple-element.37), channel_id=1, source_target_pairs={{0,5},{1,4},{2,7},{3,6},{4,1},{5,0},{6,3},{7,2},{8,13},{9,12},{10,... | collective-permute-start | bytes 18440 | tf_op jit(solution)/shard_map/ppermute | solution.py:51
  4.1 4.3 %collective-permute-start.1 = (bf16[3,1024]{1,0:T(4,128)(2,1)S(1)}, bf16[3,1024]{1,0:T(4,128)(2,1)S(1)}, u32[]{:S(2)}, u32[]{:S(2)}) collective-permute-start(bf16[3,1024]{1,0:T(4,128)(2,1)S(1)} %get-tuple-element.38), channel_id=1, source_target_pairs={{0,9},{1,8},{2,11},{3,10},{4,13},{5,12},{6,15},{7,14},{8,1},{9,0},... | collective-permute-start | bytes 18440 | tf_op jit(solution)/shard_map/ppermute | solution.py:51
  6.9 4.9 %collective-permute-start.2 = (bf16[3,1024]{1,0:T(4,128)(2,1)S(1)}, bf16[3,1024]{1,0:T(4,128)(2,1)S(1)}, u32[]{:S(2)}, u32[]{:S(2)}) collective-permute-start(bf16[3,1024]{1,0:T(4,128)(2,1)S(1)} %get-tuple-element.39), channel_id=1, source_target_pairs={{0,13},{1,12},{2,15},{3,14},{4,9},{5,8},{6,11},{7,10},{8,5},{9,4},... | collective-permute-start | bytes 18440 | tf_op jit(solution)/shard_map/ppermute | solution.py:51
  11.9 6.5 %copy-start.15 = (f32[1,3,32]{2,0,1:T(1,128)S(1)}, f32[1,3,32]{2,0,1:T(1,128)}, u32[]{:S(2)}) copy-start(f32[1,3,32]{2,0,1:T(1,128)} %param.31) | copy-start | bytes 1156
  11.9 6.5 %copy-start = (f32[1,3,32,64,64]{4,3,2,1,0:T(8,128)S(1)}, f32[1,3,32,64,64]{4,3,2,1,0:T(8,128)}, u32[]{:S(2)}) copy-start(f32[1,3,32,64,64]{4,3,2,1,0:T(8,128)} %start.3) | copy-start | bytes 4718596
  11.9 6.5 %copy-start.8 = (bf16[1,6,2,1152]{3,2,1,0:T(2,128)(2,1)S(1)}, bf16[1,6,2,1152]{3,2,1,0:T(2,128)(2,1)}, u32[]{:S(2)}) copy-start(bf16[1,6,2,1152]{3,2,1,0:T(2,128)(2,1)} %refs_1_.1) | copy-start | bytes 82948
  11.9 6.5 %copy-start.10 = (bf16[4,2,1152]{2,1,0:T(2,128)(2,1)S(1)}, bf16[4,2,1152]{2,1,0:T(2,128)(2,1)}, u32[]{:S(2)}) copy-start(bf16[4,2,1152]{2,1,0:T(2,128)(2,1)} %taps.1) | copy-start | bytes 55300
  12.0 6.9 %copy-start.6 = (bf16[4096,32]{0,1:T(8,128)(2,1)S(1)}, bf16[4096,32]{0,1:T(8,128)(2,1)}, u32[]{:S(2)}) copy-start(bf16[4096,32]{0,1:T(8,128)(2,1)} %param.23) | copy-start | bytes 786436
  12.0 6.9 %copy-start.7 = (bf16[1,3,4096]{2,1,0:T(4,128)(2,1)S(1)}, bf16[1,3,4096]{2,1,0:T(4,128)(2,1)}, u32[]{:S(2)}) copy-start(bf16[1,3,4096]{2,1,0:T(4,128)(2,1)} %tokens.3) | copy-start | bytes 73732
  12.0 6.9 %copy-start.12 = (f32[32]{0:T(128)S(1)}, f32[32]{0:T(128)}, u32[]{:S(2)}) copy-start(f32[32]{0:T(128)} %param.24) | copy-start | bytes 388
  12.0 6.9 %copy-start.13 = (f32[32]{0:T(128)S(1)}, f32[32]{0:T(128)}, u32[]{:S(2)}) copy-start(f32[32]{0:T(128)} %param.25) | copy-start | bytes 388
  12.0 6.9 %copy-start.14 = (f32[32]{0:T(128)S(1)}, f32[32]{0:T(128)}, u32[]{:S(2)}) copy-start(f32[32]{0:T(128)} %param.26) | copy-start | bytes 388
  12.0 7.8 %copy-start.11 = (f32[2048]{0:T(1024)S(1)}, f32[2048]{0:T(1024)}, u32[]{:S(2)}) copy-start(f32[2048]{0:T(1024)} %param.32) | copy-start | bytes 24580
  13.3 6.4 %collective-permute-start.3 = (bf16[4,3328]{1,0:T(4,128)(2,1)S(1)}, bf16[4,3328]{1,0:T(4,128)(2,1)S(1)}, u32[]{:S(2)}, u32[]{:S(2)}) collective-permute-start(bf16[4,3328]{1,0:T(4,128)(2,1)S(1)} %get-tuple-element.41), channel_id=1, source_target_pairs={{0,4},{4,0},{8,12},{12,8},{1,5},{5,1},{9,13},{13,9},{2,6},{6,2},{1... | collective-permute-start | bytes 79880 | tf_op jit(solution)/shard_map/ppermute | solution.py:67
  13.3 6.4 %collective-permute-start.4 = (bf16[4,3328]{1,0:T(4,128)(2,1)S(1)}, bf16[4,3328]{1,0:T(4,128)(2,1)S(1)}, u32[]{:S(2)}, u32[]{:S(2)}) collective-permute-start(bf16[4,3328]{1,0:T(4,128)(2,1)S(1)} %get-tuple-element.42), channel_id=1, source_target_pairs={{0,8},{4,12},{8,0},{12,4},{1,9},{5,13},{9,1},{13,5},{2,10},{6,14},... | collective-permute-start | bytes 79880 | tf_op jit(solution)/shard_map/ppermute | solution.py:67
  13.7 6.1 %collective-permute-start.5 = (bf16[4,3328]{1,0:T(4,128)(2,1)S(1)}, bf16[4,3328]{1,0:T(4,128)(2,1)S(1)}, u32[]{:S(2)}, u32[]{:S(2)}) collective-permute-start(bf16[4,3328]{1,0:T(4,128)(2,1)S(1)} %get-tuple-element.43), channel_id=1, source_target_pairs={{0,12},{4,8},{8,4},{12,0},{1,13},{5,9},{9,5},{13,1},{2,14},{6,10},... | collective-permute-start | bytes 79880 | tf_op jit(solution)/shard_map/ppermute | solution.py:67
  18.4 10.9 %copy-start.1 = (bf16[2048,1024]{1,0:T(8,128)(2,1)S(1)}, bf16[2048,1024]{1,0:T(8,128)(2,1)}, u32[]{:S(2)}) copy-start(bf16[2048,1024]{1,0:T(8,128)(2,1)} %refs_4_.3) | copy-start | bytes 12582916
  20.3 5.4 %collective-permute-start.8 = (bf16[4,1536]{1,0:T(4,128)(2,1)S(1)}, bf16[4,1536]{1,0:T(4,128)(2,1)S(1)}, u32[]{:S(2)}, u32[]{:S(2)}) collective-permute-start(bf16[4,1536]{1,0:T(4,128)(2,1)S(1)} %get-tuple-element.49.refs_0_), channel_id=1, source_target_pairs={{0,12},{4,0},{8,4},{12,8},{1,13},{5,1},{9,5},{13,9},{2,14},{6,2},{... | collective-permute-start | bytes 36872 | tf_op jit(solution)/shard_map/ppermute | solution.py:59
  23.8 4.6 %collective-permute-start.7 = (bf16[4,1536]{1,0:T(4,128)(2,1)S(1)}, bf16[4,1536]{1,0:T(4,128)(2,1)S(1)}, u32[]{:S(2)}, u32[]{:S(2)}) collective-permute-start(bf16[4,1536]{1,0:T(4,128)(2,1)S(1)} %get-tuple-element.49.refs_0_), channel_id=1, source_target_pairs={{0,8},{4,12},{8,0},{12,4},{1,9},{5,13},{9,1},{13,5},{2,10},{6,14},... | collective-permute-start | bytes 36872 | tf_op jit(solution)/shard_map/ppermute | solution.py:59
  23.8 5.5 %collective-permute-start.6 = (bf16[4,1536]{1,0:T(4,128)(2,1)S(1)}, bf16[4,1536]{1,0:T(4,128)(2,1)S(1)}, u32[]{:S(2)}, u32[]{:S(2)}) collective-permute-start(bf16[4,1536]{1,0:T(4,128)(2,1)S(1)} %get-tuple-element.49.refs_0_), channel_id=1, source_target_pairs={{0,4},{4,8},{8,12},{12,0},{1,5},{5,9},{9,13},{13,1},{2,6},{6,10},{... | collective-permute-start | bytes 36872 | tf_op jit(solution)/shard_map/ppermute | solution.py:59
  30.0 3.7 %collective-permute-start.9 = (bf16[4,1024]{1,0:T(4,128)(2,1)S(1)}, bf16[4,1024]{1,0:T(4,128)(2,1)S(1)}, u32[]{:S(2)}, u32[]{:S(2)}) collective-permute-start(bf16[4,1024]{1,0:T(4,128)(2,1)S(1)} %get-tuple-element.54), channel_id=1, source_target_pairs={{0,1},{1,0},{2,3},{3,2},{4,5},{5,4},{6,7},{7,6},{8,9},{9,8},{10,11... | collective-permute-start | bytes 24584 | tf_op jit(solution)/shard_map/ppermute | solution.py:67
  30.1 3.7 %collective-permute-start.10 = (bf16[4,1024]{1,0:T(4,128)(2,1)S(1)}, bf16[4,1024]{1,0:T(4,128)(2,1)S(1)}, u32[]{:S(2)}, u32[]{:S(2)}) collective-permute-start(bf16[4,1024]{1,0:T(4,128)(2,1)S(1)} %get-tuple-element.55), channel_id=1, source_target_pairs={{0,2},{1,3},{2,0},{3,1},{4,6},{5,7},{6,4},{7,5},{8,10},{9,11},{10,... | collective-permute-start | bytes 24584 | tf_op jit(solution)/shard_map/ppermute | solution.py:67
  31.7 3.1 %collective-permute-start.11 = (bf16[4,1024]{1,0:T(4,128)(2,1)S(1)}, bf16[4,1024]{1,0:T(4,128)(2,1)S(1)}, u32[]{:S(2)}, u32[]{:S(2)}) collective-permute-start(bf16[4,1024]{1,0:T(4,128)(2,1)S(1)} %get-tuple-element.56), channel_id=1, source_target_pairs={{0,3},{1,2},{2,1},{3,0},{4,7},{5,6},{6,5},{7,4},{8,11},{9,10},{10,... | collective-permute-start | bytes 24584 | tf_op jit(solution)/shard_map/ppermute | solution.py:67
